TPU v7x, 256 devices: a whole 4x4x8 slice. The times are simulated.
256 devices in a mesh: ep: 64 (over z, x, core), tp: 4 (over y).
Axes of the slice: x: 4, y: 4, z: 8, core: 2. Of those that a mesh axis runs over, the one named last changes fastest.
Arguments:
- tokens: bfloat16 [1024, 2048], P('ep'), may hold values from -6 to 6
- attn_gain: bfloat16 [2048], replicated, may hold values from 0.099609375 to 1.8984375
- query_weight: bfloat16 [2048, 1024], P('ep', 'tp'), may hold values from -0.125 to 0.125
- key_weight: bfloat16 [2048, 512], P('ep', 'tp'), may hold values from -0.125 to 0.125
- value_weight: bfloat16 [2048, 512], P('ep', 'tp'), may hold values from -0.125 to 0.125
- out_weight: bfloat16 [2048, 1024], P('ep', 'tp'), may hold values from -0.1875 to 0.1875
- head_gain: bfloat16 [1024], P('tp'), may hold values from 0.099609375 to 1.8984375
- past_keys: bfloat16 [1024, 1024, 4, 128], P('ep', None, 'tp'), may hold values from -6 to 6
- past_values: bfloat16 [1024, 1024, 4, 128], P('ep', None, 'tp'), may hold values from -50 to 50
- break_offset: float32 [1024, 8, 1024], P('ep', 'tp'), may hold values from -12.5 to 1
- cache_lengths: int32 [1024], P('ep'), may hold values from 1 to 1024, 524288 in all
- ffn_gain: bfloat16 [2048], replicated, may hold values from 0.099609375 to 1.8984375
- router_weight: bfloat16 [2048, 64], replicated, may hold values from -0.25 to 0.25
- expert_routes: int32 [1024, 6], P('ep'), may hold values from 0 to 63, all different within a row; in each aligned block of 16 rows (0 to 15, 16 to 31, ...) at most 3 rows name the same one
- expert_gate: bfloat16 [64, 2048, 512], P('ep', None, 'tp'), may hold values from -0.125 to 0.125
- expert_up: bfloat16 [64, 2048, 512], P('ep', None, 'tp'), may hold values from -0.125 to 0.125
- expert_down: bfloat16 [64, 512, 2048], P('ep', 'tp'), may hold values from -0.25 to 0.25
- shared_gate: bfloat16 [2048, 512], P(None, 'tp'), may hold values from -0.125 to 0.125
- shared_up: bfloat16 [2048, 512], P(None, 'tp'), may hold values from -0.125 to 0.125
- shared_down: bfloat16 [512, 2048], P('tp'), may hold values from -0.25 to 0.25
Outputs:
- mixed: bfloat16 [1024, 2048], P('ep', 'tp')
- fresh_keys: bfloat16 [1024, 512], P('ep', 'tp')
- fresh_values: bfloat16 [1024, 512], P('ep', 'tp')
Inputs may be any that keep to these rules, and one draw needn't show every extreme that they name: `cache_lengths`: the lengths add up to half of 1048576, and some sequence has length 1024. `expert_routes`: each row names 6 different experts. Among the rows of one device no expert is named more than 3 times, and 3 is reached in some device's rows.
All inputs are finite; a program needn't handle non-finite values. No bound on the sum of `cache_lengths` on one device may be relied on, other than what follows from the above.
Results may differ from a plain program's by a relative error of at most 0.0095.
Values may be sent and summed in bfloat16 or wider, within the bound.
A program may use at most 64 MiB of HBM per device.

v0:
```python
import jax
import jax.numpy as jnp
from jax import lax
from jax.sharding import Mesh
from jax.sharding import PartitionSpec as P

HQ = 8
HD = 128
EP = ("ep_0", "ep_1", "ep_2")


epsilon = 1e-06
routed_scale = 2.5


def copy_for_each(array, axis):
    devices = lax.axis_size(axis)
    return lax.all_to_all(
        jnp.broadcast_to(array[None], (devices, *array.shape)), axis, 0, 0, tiled=True
    )


def laid_out(parts, dim):
    shape = list(parts.shape[1:])
    shape[dim] *= parts.shape[0]
    return jnp.moveaxis(parts, 0, dim).reshape(shape)


def gathered_by_axis(array, axes, dim):
    far, near = axes
    initial = copy_for_each(array, far)
    parts = jnp.swapaxes(copy_for_each(initial, near), 0, 1)
    return laid_out(parts.reshape(-1, *array.shape), dim)


def side_by_side(arrays, axis, dim, along):
    both = jnp.concatenate(arrays, axis=along)
    filled, at, outs = (gathered_by_axis(both, axis, dim), 0, [])
    for a in arrays:
        outs.append(lax.slice_in_dim(filled, at, at + a.shape[along], axis=along))
        at += a.shape[along]
    return tuple(outs)


def collect(array, axis, dim):
    return laid_out(copy_for_each(array, axis), dim)


def over_copies(array, axis):
    return copy_for_each(array, axis).sum(axis=0)


def root_norm(values, gain):
    data = values.astype(jnp.float32)
    factor = lax.rsqrt(jnp.mean(data * data, axis=-1, keepdims=True) + epsilon)
    return (data * factor * gain.astype(jnp.float32)).astype(jnp.bfloat16)


def stick_attend(queries, key_cache, value_cache, offsets, lengths):
    seq_count, positions, key_heads, head_size = key_cache.shape
    heads_local = offsets.shape[1]
    group_size = heads_local // key_heads
    grouped = queries.reshape(seq_count, key_heads, group_size, head_size)
    scores = jnp.einsum("bgrd,blgd->bgrl", grouped, key_cache, preferred_element_type=jnp.float32)
    logits = scores.reshape(seq_count, heads_local, positions) * head_size ** (-0.5) + offsets
    places = lax.broadcasted_iota(jnp.int32, (1, 1, positions), 2)
    usable = places < lengths[:, None, None]
    keep_log = jnp.where(usable, jax.nn.log_sigmoid(-logits), 0.0)
    after_sum = jnp.sum(keep_log, axis=-1, keepdims=True) - jnp.cumsum(keep_log, axis=-1)
    sticks = jnp.where(usable, jnp.exp(jax.nn.log_sigmoid(logits) + after_sum), 0.0).astype(
        jnp.bfloat16
    )
    sticks = sticks.reshape(seq_count, key_heads, group_size, positions)
    outputs = jnp.einsum("bgrl,blgd->bgrd", sticks, value_cache, preferred_element_type=jnp.float32)
    return outputs.reshape(seq_count, heads_local * head_size)


def body(
    tokens,
    attn_gain,
    query_weight,
    key_weight,
    value_weight,
    out_weight,
    head_gain,
    past_keys,
    past_values,
    break_offset,
    cache_lengths,
    ffn_gain,
    router_weight,
    expert_routes,
    expert_gate,
    expert_up,
    expert_down,
    shared_gate,
    shared_up,
    shared_down,
):
    seq_count = tokens.shape[0]
    model_width = tokens.shape[1]
    query_cols = query_weight.shape[1]
    key_cols = key_weight.shape[1]
    normed = root_norm(tokens, attn_gain)
    query_piece, key_piece, value_piece, out_piece = side_by_side(
        (query_weight, key_weight, value_weight, out_weight), (("ep_0", "ep_1"), "ep_2"), 0, 1
    )
    joined = jnp.concatenate([query_piece, key_piece, value_piece], axis=1)
    totals = jnp.dot(normed, joined, preferred_element_type=jnp.float32)
    queries = totals[:, :query_cols].astype(jnp.bfloat16)
    fresh_keys = totals[:, query_cols : query_cols + key_cols].astype(jnp.bfloat16)
    fresh_values = totals[:, query_cols + key_cols :].astype(jnp.bfloat16)
    experts = router_weight.shape[1]
    top_count = expert_routes.shape[1]
    capacity = max(2, min(seq_count, (2 * seq_count * top_count + experts - 1) // experts))
    local_experts = expert_gate.shape[0]
    column_width = model_width // lax.axis_size("tp")
    block_count = 1
    block_rows = seq_count // block_count
    heads_out = stick_attend(queries, past_keys, past_values, break_offset, cache_lengths)
    scaled = (heads_out * head_gain.astype(jnp.float32)).astype(jnp.bfloat16)
    square_sum = jnp.sum(heads_out * heads_out, axis=-1)
    partial_value = jnp.einsum(
        "nc,dc->nd", scaled, out_piece, preferred_element_type=jnp.float32
    ).astype(jnp.bfloat16)
    all_parts = collect(partial_value[None], "tp", 0)
    head_total = jnp.sum(all_parts.astype(jnp.float32), axis=0)
    square_total = over_copies(square_sum, "tp")
    attention = head_total * lax.rsqrt(square_total[:, None] / (HQ * HD) + epsilon)
    residual = (tokens.astype(jnp.float32) + attention).astype(jnp.bfloat16)
    normed_ffn = root_norm(residual, ffn_gain)
    router_prob = jax.nn.sigmoid(
        jnp.dot(normed_ffn, router_weight, preferred_element_type=jnp.float32)
    )
    chosen = expert_routes[:, :, None] == lax.broadcasted_iota(jnp.int32, (1, 1, experts), 2)
    picked = jnp.sum(jnp.where(chosen, router_prob[:, None, :], 0.0), axis=-1)
    route_weight = routed_scale * picked / jnp.sum(picked, axis=-1, keepdims=True)
    flat_hot = chosen.reshape(block_rows * top_count, experts).astype(jnp.int32)
    earlier = jnp.cumsum(flat_hot, axis=0) - flat_hot
    slot_index = jnp.sum(earlier * flat_hot, axis=-1).reshape(block_rows, top_count)
    slot_hot = (
        slot_index[:, :, None] == lax.broadcasted_iota(jnp.int32, (1, 1, capacity), 2)
    ).astype(jnp.float32)
    expert_hot = chosen.astype(jnp.float32)
    dispatch = jnp.einsum("ske,skc->ecs", expert_hot, slot_hot)
    weighted = jnp.sum(
        route_weight[:, :, None, None] * expert_hot[:, :, :, None] * slot_hot[:, :, None, :], axis=1
    )
    outbound = jnp.einsum(
        "ecs,sd->ecd", dispatch.astype(jnp.bfloat16), normed_ffn, preferred_element_type=jnp.float32
    ).astype(jnp.bfloat16)
    arrived = lax.all_to_all(outbound, EP, split_axis=0, concat_axis=0, tiled=True)
    item_count = arrived.shape[1]
    sources = arrived.shape[0] // local_experts
    grouped = arrived.reshape(sources, local_experts, item_count, model_width)
    gate_part = jnp.einsum(
        "sxcd,xdf->sxcf", grouped, expert_gate, preferred_element_type=jnp.float32
    )
    up_part = jnp.einsum("sxcd,xdf->sxcf", grouped, expert_up, preferred_element_type=jnp.float32)
    hidden = (jax.nn.silu(gate_part) * up_part).astype(jnp.bfloat16)
    down_part = jnp.einsum(
        "sxcf,xfd->sxcd", hidden, expert_down, preferred_element_type=jnp.float32
    )
    expert_part = down_part.astype(jnp.bfloat16).reshape(arrived.shape)
    shared_hidden = (
        jax.nn.silu(jnp.dot(normed_ffn, shared_gate, preferred_element_type=jnp.float32))
        * jnp.dot(normed_ffn, shared_up, preferred_element_type=jnp.float32)
    ).astype(jnp.bfloat16)
    shared_part = jnp.dot(shared_hidden, shared_down, preferred_element_type=jnp.float32).astype(
        jnp.bfloat16
    )
    expert_pieces = lax.all_to_all(expert_part[None], "tp", split_axis=3, concat_axis=0, tiled=True)
    shared_pieces = lax.all_to_all(
        shared_part[None, None], "tp", split_axis=3, concat_axis=0, tiled=True
    )
    expert_total = jnp.sum(expert_pieces.astype(jnp.float32), axis=0)
    shared_total = jnp.sum(shared_pieces.astype(jnp.float32), axis=0)
    returned = lax.all_to_all(
        expert_total.astype(jnp.bfloat16), EP, split_axis=0, concat_axis=0, tiled=True
    )
    routed = jnp.einsum("sec,ecd->sd", weighted, returned.astype(jnp.float32))
    own_cols = lax.dynamic_slice_in_dim(
        residual, lax.axis_index("tp") * column_width, column_width, 1
    )
    results = (own_cols.astype(jnp.float32) + routed + shared_total[0]).astype(jnp.bfloat16)
    return (results, fresh_keys, fresh_values)


def solution(mesh):
    torus = Mesh(mesh.devices.reshape(8, 4, 2, mesh.shape["tp"]), ("ep_0", "ep_1", "ep_2", "tp"))
    return jax.shard_map(
        body,
        mesh=torus,
        in_specs=(
            P(EP, None),
            P(),
            P(EP, "tp"),
            P(EP, "tp"),
            P(EP, "tp"),
            P(EP, "tp"),
            P("tp"),
            P(EP, None, "tp", None),
            P(EP, None, "tp", None),
            P(EP, "tp", None),
            P(EP),
            P(),
            P(),
            P(EP, None),
            P(EP, None, "tp"),
            P(EP, None, "tp"),
            P(EP, "tp", None),
            P(None, "tp"),
            P(None, "tp"),
            P("tp", None),
        ),
        out_specs=(P(EP, "tp"), P(EP, "tp"), P(EP, "tp")),
        check_vma=False,
    )
```

profile of v0, /device:TPU:1, one launch (start us, length us, event | category | flops | bytes accessed | tf_op | source)
XLA Modules:
  0.0 194.7 jit_solution(5498122915484708113)
XLA Ops:
  2.9 11.9 %all-to-all-start = ((bf16[32,32,768]{2,1,0:T(8,128)(2,1)}), bf16[32,32,768]{2,1,0:T(8,128)(2,1)S(1)}, u32[]{:S(2)}, u32[]{:S(2)}) async-start(bf16[32,32,768]{2,1,0:T(8,128)(2,1)} %broadcast_in_dim.33), calls=%async_computation | async-start | bytes 3145728 | tf_op jit(solution)/shard_map/all_to_all | solution.py:18
  16.0 36.7 %all-to-all-done = bf16[32,32,768]{2,1,0:T(8,128)(2,1)S(1)} async-done(((bf16[32,32,768]{2,1,0:T(8,128)(2,1)}), bf16[32,32,768]{2,1,0:T(8,128)(2,1)S(1)}, u32[]{:S(2)}, u32[]{:S(2)}) %all-to-all-start) | async-done | bytes 1572896 | tf_op jit(solution)/shard_map/all_to_all | solution.py:18
  53.0 8.1 %all_to_all.52 = bf16[2,32,32,768]{3,2,1,0:T(8,128)(2,1)S(1)} all-to-all(bf16[2,32,32,768]{3,2,1,0:T(8,128)(2,1)S(1)} %broadcast_in_dim.34), channel_id=1, replica_groups=mesh['ep_0'=8,'ep_1'=4,'ep_2'=2,'tp'=4] {'ep_2'}, dimensions={0} | all-to-all | bytes 6291456 | tf_op jit(solution)/shard_map/all_to_all | solution.py:18
  61.4 1.7 copy-done.1
  63.5 3.4 %fusion.75 = (u16[2,1024]{1,0:T(2,128)(2,1)S(1)}, f32[16,2,1024]{2,1,0:T(2,128)S(1)}) fusion(f32[16,2,1024]{2,1,0:T(2,128)S(1)} %copy-done.7, bf16[16,2,128]{2,1,0:T(2,128)(2,1)S(1)} %reshape.175, bf16[16,1024,1,128]{3,1,2,0:T(8,128)(2,1)} %param.27), kind=kOutput, calls=%fused_computation.90 | convolution fusion | flops 8615936 | bytes 4468736 | tf_op jit(solution)/shard_map/bgrd,blgd->bgrl/dot_general | solution.py:64
  67.4 9.0 %reduce-window.6 = f32[16,2,8,128]{3,2,1,0:T(8,128)S(1)} reduce-window(f32[16,2,8,128]{3,2,1,0:T(8,128)S(1)} %reshape.177, f32[]{:T(128)} %constant.20.clone.1), window={size=1x1x1x128 pad=0_0x0_0x0_0x127_0}, to_apply=%region_2.3 | reduce-window | flops 4161536 | bytes 262148 | tf_op jit(solution)/shard_map/reduce-window
  77.0 3.5 %multiply_reduce_fusion.1 = (f32[16]{0:T(128)S(1)}, f32[16,2,128]{2,1,0:T(2,128)S(1)}) fusion(bf16[16,1024,1,128]{3,1,2,0:T(8,128)(2,1)} %param.28, f32[16,2,1024]{2,1,0:T(2,128)S(1)} %reduce_window_sum.27, f32[16,2,1024]{2,1,0:T(2,128)S(1)} %get-tuple-element.10, pred[16,1024]{1,0:T(8,128)(4,1)S(1)} %iota_compare_fusion.2, ...), kind=kOutput, calls=%fused_computation.102 | convolution fusion | flops 9151503 | bytes 4493376 | tf_op jit(solution)/shard_map/bgrl,blgd->bgrd/dot_general | solution.py:74
  81.1 4.2 %all-to-all-start.3 = ((f32[4,1,16]{2,1,0:T(1,128)}), f32[4,1,16]{2,1,0:T(1,128)S(1)}, u32[]{:S(2)}, u32[]{:S(2)}) async-start(f32[4,1,16]{2,1,0:T(1,128)} %broadcast_in_dim.36), calls=%async_computation.3 | async-start | bytes 4096 | tf_op jit(solution)/shard_map/all_to_all | solution.py:18
  85.2 1.6 convolution_convert_fusion.3
  86.8 2.5 %all-to-all-done.3 = f32[4,1,16]{2,1,0:T(1,128)S(1)} async-done(((f32[4,1,16]{2,1,0:T(1,128)}), f32[4,1,16]{2,1,0:T(1,128)S(1)}, u32[]{:S(2)}, u32[]{:S(2)}) %all-to-all-start.3) | async-done | bytes 288 | tf_op jit(solution)/shard_map/all_to_all | solution.py:18
  90.0 3.4 %all-to-all-start.2 = ((bf16[4,1,16,2048]{3,2,1,0:T(8,128)(2,1)}), bf16[4,1,16,2048]{3,2,1,0:T(8,128)(2,1)S(1)}, u32[]{:S(2)}, u32[]{:S(2)}) async-start(bf16[4,1,16,2048]{3,2,1,0:T(8,128)(2,1)} %broadcast_in_dim.35), calls=%async_computation.2 | async-start | bytes 524288 | tf_op jit(solution)/shard_map/all_to_all | solution.py:18
  93.5 5.5 %all-to-all-done.2 = bf16[4,1,16,2048]{3,2,1,0:T(8,128)(2,1)S(1)} async-done(((bf16[4,1,16,2048]{3,2,1,0:T(8,128)(2,1)}), bf16[4,1,16,2048]{3,2,1,0:T(8,128)(2,1)S(1)}, u32[]{:S(2)}, u32[]{:S(2)}) %all-to-all-start.2) | async-done | bytes 262176 | tf_op jit(solution)/shard_map/all_to_all | solution.py:18
  99.6 1.7 copy.82
  101.3 8.9 %all-to-all-start.4 = ((bf16[64,3,2048]{2,1,0:T(4,128)(2,1)}), bf16[64,3,2048]{2,1,0:T(4,128)(2,1)S(1)}, u32[]{:S(2)}, u32[]{:S(2)}) async-start(bf16[64,3,2048]{2,1,0:T(4,128)(2,1)} %copy.82), calls=%async_computation.4 | async-start | bytes 2097152 | tf_op jit(solution)/shard_map/all_to_all | solution.py:152
  111.7 26.6 %all-to-all-done.4 = bf16[64,3,2048]{2,1,0:T(4,128)(2,1)S(1)} async-done(((bf16[64,3,2048]{2,1,0:T(4,128)(2,1)}), bf16[64,3,2048]{2,1,0:T(4,128)(2,1)S(1)}, u32[]{:S(2)}, u32[]{:S(2)}) %all-to-all-start.4) | async-done | bytes 786464 | tf_op jit(solution)/shard_map/all_to_all | solution.py:152
  140.6 1.4 copy.85
  142.0 2.5 %reshape.193 = bf16[4,2,49152]{2,1,0:T(2,128)(2,1)} reshape(bf16[2048,1,3,64]{3,2,1,0:T(4,128)(2,1)S(1)} %bitcast.101) | data formatting | bytes 1572864
  144.5 3.8 %all-to-all-start.5 = ((bf16[4,2,49152]{2,1,0:T(2,128)(2,1)}), bf16[4,2,49152]{2,1,0:T(2,128)(2,1)S(1)}, u32[]{:S(2)}, u32[]{:S(2)}) async-start(bf16[4,2,49152]{2,1,0:T(2,128)(2,1)} %reshape.193), calls=%async_computation.5 | async-start | bytes 1572864 | tf_op jit(solution)/shard_map/all_to_all | solution.py:172
  148.3 1.4 fusion.6
  151.1 11.5 %reduce.14 = bf16[2048,16]{1,0:T(8,128)(2,1)S(1)} reduce(bf16[2048,1,1,16]{3,2,1,0:T(2,128)(2,1)S(1)} %bitcast.104, bf16[]{:T(256)} %broadcast.143), dimensions={1,2}, to_apply=%bitcast.85.reduce_sub_computation | reduce | bytes 131074
  164.4 4.0 %all-to-all-start.7 = ((bf16[4,2,4096]{2,1,0:T(2,128)(2,1)}), bf16[4,2,4096]{2,1,0:T(2,128)(2,1)S(1)}, u32[]{:S(2)}, u32[]{:S(2)}) async-start(bf16[4,2,4096]{2,1,0:T(2,128)(2,1)} %reshape.191), calls=%async_computation.7 | async-start | bytes 131072 | tf_op jit(solution)/shard_map/all_to_all | solution.py:173
  170.4 2.0 %reduce_sum.121 = bf16[64,3,512]{0,1,2:T(4,128)(2,1)S(1)} reduce(bf16[64,3,4,512]{0,1,3,2:T(4,128)(2,1)S(1)} %bitcast.100, bf16[]{:T(256)} %constant.44.clone.1), dimensions={2}, to_apply=%region_13.14 | reduce | flops 294912 | bytes 983042 | tf_op jit(solution)/shard_map/reduce_sum | solution.py:176
  173.5 7.4 %all-to-all-start.6 = ((bf16[64,3,512]{2,1,0:T(4,128)(2,1)}), bf16[64,3,512]{2,1,0:T(4,128)(2,1)S(1)}, u32[]{:S(2)}, u32[]{:S(2)}) async-start(bf16[64,3,512]{2,1,0:T(4,128)(2,1)} %copy.86), calls=%async_computation.6 | async-start | bytes 524288 | tf_op jit(solution)/shard_map/all_to_all | solution.py:178
  183.2 10.7 %all-to-all-done.6 = bf16[64,3,512]{2,1,0:T(4,128)(2,1)S(1)} async-done(((bf16[64,3,512]{2,1,0:T(4,128)(2,1)}), bf16[64,3,512]{2,1,0:T(4,128)(2,1)S(1)}, u32[]{:S(2)}, u32[]{:S(2)}) %all-to-all-start.6) | async-done | bytes 196640 | tf_op jit(solution)/shard_map/all_to_all | solution.py:178
  (92 shorter events, 20.5 us)
Async XLA Ops:
  0.6 138.7 %copy-start = (bf16[1,128,2048]{2,1,0:T(8,128)(2,1)S(1)}, bf16[1,128,2048]{2,1,0:T(8,128)(2,1)}, u32[]{:S(2)}) copy-start(bf16[1,128,2048]{2,1,0:T(8,128)(2,1)} %param.36) | copy-start | bytes 1572868
  0.6 14.1 %copy-start.9 = (bf16[2048]{0:T(1024)(128)(2,1)S(1)}, bf16[2048]{0:T(1024)(128)(2,1)}, u32[]{:S(2)}) copy-start(bf16[2048]{0:T(1024)(128)(2,1)} %param.21) | copy-start | bytes 12292
  0.7 14.1 %copy-start.15 = (bf16[256]{0:T(256)(128)(2,1)S(1)}, bf16[256]{0:T(256)(128)(2,1)}, u32[]{:S(2)}) copy-start(bf16[256]{0:T(256)(128)(2,1)} %param.26) | copy-start | bytes 1540
  0.7 14.1 %copy-start.10 = (s32[16,6]{0,1:T(8,128)S(1)}, s32[16,6]{0,1:T(8,128)}, u32[]{:S(2)}) copy-start(s32[16,6]{0,1:T(8,128)} %param.33) | copy-start | bytes 1156
  0.7 14.8 %copy-start.11 = (bf16[2048]{0:T(1024)(128)(2,1)S(1)}, bf16[2048]{0:T(1024)(128)(2,1)}, u32[]{:S(2)}) copy-start(bf16[2048]{0:T(1024)(128)(2,1)} %param.31) | copy-start | bytes 12292
  0.7 14.8 %copy-start.5 = (bf16[16,2048]{1,0:T(8,128)(2,1)S(1)}, bf16[16,2048]{1,0:T(8,128)(2,1)}, u32[]{:S(2)}) copy-start(bf16[16,2048]{1,0:T(8,128)(2,1)} %param.20) | copy-start | bytes 196612
  0.7 15.0 %copy-start.12 = (s32[16]{0:T(128)S(1)}, s32[16]{0:T(128)}, u32[]{:S(2)}) copy-start(s32[16]{0:T(128)} %param.30) | copy-start | bytes 196
  2.9 49.7 %all-to-all-start = ((bf16[32,32,768]{2,1,0:T(8,128)(2,1)}), bf16[32,32,768]{2,1,0:T(8,128)(2,1)S(1)}, u32[]{:S(2)}, u32[]{:S(2)}) async-start(bf16[32,32,768]{2,1,0:T(8,128)(2,1)} %broadcast_in_dim.33), calls=%async_computation | async-start | bytes 3145728 | tf_op jit(solution)/shard_map/all_to_all | solution.py:18
  61.1 2.4 %copy-start.7 = (f32[16,2,1024]{2,1,0:T(2,128)S(1)}, f32[16,2,1024]{2,1,0:T(2,128)}, u32[]{:S(2)}) copy-start(f32[16,2,1024]{2,1,0:T(2,128)} %param.29) | copy-start | bytes 393220
  61.4 1.7 copy-start.1
  81.1 8.2 %all-to-all-start.3 = ((f32[4,1,16]{2,1,0:T(1,128)}), f32[4,1,16]{2,1,0:T(1,128)S(1)}, u32[]{:S(2)}, u32[]{:S(2)}) async-start(f32[4,1,16]{2,1,0:T(1,128)} %broadcast_in_dim.36), calls=%async_computation.3 | async-start | bytes 4096 | tf_op jit(solution)/shard_map/all_to_all | solution.py:18
  86.8 24.6 %copy-start.2 = (bf16[2048,128]{1,0:T(8,128)(2,1)S(1)}, bf16[2048,128]{1,0:T(8,128)(2,1)}, u32[]{:S(2)}) copy-start(bf16[2048,128]{1,0:T(8,128)(2,1)} %param.37) | copy-start | bytes 1572868
  90.0 8.9 %all-to-all-start.2 = ((bf16[4,1,16,2048]{3,2,1,0:T(8,128)(2,1)}), bf16[4,1,16,2048]{3,2,1,0:T(8,128)(2,1)S(1)}, u32[]{:S(2)}, u32[]{:S(2)}) async-start(bf16[4,1,16,2048]{3,2,1,0:T(8,128)(2,1)} %broadcast_in_dim.35), calls=%async_computation.2 | async-start | bytes 524288 | tf_op jit(solution)/shard_map/all_to_all | solution.py:18
  93.4 44.9 %copy-start.13 = (bf16[1,2048,128]{2,1,0:T(8,128)(2,1)S(1)}, bf16[1,2048,128]{2,1,0:T(8,128)(2,1)}, u32[]{:S(2)}) copy-start(bf16[1,2048,128]{2,1,0:T(8,128)(2,1)} %param.34) | copy-start | bytes 1572868
  99.6 39.7 %copy-start.4 = (bf16[1,2048,128]{2,1,0:T(8,128)(2,1)S(1)}, bf16[1,2048,128]{2,1,0:T(8,128)(2,1)}, u32[]{:S(2)}) copy-start(bf16[1,2048,128]{2,1,0:T(8,128)(2,1)} %param.35) | copy-start | bytes 1572868
  101.3 37.1 %all-to-all-start.4 = ((bf16[64,3,2048]{2,1,0:T(4,128)(2,1)}), bf16[64,3,2048]{2,1,0:T(4,128)(2,1)S(1)}, u32[]{:S(2)}, u32[]{:S(2)}) async-start(bf16[64,3,2048]{2,1,0:T(4,128)(2,1)} %copy.82), calls=%async_computation.4 | async-start | bytes 2097152 | tf_op jit(solution)/shard_map/all_to_all | solution.py:152
  142.0 6.3 %copy-start.3 = (bf16[128,2048]{1,0:T(8,128)(2,1)S(1)}, bf16[128,2048]{1,0:T(8,128)(2,1)}, u32[]{:S(2)}) copy-start(bf16[128,2048]{1,0:T(8,128)(2,1)} %param.39) | copy-start | bytes 1572868
  144.5 19.3 %copy-start.14 = (bf16[2048,64]{0,1:T(8,128)(2,1)S(1)}, bf16[2048,64]{0,1:T(8,128)(2,1)}, u32[]{:S(2)}) copy-start(bf16[2048,64]{0,1:T(8,128)(2,1)} %param.32) | copy-start | bytes 786436
  144.5 19.9 %all-to-all-start.5 = ((bf16[4,2,49152]{2,1,0:T(2,128)(2,1)}), bf16[4,2,49152]{2,1,0:T(2,128)(2,1)S(1)}, u32[]{:S(2)}, u32[]{:S(2)}) async-start(bf16[4,2,49152]{2,1,0:T(2,128)(2,1)} %reshape.193), calls=%async_computation.5 | async-start | bytes 1572864 | tf_op jit(solution)/shard_map/all_to_all | solution.py:172
  164.4 9.1 %all-to-all-start.7 = ((bf16[4,2,4096]{2,1,0:T(2,128)(2,1)}), bf16[4,2,4096]{2,1,0:T(2,128)(2,1)S(1)}, u32[]{:S(2)}, u32[]{:S(2)}) async-start(bf16[4,2,4096]{2,1,0:T(2,128)(2,1)} %reshape.191), calls=%async_computation.7 | async-start | bytes 131072 | tf_op jit(solution)/shard_map/all_to_all | solution.py:173
  169.1 11.7 %copy-start.8 = (f32[16,6,3]{0,2,1:T(4,128)S(1)}, f32[16,6,3]{0,2,1:T(4,128)}, u32[]{:S(2)}) copy-start(f32[16,6,3]{0,2,1:T(4,128)} %copy.80) | copy-start | bytes 3460
  170.4 10.5 %copy-start.6 = (f32[16,6,64]{2,0,1:T(8,128)S(1)}, f32[16,6,64]{2,0,1:T(8,128)}, u32[]{:S(2)}) copy-start(f32[16,6,64]{2,0,1:T(8,128)} %copy.78) | copy-start | bytes 73732
  173.5 20.5 %all-to-all-start.6 = ((bf16[64,3,512]{2,1,0:T(4,128)(2,1)}), bf16[64,3,512]{2,1,0:T(4,128)(2,1)S(1)}, u32[]{:S(2)}, u32[]{:S(2)}) async-start(bf16[64,3,512]{2,1,0:T(4,128)(2,1)} %copy.86), calls=%async_computation.6 | async-start | bytes 524288 | tf_op jit(solution)/shard_map/all_to_all | solution.py:178
where the time goes:
time: 196 us; the launch traced here: 195 us
  waiting for transfers between devices  81.9 us (42%)
  starting transfers between devices  43.5 us (22%)
  other arithmetic  26.6 us (14%)
  local copies, waits for them, and re-layouts  19.1 us (10%)
  matrix products  14.4 us (7%)
  blocking collectives  8.08 us (4%)
    all_to_all x3, waiting for transfers between devices, copy_for_each(): lax.all_to_all(jnp.broadcast_to(array[None], (devices, *array.shape)), ax...  44.6 us
    all_to_all x1, waiting for transfers between devices, body(): lax.all_to_all(outbound, EP, split_axis=0, concat_axis=0, tiled=True)  26.6 us
    all_to_all x3, starting transfers between devices, copy_for_each(): lax.all_to_all(jnp.broadcast_to(array[None], (devices, *array.shape)), ax...  19.4 us
    unnamed x1, other arithmetic  11.5 us
    all_to_all x1, waiting for transfers between devices, body(): lax.all_to_all(expert_total.astype(jnp.bfloat16), EP, split_axis=0, conca...  10.7 us
    another operation x3, other arithmetic  9.15 us
    all_to_all x1, starting transfers between devices, body(): lax.all_to_all(outbound, EP, split_axis=0, concat_axis=0, tiled=True)  8.88 us
    unnamed x38, local copies, waits for them, and re-layouts  8.22 us
  transfers between devices with their start and end apart: 7, of which 5 were waited for; matrix products, arithmetic and copies ran while one was open for 14% of the time, Pallas kernels for 0%

commit v1 on v0

v1 whole, which is shorter than its diff:
```python
import jax
import jax.numpy as jnp
from jax import lax
from jax.experimental import pallas as pl
from jax.experimental.pallas import tpu as pltpu
from jax.sharding import Mesh
from jax.sharding import PartitionSpec as P

MESH = pl.DeviceIdType.MESH
EP = ("ep_0", "ep_1", "ep_2")
NZ, NX, NC, NT = 8, 4, 2, 4
NE = NZ * NX * NC
SEQ = 16
POS = 1024
HD = 128
EPS = 1e-06
SCALE = 2.5
F32 = jnp.float32
BF16 = jnp.bfloat16


def dot(a, b):
    return jnp.dot(a, b, preferred_element_type=F32)


def dot_nt(a, b):
    return lax.dot_general(a, b, (((1,), (1,)), ((), ())), preferred_element_type=F32)


def iota(shape, dim):
    return lax.broadcasted_iota(jnp.int32, shape, dim)


def ones_where(cond):
    return jnp.where(cond, 1.0, 0.0).astype(BF16)


def root_norm(data, gain):
    factor = lax.rsqrt(jnp.mean(data * data, axis=-1, keepdims=True) + EPS)
    return (data * factor * gain).astype(BF16)


def kernel(
    tok_h, ag_h, wq_h, wk_h, wv_h, wo_h, hg_h, pk_h, pv_h, off_h, lens, fg_h, rt_h, er_h,
    eg_h, eu_h, ed_h, sg_h, su_h, sd_h,
    mixed_o, fk_o, fv_o,
    tok, ag, hg, fg, rt, er, off, kb, vb, wb, ob, wgu, wd, sgu, sd,
    qs, lg, lenb, ho, pc, sq, nf, res, sbuf, rbuf, xb, gs, gr, hs, obuf, cbuf, ssb, ssr,
    lsem, kvsem,
    wxs, wxr, wzs, wzr, wds, wdr,
    oxs, oxr, ozs, ozr, ods, odr,
    ys, yr, cs, cr, as_, ar, gss, gsr, hss, hsr, rs_, rr, sss, ssrr,
):
    z = lax.axis_index("ep_0")
    x = lax.axis_index("ep_1")
    c = lax.axis_index("ep_2")
    t = lax.axis_index("tp")
    e = (z * NX + x) * NC + c

    def ep_dev(i):
        return (i // (NX * NC), lax.rem(i // NC, NX), lax.rem(i, NC), t)

    def tp_dev(i):
        return (z, x, c, i)

    def remote(src, dst, ssem, rsem, dev):
        return pltpu.make_async_remote_copy(
            src_ref=src, dst_ref=dst, send_sem=ssem, recv_sem=rsem,
            device_id=dev, device_id_type=MESH,
        )

    loads = []

    def load(src, dst):
        cp = pltpu.make_async_copy(src, dst, lsem.at[len(loads)])
        cp.start()
        loads.append(cp)
        return cp

    ld_w = [
        load(wq_h, wb.at[z, x, c, :, pl.ds(0, 256)]),
        load(wk_h, wb.at[z, x, c, :, pl.ds(256, 128)]),
        load(wv_h, wb.at[z, x, c, :, pl.ds(384, 128)]),
    ]
    ld_o = load(wo_h, ob.at[z, x, c])
    ld_tok = [load(tok_h, tok), load(ag_h, ag)]
    ld_er = load(er_h, er)
    ld_att = [load(off_h, off), load(hg_h, hg)]
    kv_loads = []
    for i in range(4):
        ds = pl.ds(4 * i, 4)
        kv_loads.append(pltpu.make_async_copy(pk_h.at[ds], kb.at[ds], kvsem.at[i]))
        kv_loads.append(pltpu.make_async_copy(pv_h.at[ds], vb.at[ds], kvsem.at[4 + i]))
    for cp in kv_loads:
        cp.start()
    ld_ffn = [load(fg_h, fg), load(rt_h, rt)]
    ld_sh = [
        load(sg_h, sgu.at[:, pl.ds(0, 128)]),
        load(su_h, sgu.at[:, pl.ds(128, 128)]),
        load(sd_h, sd),
    ]
    mine = pl.ds(pl.multiple_of(t * 512, 512), 512)
    ld_ex = [
        load(eg_h.at[0, mine, :], wgu.at[t, :, pl.ds(0, 128)]),
        load(eu_h.at[0, mine, :], wgu.at[t, :, pl.ds(128, 128)]),
        load(ed_h.at[0, :, mine], wd.at[t]),
    ]

    barrier = pltpu.get_barrier_semaphore()

    @pl.loop(1, NE)
    def _(d):
        pl.semaphore_signal(
            barrier, inc=1, device_id=ep_dev(lax.rem(e + d, NE)), device_id_type=MESH
        )

    for d in range(1, NT):
        pl.semaphore_signal(
            barrier, inc=1, device_id=tp_dev(lax.rem(t + d, NT)), device_id_type=MESH
        )
    pl.semaphore_wait(barrier, NE - 1 + NT - 1)

    pending = []

    def gather(buf, xs, xr, zs, zr, dsm, drm):
        def at(r, i):
            return buf.at[lax.rem(z + r + NZ, NZ), lax.rem(x + i, NX), c]

        up = (lax.rem(z + 1, NZ), x, c, t)
        down = (lax.rem(z + NZ - 1, NZ), x, c, t)
        partner = (z, x, 1 - c, t)

        def send(src, ssem, rsem, dev):
            cp = remote(src, src, ssem, rsem, dev)
            cp.start()
            pending.append(cp)

        def arrived(dst, ssem, rsem, dev):
            remote(dst, dst, ssem, rsem, dev).wait_recv()

        def first():
            for i in (1, 3, 2):
                send(at(0, 0), xs.at[i], xr.at[i], (z, lax.rem(x + i, NX), c, t))
            send(at(0, 0), zs.at[0, 0, 0], zr.at[0, 0, 0], up)
            send(at(0, 0), zs.at[1, 0, 0], zr.at[1, 0, 0], down)
            send(at(0, 0), dsm.at[0, 0], drm.at[0, 0], partner)

        def second():
            for i in (1, 3, 2):
                arrived(at(0, i), xs.at[NX - i], xr.at[NX - i], partner)
                send(at(0, i), zs.at[0, 0, i], zr.at[0, 0, i], up)
                send(at(0, i), zs.at[1, 0, i], zr.at[1, 0, i], down)
                send(at(0, i), dsm.at[0, i], drm.at[0, i], partner)

        def ring(s):
            for i in (0, 1, 3, 2):
                arrived(at(-s, i), zs.at[0, s - 1, i], zr.at[0, s - 1, i], partner)
                if s < 4:
                    send(at(-s, i), zs.at[0, s, i], zr.at[0, s, i], up)
                send(at(-s, i), dsm.at[NZ - s, i], drm.at[NZ - s, i], partner)
                if s < 4:
                    arrived(at(s, i), zs.at[1, s - 1, i], zr.at[1, s - 1, i], partner)
                    if s < 3:
                        send(at(s, i), zs.at[1, s, i], zr.at[1, s, i], down)
                    send(at(s, i), dsm.at[s, i], drm.at[s, i], partner)

        def last():
            for r in range(NZ):
                for i in range(NX):
                    dst = buf.at[lax.rem(z + r, NZ), lax.rem(x + i, NX), 1 - c]
                    arrived(dst, dsm.at[r, i], drm.at[r, i], partner)

        return first, second, ring, last

    w_first, w_second, w_ring, w_last = gather(wb, wxs, wxr, wzs, wzr, wds, wdr)
    o_first, o_second, o_ring, o_last = gather(ob, oxs, oxr, ozs, ozr, ods, odr)
    for cp in ld_w:
        cp.wait()
    w_first()
    ld_o.wait()

    def y_send(src, dst, ssem, rsem, dev):
        cp = remote(src, dst, ssem, rsem, dev)
        cp.start()
        pending.append(cp)

    for d in (1, 3, 2):
        p = lax.rem(t + d, NT)
        theirs = pl.ds(pl.multiple_of(p * 512, 512), 512)
        y_send(eg_h.at[0, theirs, :], wgu.at[t, :, pl.ds(0, 128)], ys.at[0, d], yr.at[0, d], tp_dev(p))
        y_send(eu_h.at[0, theirs, :], wgu.at[t, :, pl.ds(128, 128)], ys.at[1, d], yr.at[1, d], tp_dev(p))
        y_send(ed_h.at[0, :, theirs], wd.at[t], ys.at[2, d], yr.at[2, d], tp_dev(p))

    w_second()
    o_first()

    for cp in ld_tok:
        cp.wait()
    normed = root_norm(tok[...].astype(F32), ag[...])
    w_ring(1)
    o_second()
    w_ring(2)
    w_ring(3)
    w_ring(4)

    ld_er.wait()
    rows = NE * SEQ
    chosen = iota((NE, SEQ), 0) == er[0:1, :]
    for k in range(1, 6):
        chosen = chosen | (iota((NE, SEQ), 0) == er[k : k + 1, :])
    hot_t = ones_where(chosen)
    before = ones_where(iota((SEQ, SEQ), 0) < iota((SEQ, SEQ), 1))
    code_t = jnp.where(chosen, dot(hot_t, before) + 1.0, 0.0).astype(BF16)
    repeat = ones_where((iota((SEQ, 64), 1) & 15) == iota((SEQ, 64), 0))
    eye = ones_where(iota((SEQ, SEQ), 0) == iota((SEQ, SEQ), 1))
    code4_t = dot(code_t, repeat).astype(BF16)
    code = dot_nt(eye, code_t)
    r0 = iota((rows, 64), 0)
    c0 = iota((rows, 64), 1)
    spread = ones_where((r0 >> 4) == c0)
    slot_of = dot(spread, code4_t)
    want = ((r0 & 3) + 1).astype(F32)
    dispatch = ones_where((slot_of == want) & (((r0 >> 2) & 3) == (c0 >> 4)))

    w_last()
    total = jnp.zeros((SEQ, 512), F32)
    for zi in range(NZ):
        total = total + dot(normed[:, 256 * zi : 256 * zi + 256], wb[zi].reshape(256, 512))
    queries = total[:, 0:256].astype(BF16).astype(F32)
    fk_o[...] = total[:, 256:384].astype(BF16)
    fv_o[...] = total[:, 384:512].astype(BF16)
    o_ring(1)

    for h in range(2):
        qs[pl.ds(h, SEQ, stride=2), :] = queries[:, HD * h : HD * h + HD]
    for cp in ld_att:
        cp.wait()
    for b in range(SEQ):
        if b % 4 == 0:
            kv_loads[2 * (b // 4)].wait()
        q = qs[2 * b : 2 * b + 2, :].astype(BF16)
        lg[2 * b : 2 * b + 2, :] = dot_nt(q, kb[b]) * HD ** (-0.5) + off[b]
        lenb[2 * b : 2 * b + 2, :] = jnp.full((2, HD), lens[b], jnp.int32)
    o_ring(2)
    logits = lg[...]
    length = lenb[:, 0:1]
    usable = iota((2 * SEQ, POS), 1) < length
    tail = jnp.log(1.0 + jnp.exp(-jnp.abs(logits)))
    keep = jnp.where(usable, jnp.minimum(-logits, 0.0) - tail, 0.0)
    nb = POS // HD
    stacked = jnp.concatenate([keep[:, HD * i : HD * i + HD] for i in range(nb)], axis=0)
    k1 = stacked.astype(BF16)
    left = stacked - k1.astype(F32)
    k2 = left.astype(BF16)
    k3 = (left - k2.astype(F32)).astype(BF16)
    later = ones_where(iota((HD, HD), 0) > iota((HD, HD), 1))
    inner = dot(k1, later) + dot(k2, later) + dot(k3, later)
    carry = jnp.zeros((2 * SEQ, 1), F32)
    after = [None] * nb
    n2 = 2 * SEQ
    for i in range(nb - 1, -1, -1):
        after[i] = inner[n2 * i : n2 * i + n2] + carry
        carry = carry + jnp.sum(stacked[n2 * i : n2 * i + n2], axis=-1, keepdims=True)
    after = jnp.concatenate(after, axis=1)
    sticks = jnp.where(usable, jnp.exp(jnp.minimum(logits, 0.0) - tail + after), 0.0)
    lg[...] = sticks
    o_ring(3)
    for b in range(SEQ):
        if b % 4 == 0:
            kv_loads[2 * (b // 4) + 1].wait()
        got = dot(lg[2 * b : 2 * b + 2, :].astype(BF16), vb[b])
        ho[b : b + 1, 0:HD] = got[0:1, :]
        ho[b : b + 1, HD : 2 * HD] = got[1:2, :]
    o_ring(4)
    heads_out = ho[...]
    scaled = (heads_out * hg[...]).astype(BF16)
    sq[t] = jnp.broadcast_to(jnp.sum(heads_out * heads_out, axis=-1, keepdims=True), (SEQ, HD))
    o_last()
    for zi in range(NZ):
        part = dot_nt(scaled, ob[zi].reshape(256, 256))
        pc[t, :, 256 * zi : 256 * zi + 256] = part.astype(BF16)

    c_moves = []
    for d in (2, 1, 3):
        p = lax.rem(t + d, NT)
        for k, buf in enumerate((sq, pc)):
            cp = remote(buf.at[t], buf.at[t], cs.at[k, d], cr.at[k, d], tp_dev(p))
            cp.start()
            pending.append(cp)
            c_moves.append((k, d, buf))
    for k, d, buf in c_moves:
        src = lax.rem(t + NT - d, NT)
        remote(buf.at[src], buf.at[src], cs.at[k, d], cr.at[k, d], tp_dev(src)).wait_recv()
    head_total = pc[0].astype(F32)
    square = sq[0]
    for i in range(1, NT):
        head_total = head_total + pc[i].astype(F32)
        square = square + sq[i]
    attention = head_total * lax.rsqrt(square[:, 0:1] / 1024.0 + EPS)
    residual = (tok[...].astype(F32) + attention).astype(BF16)
    for i in range(NT):
        res[i] = residual[:, 512 * i : 512 * i + 512]
    for cp in ld_ffn:
        cp.wait()
    normed_ffn = root_norm(residual.astype(F32), fg[...])
    for i in range(16):
        nf[i] = normed_ffn[:, HD * i : HD * i + HD]

    block = nf[pl.ds(4 * t, 4)].reshape(64, HD)
    sbuf[...] = dot(dispatch, block).astype(BF16).reshape(NE, SEQ, HD)

    @pl.loop(1, NE)
    def _(d):
        p = lax.rem(e + d, NE)
        remote(sbuf.at[p], rbuf.at[e], as_, ar, ep_dev(p)).start()

    rbuf[e] = sbuf[e]

    for cp in ld_sh:
        cp.wait()
    both = dot(normed_ffn, sgu[...])
    gate = both[:, 0:HD]
    shared_hidden = (gate / (1.0 + jnp.exp(-gate)) * both[:, HD : 2 * HD]).astype(BF16)
    shared_part = dot(shared_hidden, sd[...]).astype(BF16)
    for i in range(NT):
        ssb[i] = shared_part[:, 512 * i : 512 * i + 512]
    for d in (2, 1, 3):
        p = lax.rem(t + d, NT)
        y_send(ssb.at[p], ssr.at[t], sss.at[d], ssrr.at[d], tp_dev(p))
    ssr[t] = ssb[t]
    logit = dot_nt(normed_ffn, rt[...])
    prob = 1.0 / (1.0 + jnp.exp(-logit))
    picked = jnp.where(code > 0.5, prob, 0.0)
    weight = SCALE * picked / jnp.sum(picked, axis=-1, keepdims=True)
    weight4 = jnp.concatenate([weight] * 4, axis=0)
    w_hi = weight4.astype(BF16)
    w_lo = (weight4 - w_hi.astype(F32)).astype(BF16)
    code4 = jnp.concatenate([code] * 4, axis=0).astype(BF16)
    r1 = iota((64, rows), 1)
    c1 = iota((64, rows), 0)
    spread_t = ones_where((r1 >> 4) == c1)
    slot_to = dot(code4, spread_t)
    fits = (slot_to == ((r1 & 3) + 1).astype(F32)) & (((r1 >> 2) & 3) == (c1 >> 4))
    comb_hi = jnp.where(fits, dot(w_hi, spread_t), 0.0).astype(BF16)
    comb_lo = jnp.where(fits, dot(w_lo, spread_t), 0.0).astype(BF16)

    def everyone(buf):
        return buf.at[pl.ds(0, NE - 1)]

    def wait_all(src, dst, ssem, rsem):
        cp = remote(everyone(src), everyone(dst), ssem, rsem, tp_dev(lax.rem(t + 1, NT)))
        cp.wait_recv()
        cp.wait_send()

    wait_all(sbuf, rbuf, as_, ar)

    p48 = iota((48, 256), 0)
    q48 = iota((48, 256), 1)
    for g in range(4):
        group = rbuf[16 * g : 16 * g + 16].reshape(256, HD)
        for j in range(4):
            pick = ones_where(q48 == ((p48 & 15) << 4) + 4 * j + (p48 >> 4))
            xb[48 * g : 48 * g + 48, HD * j : HD * j + HD] = dot(pick, group).astype(BF16)
    for cp in ld_ex:
        cp.wait()
    for d in (1, 3, 2):
        src = lax.rem(t + NT - d, NT)
        remote(wgu.at[src, :, pl.ds(0, 128)], wgu.at[src, :, pl.ds(0, 128)], ys.at[0, d], yr.at[0, d], tp_dev(src)).wait_recv()
        remote(wgu.at[src, :, pl.ds(128, 128)], wgu.at[src, :, pl.ds(128, 128)], ys.at[1, d], yr.at[1, d], tp_dev(src)).wait_recv()
        remote(wd.at[src], wd.at[src], ys.at[2, d], yr.at[2, d], tp_dev(src)).wait_recv()
    xv = xb[...]
    for d in (2, 1, 3):
        p = lax.rem(t + d, NT)
        gs[d] = dot(xv, wgu[p]).astype(BF16)
        y_send(gs.at[d], gr.at[d], gss.at[d], gsr.at[d], tp_dev(p))
    gate_up = dot(xv, wgu[t])
    for d in (2, 1, 3):
        src = lax.rem(t + NT - d, NT)
        remote(gr.at[d], gr.at[d], gss.at[d], gsr.at[d], tp_dev(src)).wait_recv()
        gate_up = gate_up + gr[d].astype(F32)
    gate = gate_up[:, 0:HD]
    hidden = (gate / (1.0 + jnp.exp(-gate)) * gate_up[:, HD : 2 * HD]).astype(BF16)
    hs[t] = hidden
    for d in (2, 1, 3):
        p = lax.rem(t + d, NT)
        y_send(hs.at[t], hs.at[t], hss.at[d], hsr.at[d], tp_dev(p))
    for d in (2, 1, 3):
        src = lax.rem(t + NT - d, NT)
        remote(hs.at[src], hs.at[src], hss.at[d], hsr.at[d], tp_dev(src)).wait_recv()
    out = dot(hs[0], wd[0])
    for i in range(1, NT):
        out = out + dot(hs[i], wd[i])
    out = out.astype(BF16)

    pt = iota((256, 48), 1)
    qt = iota((256, 48), 0)
    for g in range(4):
        back = jnp.zeros((256, HD), F32)
        for j in range(4):
            pick = ones_where(qt == ((pt & 15) << 4) + 4 * j + (pt >> 4))
            back = back + dot(pick, out[48 * g : 48 * g + 48, HD * j : HD * j + HD])
        obuf[16 * g : 16 * g + 16] = back.astype(BF16).reshape(16, 16, HD)

    @pl.loop(1, NE)
    def _(d):
        p = lax.rem(e + d, NE)
        remote(obuf.at[p], cbuf.at[e], rs_, rr, ep_dev(p)).start()

    cbuf[e] = obuf[e]
    shared_total = jnp.zeros((SEQ, 512), F32)
    for d in (2, 1, 3):
        src = lax.rem(t + NT - d, NT)
        remote(ssr.at[src], ssr.at[src], sss.at[d], ssrr.at[d], tp_dev(src)).wait_recv()
    for i in range(NT):
        shared_total = shared_total + ssr[i].astype(F32)
    base = res[t].astype(F32) + shared_total
    wait_all(obuf, cbuf, rs_, rr)
    came = cbuf[...].reshape(rows, HD)
    routed = dot(comb_hi, came) + dot(comb_lo, came)
    for j in range(4):
        mixed_o[:, HD * j : HD * j + HD] = (
            base[:, HD * j : HD * j + HD] + routed[SEQ * j : SEQ * j + SEQ]
        ).astype(BF16)
    for cp in pending:
        cp.wait_send()


def body(
    tokens, attn_gain, query_weight, key_weight, value_weight, out_weight, head_gain,
    past_keys, past_values, break_offset, cache_lengths, ffn_gain, router_weight,
    expert_routes, expert_gate, expert_up, expert_down, shared_gate, shared_up, shared_down,
):
    hbm = pl.BlockSpec(memory_space=pl.ANY)
    vmem = pl.BlockSpec(memory_space=pltpu.VMEM)
    smem = pl.BlockSpec(memory_space=pltpu.SMEM)
    v, dma = pltpu.VMEM, pltpu.SemaphoreType.DMA
    ring = [dma((4,)), dma((4,)), dma((2, 4, 4)), dma((2, 4, 4)), dma((8, 4)), dma((8, 4))]
    return pl.pallas_call(
        kernel,
        out_shape=(
            jax.ShapeDtypeStruct((SEQ, 512), BF16),
            jax.ShapeDtypeStruct((SEQ, HD), BF16),
            jax.ShapeDtypeStruct((SEQ, HD), BF16),
        ),
        in_specs=[smem if i == 10 else hbm for i in range(20)],
        out_specs=(vmem, vmem, vmem),
        scratch_shapes=[
            v((SEQ, 2048), BF16), v((1, 2048), F32), v((1, 256), F32), v((1, 2048), F32),
            v((64, 2048), BF16), v((6, SEQ), jnp.int32), v((SEQ, 2, POS), F32),
            v((SEQ, POS, HD), BF16), v((SEQ, POS, HD), BF16),
            v((NZ, NX, NC, 32, 512), BF16), v((NZ, NX, NC, 32, 256), BF16),
            v((NT, 512, 256), BF16), v((NT, 128, 512), BF16),
            v((2048, 256), BF16), v((128, 2048), BF16),
            v((2 * SEQ, HD), F32), v((2 * SEQ, POS), F32), v((2 * SEQ, HD), jnp.int32),
            v((SEQ, 256), F32), v((NT, SEQ, 2048), BF16), v((NT, SEQ, HD), F32),
            v((16, SEQ, HD), BF16), v((NT, SEQ, 512), BF16),
            v((NE, SEQ, HD), BF16), v((NE, SEQ, HD), BF16), v((192, 512), BF16),
            v((NT, 192, 256), BF16), v((NT, 192, 256), BF16), v((NT, 192, HD), BF16),
            v((NE, SEQ, HD), BF16), v((NE, SEQ, HD), BF16),
            v((NT, SEQ, 512), BF16), v((NT, SEQ, 512), BF16),
            dma((24,)), dma((8,)),
            *ring, *ring,
            dma((3, 4)), dma((3, 4)), dma((2, 4)), dma((2, 4)), dma, dma,
            dma((4,)), dma((4,)), dma((4,)), dma((4,)), dma, dma, dma((4,)), dma((4,)),
        ],
        compiler_params=pltpu.CompilerParams(
            collective_id=0, has_side_effects=True, vmem_limit_bytes=60 * 1024 * 1024
        ),
    )(
        tokens, attn_gain.astype(F32)[None], query_weight, key_weight, value_weight, out_weight,
        head_gain.astype(F32)[None], past_keys.reshape(SEQ, POS, HD),
        past_values.reshape(SEQ, POS, HD), break_offset, cache_lengths,
        ffn_gain.astype(F32)[None], router_weight.T, expert_routes.T, expert_gate, expert_up,
        expert_down, shared_gate, shared_up, shared_down,
    )


def solution(mesh):
    torus = Mesh(mesh.devices.reshape(NZ, NX, NC, NT), (*EP, "tp"))
    return jax.shard_map(
        body,
        mesh=torus,
        in_specs=(
            P(EP, None),
            P(),
            P(EP, "tp"),
            P(EP, "tp"),
            P(EP, "tp"),
            P(EP, "tp"),
            P("tp"),
            P(EP, None, "tp", None),
            P(EP, None, "tp", None),
            P(EP, "tp", None),
            P(EP),
            P(),
            P(),
            P(EP, None),
            P(EP, None, "tp"),
            P(EP, None, "tp"),
            P(EP, "tp", None),
            P(None, "tp"),
            P(None, "tp"),
            P("tp", None),
        ),
        out_specs=(P(EP, "tp"), P(EP, "tp"), P(EP, "tp")),
        check_vma=False,
    )
```

time: 196 us -> 94.1 us (0.48)
  Pallas kernels: 0 us -> 85.5 us
  waiting for transfers between devices: 81.9 us -> 0 us
  starting transfers between devices: 43.5 us -> 0 us
  other arithmetic: 26.6 us -> 3.78 us
  local copies, waits for them, and re-layouts: 19.1 us -> 3.86 us
  matrix products: 14.4 us -> 0 us
  blocking collectives: 8.08 us -> 0 us
    pallas_call x0 -> x1, Pallas kernels: none -> 85.5 us  [body(): pl.pallas_call(kernel, out_shape=(jax.ShapeDtypeStruct((SEQ, 512), BF16),...]
    all_to_all x7 -> x0, waiting for transfers between devices: 81.9 us -> none  [the longest x3 44.6 us: copy_for_each(): lax.all_to_all(jnp.broadcast_to(array[None], (devices, *array.shape)), ax...]
    all_to_all x7 -> x0, starting transfers between devices: 43.5 us -> none  [the longest x3 19.4 us: copy_for_each(): lax.all_to_all(jnp.broadcast_to(array[None], (devices, *array.shape)), ax...]
    dot_general x12 -> x0, matrix products: 14.4 us -> none  [the longest x1 3.45 us: stick_attend(): jnp.einsum('bgrl,blgd->bgrd', sticks, value_cache, preferred_element_type...]
    unnamed x1 -> x0, other arithmetic: 11.5 us -> none
    another operation x4 -> x0, other arithmetic: 9.28 us -> none
    all_to_all x1 -> x0, blocking collectives: 8.08 us -> none  [copy_for_each(): lax.all_to_all(jnp.broadcast_to(array[None], (devices, *array.shape)), ax...]
    unnamed x38 -> x3, local copies, waits for them, and re-layouts: 8.22 us -> 3.86 us
  transfers between devices with their start and end apart: 7 -> 0, of which waited for: 5 -> 0; matrix products, arithmetic and copies ran while one was open for 14% -> 0% of each run, Pallas kernels for 0% -> 0%
where the time goes in v1:
time: 94.1 us; the launch traced here: 93.8 us
  Pallas kernels  85.5 us (91%)
  local copies, waits for them, and re-layouts  3.86 us (4%)
  other arithmetic  3.78 us (4%)
    pallas_call x1, Pallas kernels, body(): pl.pallas_call(kernel, out_shape=(jax.ShapeDtypeStruct((SEQ, 512), BF16),...  85.5 us
    unnamed x3, local copies, waits for them, and re-layouts  3.86 us

profile of v1, /device:TPU:1, one launch (start us, length us, event | category | flops | bytes accessed | tf_op | source)
XLA Modules:
  0.0 93.8 jit_solution(17181581849040907038)
XLA Ops:
  0.6 1.2 %broadcast_in_dim.22 = f32[256]{0:T(256)} convert(bf16[256]{0:T(256)(128)(2,1)} %param.26) | non-fusion elementwise | flops 256 | bytes 1536 | tf_op jit(solution)/shard_map/broadcast_in_dim | solution.py:471
  1.8 1.3 %broadcast_in_dim.21 = f32[2048]{0:T(1024)} convert(bf16[2048]{0:T(1024)(128)(2,1)} %param.21) | non-fusion elementwise | flops 2048 | bytes 12288 | tf_op jit(solution)/shard_map/broadcast_in_dim | solution.py:470
  3.1 1.3 %broadcast_in_dim.23 = f32[2048]{0:T(1024)} convert(bf16[2048]{0:T(1024)(128)(2,1)} %param.31) | non-fusion elementwise | flops 2048 | bytes 12288 | tf_op jit(solution)/shard_map/broadcast_in_dim | solution.py:473
  4.4 85.5 %shard_map.211 = (bf16[16,512]{1,0:T(8,128)(2,1)}, bf16[16,128]{1,0:T(8,128)(2,1)}, bf16[16,128]{1,0:T(8,128)(2,1)}) custom-call(bf16[16,2048]{1,0:T(8,128)(2,1)} %tok_h.1, f32[1,2048]{1,0:T(1,128)} %bitcast.10, bf16[32,256]{1,0:T(8,128)(2,1)} %wq_h.1, bf16[32,128]{1,0:T(8,128)(2,1)} %wk_h.1, bf16[32,128]{1,0:T(8,128)(2,1)} %wv_h.1, bf16[32,256]{1,0:T(8,128)(2,1)} %wo_h.1, ...), custom_call_target="tpu_custom_call" | custom-call | tf_op jit(solution)/shard_map/pallas_call | solution.py:438
  89.9 1.3 %copy.26 = bf16[16,512]{1,0:T(8,128)(2,1)} copy(bf16[16,512]{1,0:T(8,128)(2,1)} %get-tuple-element.6) | data formatting | bytes 32768
  91.2 1.3 %copy.27 = bf16[16,128]{1,0:T(8,128)(2,1)} copy(bf16[16,128]{1,0:T(8,128)(2,1)} %get-tuple-element.7) | data formatting | bytes 8192
  92.5 1.3 %copy.28 = bf16[16,128]{1,0:T(8,128)(2,1)} copy(bf16[16,128]{1,0:T(8,128)(2,1)} %get-tuple-element.8) | data formatting | bytes 8192

commit v2 on v1

v2 whole, which is shorter than its diff:
```python
import jax
import jax.numpy as jnp
from jax import lax
from jax.experimental import pallas as pl
from jax.experimental.pallas import tpu as pltpu
from jax.sharding import Mesh
from jax.sharding import PartitionSpec as P

MESH = pl.DeviceIdType.MESH
EP = ("ep_0", "ep_1", "ep_2")
NZ, NX, NC, NT = 8, 4, 2, 4
NE = NZ * NX * NC
SEQ = 16
POS = 1024
HD = 128
EPS = 1e-06
SCALE = 2.5
F32 = jnp.float32
BF16 = jnp.bfloat16


def dot(a, b):
    return jnp.dot(a, b, preferred_element_type=F32)


def dot_nt(a, b):
    return lax.dot_general(a, b, (((1,), (1,)), ((), ())), preferred_element_type=F32)


def iota(shape, dim):
    return lax.broadcasted_iota(jnp.int32, shape, dim)


def ones_where(cond):
    return jnp.where(cond, 1.0, 0.0).astype(BF16)


def kernel(
    tok_h, ag_h, wq_h, wk_h, wv_h, wo_h, hg_h, pk_h, pv_h, off_h, lens, fg_h, rt_h, er_h,
    eg_h, eu_h, ed_h, sg_h, su_h, sd_h,
    mixed_o, fk_o, fv_o,
    tok, ag, hg, fg, rt, er, off, kb, vb, qb, kvb, ob, wgu, wd, sgu, sd,
    tkb, tk, part, qp, kvpart, kvp,
    qs, lg, lenb, ho, pc, sq, nf, res, sbuf, rbuf, xb, gs, gr, hs, obuf, cbuf, ssb, ssr,
    lsem, kvsem,
    qzs, qzr, kzs, kzr, ozs, ozr, oxs, oxr, ods, odr, tks, tkr, qps, qpr, kps, kpr,
    ys, yr, cs, cr, as_, ar, gss, gsr, hss, hsr, rs_, rr, sss, ssrr,
):
    z = lax.axis_index("ep_0")
    x = lax.axis_index("ep_1")
    c = lax.axis_index("ep_2")
    t = lax.axis_index("tp")
    e = (z * NX + x) * NC + c
    m = x * NC + c
    zd = [lax.rem(z + d, NZ) for d in range(NZ)]
    xd = [lax.rem(x + d, NX) for d in range(NX)]
    td = [lax.rem(t + d, NT) for d in range(NT)]
    cd = [c, 1 - c]
    mates = [(2, 0), (2, 1), (1, 0), (3, 0), (1, 1), (3, 1), (0, 1)]
    far_first = [4, 3, 5, 2, 6, 1, 7]
    near_first = far_first[::-1]

    def remote(src, dst, ssem, rsem, dev):
        return pltpu.make_async_remote_copy(
            src_ref=src, dst_ref=dst, send_sem=ssem, recv_sem=rsem,
            device_id=dev, device_id_type=MESH,
        )

    pending = []

    def send(src, dst, ssem, rsem, dev):
        cp = remote(src, dst, ssem, rsem, dev)
        cp.start()
        pending.append(cp)

    def arrived(dst, ssem, rsem):
        remote(dst, dst, ssem, rsem, (z, x, 1 - c, t)).wait_recv()

    loads = []

    def load(src, dst):
        cp = pltpu.make_async_copy(src, dst, lsem.at[len(loads)])
        cp.start()
        loads.append(cp)
        return cp

    ld_q = load(wq_h, qb.at[z])
    ld_tok = [load(tok_h, tok), load(ag_h, ag)]
    ld_o = load(wo_h, ob.at[z, x, c])
    ld_kv = [
        load(wk_h, kvb.at[z, :, pl.ds(0, 128)]),
        load(wv_h, kvb.at[z, :, pl.ds(128, 128)]),
    ]
    ld_er = load(er_h, er)
    ld_att = [load(off_h, off), load(hg_h, hg)]
    kv_loads = []
    for i in range(4):
        ds = pl.ds(4 * i, 4)
        kv_loads.append(pltpu.make_async_copy(pk_h.at[ds], kb.at[ds], kvsem.at[i]))
        kv_loads.append(pltpu.make_async_copy(pv_h.at[ds], vb.at[ds], kvsem.at[4 + i]))
    for cp in kv_loads:
        cp.start()
    ld_ffn = [load(fg_h, fg), load(rt_h, rt)]
    ld_sh = [
        load(sg_h, sgu.at[:, pl.ds(0, 128)]),
        load(su_h, sgu.at[:, pl.ds(128, 128)]),
        load(sd_h, sd),
    ]
    mine = pl.ds(pl.multiple_of(t * 512, 512), 512)
    ld_ex = [
        load(eg_h.at[0, mine, :], wgu.at[t, :, pl.ds(0, 128)]),
        load(eu_h.at[0, mine, :], wgu.at[t, :, pl.ds(128, 128)]),
        load(ed_h.at[0, :, mine], wd.at[t]),
    ]

    barrier = pltpu.get_barrier_semaphore()
    first = [(zd[d], x, c, t) for d in range(1, NZ)]
    first += [(z, xd[dx], cd[dc], t) for dx, dc in mates]
    first += [(z, x, c, td[d]) for d in range(1, NT)]
    for dev in first:
        pl.semaphore_signal(barrier, inc=1, device_id=dev, device_id_type=MESH)
    pl.semaphore_wait(barrier, len(first))

    ld_q.wait()
    for d in far_first:
        send(qb.at[z], qb.at[z], qzs.at[d], qzr.at[d], (zd[d], x, c, t))

    for cp in ld_tok:
        cp.wait()
    data = tok[...].astype(F32)
    factor = lax.rsqrt(jnp.mean(data * data, axis=-1, keepdims=True) + EPS)
    gain = ag[...].astype(F32)
    blocks = []
    for i in range(NZ):
        halves = []
        for k in (2 * i, 2 * i + 1):
            halves.append(data[:, HD * k : HD * k + HD] * factor * gain[k : k + 1, :])
        blocks.append(jnp.concatenate(halves, axis=1).astype(BF16).astype(F32))
    chunk = iota((SEQ, 256), 1) >> 5
    for g in range(8):
        own = blocks[g]
        for k in range(1, 8):
            j = (g + k) % 8
            own = jnp.where(chunk == j, pltpu.roll(blocks[j], 32 * k, 1), own)
        part[g] = own
    for dx, dc in mates:
        g = xd[dx] * NC + cd[dc]
        tkb[g] = part[g].astype(BF16)
        send(tkb.at[g], tk.at[m], tks.at[dx, dc], tkr.at[dx, dc], (z, xd[dx], cd[dc], t))
    tk[m] = part[m].astype(BF16)

    ld_o.wait()
    mine_o = ob.at[z, x, c]
    for d in far_first:
        send(mine_o, mine_o, ozs.at[d], ozr.at[d], (zd[d], x, c, t))

    def o_along(r):
        src = ob.at[zd[r], x, c]
        for i in (2, 1, 3):
            send(src, src, oxs.at[r, i], oxr.at[r, i], (z, xd[i], c, t))

    def o_forward(r):
        src = ob.at[zd[r], x, c]
        arrived(src, ozs.at[NZ - r], ozr.at[NZ - r])
        o_along(r)

    def o_across(r):
        for i in (1, 3, 2):
            arrived(ob.at[zd[r], xd[i], c], oxs.at[r, NX - i], oxr.at[r, NX - i])
        src = ob.at[zd[r], :, c]
        send(src, src, ods.at[r], odr.at[r], (z, x, 1 - c, t))

    def o_last():
        for r in range(NZ):
            arrived(ob.at[zd[r], :, 1 - c], ods.at[r], odr.at[r])

    o_along(0)
    for cp in ld_kv:
        cp.wait()
    for d in far_first:
        send(kvb.at[z], kvb.at[z], kzs.at[d], kzr.at[d], (zd[d], x, c, t))

    for d in (1, 3, 2):
        p = td[d]
        dev = (z, x, c, p)
        theirs = pl.ds(pl.multiple_of(p * 512, 512), 512)
        for k, src in enumerate((eg_h, eu_h)):
            half = pl.ds(128 * k, 128)
            send(src.at[0, theirs, :], wgu.at[t, :, half], ys.at[k, d], yr.at[k, d], dev)
        send(ed_h.at[0, :, theirs], wd.at[t], ys.at[2, d], yr.at[2, d], dev)

    ld_er.wait()
    rows = NE * SEQ
    chosen = iota((NE, SEQ), 0) == er[0:1, :]
    for k in range(1, 6):
        chosen = chosen | (iota((NE, SEQ), 0) == er[k : k + 1, :])
    hot_t = ones_where(chosen)
    before = ones_where(iota((SEQ, SEQ), 0) < iota((SEQ, SEQ), 1))
    code_t = jnp.where(chosen, dot(hot_t, before) + 1.0, 0.0).astype(BF16)
    repeat = ones_where((iota((SEQ, 64), 1) & 15) == iota((SEQ, 64), 0))
    eye = ones_where(iota((SEQ, SEQ), 0) == iota((SEQ, SEQ), 1))
    code4_t = dot(code_t, repeat).astype(BF16)
    code = dot_nt(eye, code_t)
    r0 = iota((rows, 64), 0)
    c0 = iota((rows, 64), 1)
    spread = ones_where((r0 >> 4) == c0)
    slot_of = dot(spread, code4_t)
    want = ((r0 & 3) + 1).astype(F32)
    dispatch = ones_where((slot_of == want) & (((r0 >> 2) & 3) == (c0 >> 4)))

    for dx, dc in mates:
        src = tk.at[lax.rem(x + NX - dx, NX) * NC + cd[dc]]
        arrived(src, tks.at[dx, dc], tkr.at[dx, dc])
    for d in near_first:
        arrived(qb.at[lax.rem(z + NZ - d, NZ)], qzs.at[d], qzr.at[d])
    rows_in = tk[...].reshape(8 * SEQ, 256)
    part[...] = dot(rows_in, qb[...].reshape(256, 256)).reshape(8, SEQ, 256)
    for dx, dc in mates:
        g = xd[dx] * NC + cd[dc]
        send(part.at[g], qp.at[m], qps.at[dx, dc], qpr.at[dx, dc], (z, xd[dx], cd[dc], t))
    qp[m] = part[m]
    for r in (7, 1, 6, 2, 5, 3, 4):
        o_forward(r)
    for dx, dc in mates:
        src = qp.at[lax.rem(x + NX - dx, NX) * NC + cd[dc]]
        arrived(src, qps.at[dx, dc], qpr.at[dx, dc])
    total = qp[0]
    for i in range(1, 8):
        total = total + qp[i]
    queries = total.astype(BF16).astype(F32)

    for h in range(2):
        qs[pl.ds(h, SEQ, stride=2), :] = queries[:, HD * h : HD * h + HD]
    for cp in ld_att:
        cp.wait()
    for b in range(SEQ):
        if b % 4 == 0:
            kv_loads[2 * (b // 4)].wait()
        q = qs[2 * b : 2 * b + 2, :].astype(BF16)
        lg[2 * b : 2 * b + 2, :] = dot_nt(q, kb[b]) * HD ** (-0.5) + off[b]
        lenb[2 * b : 2 * b + 2, :] = jnp.full((2, HD), lens[b], jnp.int32)
    for r in (0, 7, 1):
        o_across(r)
    logits = lg[...]
    length = lenb[:, 0:1]
    usable = iota((2 * SEQ, POS), 1) < length
    tail = jnp.log(1.0 + jnp.exp(-jnp.abs(logits)))
    keep = jnp.where(usable, jnp.minimum(-logits, 0.0) - tail, 0.0)
    nb = POS // HD
    stacked = jnp.concatenate([keep[:, HD * i : HD * i + HD] for i in range(nb)], axis=0)
    k1 = stacked.astype(BF16)
    left = stacked - k1.astype(F32)
    k2 = left.astype(BF16)
    k3 = (left - k2.astype(F32)).astype(BF16)
    later = ones_where(iota((HD, HD), 0) > iota((HD, HD), 1))
    inner = dot(k1, later) + dot(k2, later) + dot(k3, later)
    carry = jnp.zeros((2 * SEQ, 1), F32)
    after = [None] * nb
    n2 = 2 * SEQ
    for i in range(nb - 1, -1, -1):
        after[i] = inner[n2 * i : n2 * i + n2] + carry
        carry = carry + jnp.sum(stacked[n2 * i : n2 * i + n2], axis=-1, keepdims=True)
    after = jnp.concatenate(after, axis=1)
    sticks = jnp.where(usable, jnp.exp(jnp.minimum(logits, 0.0) - tail + after), 0.0)
    lg[...] = sticks
    for r in (6, 2):
        o_across(r)
    for b in range(SEQ):
        if b % 4 == 0:
            kv_loads[2 * (b // 4) + 1].wait()
        got = dot(lg[2 * b : 2 * b + 2, :].astype(BF16), vb[b])
        ho[b : b + 1, 0:HD] = got[0:1, :]
        ho[b : b + 1, HD : 2 * HD] = got[1:2, :]
    for r in (5, 3, 4):
        o_across(r)
    heads_out = ho[...]
    scaled = jnp.concatenate(
        [heads_out[:, HD * i : HD * i + HD] * hg[i : i + 1, :].astype(F32) for i in range(2)],
        axis=1,
    ).astype(BF16)
    sq[t] = jnp.broadcast_to(jnp.sum(heads_out * heads_out, axis=-1, keepdims=True), (SEQ, HD))
    o_last()
    for zi in range(NZ):
        part = dot_nt(scaled, ob[zi].reshape(256, 256))
        pc[t, :, 256 * zi : 256 * zi + 256] = part.astype(BF16)

    for d in (2, 1, 3):
        for k, buf in enumerate((sq, pc)):
            send(buf.at[t], buf.at[t], cs.at[k, d], cr.at[k, d], (z, x, c, td[d]))
    for d in near_first:
        arrived(kvb.at[lax.rem(z + NZ - d, NZ)], kzs.at[d], kzr.at[d])
    kvpart[...] = dot(rows_in, kvb[...].reshape(256, 256)).astype(BF16).reshape(8, SEQ, 256)
    for dx, dc in mates:
        g = xd[dx] * NC + cd[dc]
        send(kvpart.at[g], kvp.at[m], kps.at[dx, dc], kpr.at[dx, dc], (z, xd[dx], cd[dc], t))
    kvp[m] = kvpart[m]
    for d in (1, 3, 2):
        src = td[NT - d]
        for k, buf in enumerate((sq, pc)):
            arrived(buf.at[src], cs.at[k, d], cr.at[k, d])
    head_total = pc[0].astype(F32)
    square = sq[0]
    for i in range(1, NT):
        head_total = head_total + pc[i].astype(F32)
        square = square + sq[i]
    attention = head_total * lax.rsqrt(square[:, 0:1] / 1024.0 + EPS)
    residual = (tok[...].astype(F32) + attention).astype(BF16)
    for i in range(NT):
        res[i] = residual[:, 512 * i : 512 * i + 512]
    for cp in ld_ffn:
        cp.wait()
    data = residual.astype(F32)
    factor = lax.rsqrt(jnp.mean(data * data, axis=-1, keepdims=True) + EPS)
    gain = fg[...].astype(F32)
    pieces = []
    for i in range(16):
        pieces.append(data[:, HD * i : HD * i + HD] * factor * gain[i : i + 1, :])
        nf[i] = pieces[i].astype(BF16)
    normed_ffn = jnp.concatenate(pieces, axis=1).astype(BF16)

    def to_all(src, dst, ssem, rsem):
        for d in far_first + [0]:
            for dx, dc in ([(0, 0)] if d else []) + mates:
                p = (zd[d] * NX + xd[dx]) * NC + cd[dc]
                remote(src.at[p], dst.at[e], ssem, rsem, (zd[d], xd[dx], cd[dc], t)).start()

    block = nf[pl.ds(4 * t, 4)].reshape(64, HD)
    sbuf[...] = dot(dispatch, block).astype(BF16).reshape(NE, SEQ, HD)

    to_all(sbuf, rbuf, as_, ar)

    rbuf[e] = sbuf[e]

    for cp in ld_sh:
        cp.wait()
    both = dot(normed_ffn, sgu[...])
    gate = both[:, 0:HD]
    shared_hidden = (gate / (1.0 + jnp.exp(-gate)) * both[:, HD : 2 * HD]).astype(BF16)
    shared_part = dot(shared_hidden, sd[...]).astype(BF16)
    for i in range(NT):
        ssb[i] = shared_part[:, 512 * i : 512 * i + 512]
    for d in (2, 1, 3):
        p = td[d]
        send(ssb.at[p], ssr.at[t], sss.at[d], ssrr.at[d], (z, x, c, p))
    ssr[t] = ssb[t]
    logit = dot_nt(normed_ffn, rt[...])
    prob = 1.0 / (1.0 + jnp.exp(-logit))
    picked = jnp.where(code > 0.5, prob, 0.0)
    weight = SCALE * picked / jnp.sum(picked, axis=-1, keepdims=True)
    weight4 = jnp.concatenate([weight] * 4, axis=0)
    w_hi = weight4.astype(BF16)
    w_lo = (weight4 - w_hi.astype(F32)).astype(BF16)
    code4 = jnp.concatenate([code] * 4, axis=0).astype(BF16)
    r1 = iota((64, rows), 1)
    c1 = iota((64, rows), 0)
    spread_t = ones_where((r1 >> 4) == c1)
    slot_to = dot(code4, spread_t)
    fits = (slot_to == ((r1 & 3) + 1).astype(F32)) & (((r1 >> 2) & 3) == (c1 >> 4))
    comb_hi = jnp.where(fits, dot(w_hi, spread_t), 0.0).astype(BF16)
    comb_lo = jnp.where(fits, dot(w_lo, spread_t), 0.0).astype(BF16)

    def everyone(buf):
        return buf.at[pl.ds(0, NE - 1)]

    def wait_all(src, dst, ssem, rsem):
        cp = remote(everyone(src), everyone(dst), ssem, rsem, (z, x, 1 - c, t))
        cp.wait_recv()
        cp.wait_send()

    wait_all(sbuf, rbuf, as_, ar)

    p48 = iota((48, 256), 0)
    q48 = iota((48, 256), 1)
    for g in range(4):
        group = rbuf[16 * g : 16 * g + 16].reshape(256, HD)
        for j in range(4):
            pick = ones_where(q48 == ((p48 & 15) << 4) + 4 * j + (p48 >> 4))
            xb[48 * g : 48 * g + 48, HD * j : HD * j + HD] = dot(pick, group).astype(BF16)
    for cp in ld_ex:
        cp.wait()
    for d in (1, 3, 2):
        src = td[NT - d]
        for k in range(2):
            arrived(wgu.at[src, :, pl.ds(128 * k, 128)], ys.at[k, d], yr.at[k, d])
        arrived(wd.at[src], ys.at[2, d], yr.at[2, d])
    xv = xb[...]
    for d in (2, 1, 3):
        gs[d] = dot(xv, wgu[td[d]]).astype(BF16)
        send(gs.at[d], gr.at[d], gss.at[d], gsr.at[d], (z, x, c, td[d]))
    gate_up = dot(xv, wgu[t])
    for d in (2, 1, 3):
        arrived(gr.at[d], gss.at[d], gsr.at[d])
        gate_up = gate_up + gr[d].astype(F32)
    gate = gate_up[:, 0:HD]
    hidden = (gate / (1.0 + jnp.exp(-gate)) * gate_up[:, HD : 2 * HD]).astype(BF16)
    hs[t] = hidden
    for d in (2, 1, 3):
        send(hs.at[t], hs.at[t], hss.at[d], hsr.at[d], (z, x, c, td[d]))
    for d in (2, 1, 3):
        arrived(hs.at[td[NT - d]], hss.at[d], hsr.at[d])
    out = dot(hs[0], wd[0])
    for i in range(1, NT):
        out = out + dot(hs[i], wd[i])
    out = out.astype(BF16)

    pt = iota((256, 48), 1)
    qt = iota((256, 48), 0)
    for g in range(4):
        back = jnp.zeros((256, HD), F32)
        for j in range(4):
            pick = ones_where(qt == ((pt & 15) << 4) + 4 * j + (pt >> 4))
            back = back + dot(pick, out[48 * g : 48 * g + 48, HD * j : HD * j + HD])
        obuf[16 * g : 16 * g + 16] = back.astype(BF16).reshape(16, 16, HD)

    to_all(obuf, cbuf, rs_, rr)

    cbuf[e] = obuf[e]
    shared_total = jnp.zeros((SEQ, 512), F32)
    for d in (2, 1, 3):
        arrived(ssr.at[td[NT - d]], sss.at[d], ssrr.at[d])
    for i in range(NT):
        shared_total = shared_total + ssr[i].astype(F32)
    base = res[t].astype(F32) + shared_total
    for dx, dc in mates:
        src = kvp.at[lax.rem(x + NX - dx, NX) * NC + cd[dc]]
        arrived(src, kps.at[dx, dc], kpr.at[dx, dc])
    fresh = kvp[0].astype(F32)
    for i in range(1, 8):
        fresh = fresh + kvp[i].astype(F32)
    fk_o[...] = fresh[:, 0:HD].astype(BF16)
    fv_o[...] = fresh[:, HD : 2 * HD].astype(BF16)
    wait_all(obuf, cbuf, rs_, rr)
    came = cbuf[...].reshape(rows, HD)
    routed = dot(comb_hi, came) + dot(comb_lo, came)
    for j in range(4):
        mixed_o[:, HD * j : HD * j + HD] = (
            base[:, HD * j : HD * j + HD] + routed[SEQ * j : SEQ * j + SEQ]
        ).astype(BF16)
    for cp in pending:
        cp.wait_send()


def body(
    tokens, attn_gain, query_weight, key_weight, value_weight, out_weight, head_gain,
    past_keys, past_values, break_offset, cache_lengths, ffn_gain, router_weight,
    expert_routes, expert_gate, expert_up, expert_down, shared_gate, shared_up, shared_down,
):
    hbm = pl.BlockSpec(memory_space=pl.ANY)
    vmem = pl.BlockSpec(memory_space=pltpu.VMEM)
    smem = pl.BlockSpec(memory_space=pltpu.SMEM)
    v, dma = pltpu.VMEM, pltpu.SemaphoreType.DMA
    return pl.pallas_call(
        kernel,
        out_shape=(
            jax.ShapeDtypeStruct((SEQ, 512), BF16),
            jax.ShapeDtypeStruct((SEQ, HD), BF16),
            jax.ShapeDtypeStruct((SEQ, HD), BF16),
        ),
        in_specs=[smem if i == 10 else hbm for i in range(20)],
        out_specs=(vmem, vmem, vmem),
        scratch_shapes=[
            v((SEQ, 2048), BF16), v((16, HD), BF16), v((2, HD), BF16), v((16, HD), BF16),
            v((64, 2048), BF16), v((6, SEQ), jnp.int32), v((SEQ, 2, POS), F32),
            v((SEQ, POS, HD), BF16), v((SEQ, POS, HD), BF16),
            v((NZ, 32, 256), BF16), v((NZ, 32, 256), BF16), v((NZ, NX, NC, 32, 256), BF16),
            v((NT, 512, 256), BF16), v((NT, 128, 512), BF16),
            v((2048, 256), BF16), v((128, 2048), BF16),
            v((8, SEQ, 256), BF16), v((8, SEQ, 256), BF16),
            v((8, SEQ, 256), F32), v((8, SEQ, 256), F32),
            v((8, SEQ, 256), BF16), v((8, SEQ, 256), BF16),
            v((2 * SEQ, HD), F32), v((2 * SEQ, POS), F32), v((2 * SEQ, HD), jnp.int32),
            v((SEQ, 256), F32), v((NT, SEQ, 2048), BF16), v((NT, SEQ, HD), F32),
            v((16, SEQ, HD), BF16), v((NT, SEQ, 512), BF16),
            v((NE, SEQ, HD), BF16), v((NE, SEQ, HD), BF16), v((192, 512), BF16),
            v((NT, 192, 256), BF16), v((NT, 192, 256), BF16), v((NT, 192, HD), BF16),
            v((NE, SEQ, HD), BF16), v((NE, SEQ, HD), BF16),
            v((NT, SEQ, 512), BF16), v((NT, SEQ, 512), BF16),
            dma((24,)), dma((8,)),
            *[dma((NZ,)) for _ in range(6)],
            dma((NZ, NX)), dma((NZ, NX)), dma((NZ,)), dma((NZ,)),
            *[dma((NX, NC)) for _ in range(6)],
            dma((3, 4)), dma((3, 4)), dma((2, 4)), dma((2, 4)), dma, dma,
            dma((4,)), dma((4,)), dma((4,)), dma((4,)), dma, dma, dma((4,)), dma((4,)),
        ],
        compiler_params=pltpu.CompilerParams(
            collective_id=0, has_side_effects=True, vmem_limit_bytes=36 * 1024 * 1024
        ),
    )(
        tokens, attn_gain.reshape(16, HD), query_weight, key_weight, value_weight, out_weight,
        head_gain.reshape(2, HD), past_keys.reshape(SEQ, POS, HD),
        past_values.reshape(SEQ, POS, HD), break_offset, cache_lengths,
        ffn_gain.reshape(16, HD), router_weight.T, expert_routes.T, expert_gate, expert_up,
        expert_down, shared_gate, shared_up, shared_down,
    )


def solution(mesh):
    torus = Mesh(mesh.devices.reshape(NZ, NX, NC, NT), (*EP, "tp"))
    return jax.shard_map(
        body,
        mesh=torus,
        in_specs=(
            P(EP, None),
            P(),
            P(EP, "tp"),
            P(EP, "tp"),
            P(EP, "tp"),
            P(EP, "tp"),
            P("tp"),
            P(EP, None, "tp", None),
            P(EP, None, "tp", None),
            P(EP, "tp", None),
            P(EP),
            P(),
            P(),
            P(EP, None),
            P(EP, None, "tp"),
            P(EP, None, "tp"),
            P(EP, "tp", None),
            P(None, "tp"),
            P(None, "tp"),
            P("tp", None),
        ),
        out_specs=(P(EP, "tp"), P(EP, "tp"), P(EP, "tp")),
        check_vma=False,
    )
```

time: 94.1 us -> 91.4 us (0.971)
  local copies, waits for them, and re-layouts: 3.86 us -> 21.3 us
  Pallas kernels: 85.5 us -> 68.6 us
  other arithmetic: 3.78 us -> 0 us
    unnamed x3 -> x43, local copies, waits for them, and re-layouts: 3.86 us -> 21.3 us
    pallas_call x1, Pallas kernels: 85.5 us -> 68.6 us  [body(): pl.pallas_call(kernel, out_shape=(jax.ShapeDtypeStruct((SEQ, 512), BF16),...]
    broadcast_in_dim x3 -> x0, other arithmetic: 3.78 us -> none  [the longest x1 1.29 us: body(): attn_gain.astype(F32)[None]]
where the time goes in v2:
time: 91.4 us; the launch traced here: 90.6 us
  Pallas kernels  68.6 us (75%)
  local copies, waits for them, and re-layouts  21.3 us (23%)
    pallas_call x1, Pallas kernels, body(): pl.pallas_call(kernel, out_shape=(jax.ShapeDtypeStruct((SEQ, 512), BF16),...  68.6 us
    unnamed x43, local copies, waits for them, and re-layouts  21.3 us

profile of v2, /device:TPU:1, one launch (start us, length us, event | category | flops | bytes accessed | tf_op | source)
XLA Modules:
  0.0 90.6 jit_solution(13487149972973965034)
XLA Ops:
  0.6 2.2 %copy-done = bf16[16,1024,1,128]{3,1,2,0:T(8,128)(2,1)S(1)} copy-done((bf16[16,1024,1,128]{3,1,2,0:T(8,128)(2,1)S(1)}, bf16[16,1024,1,128]{3,1,2,0:T(8,128)(2,1)}, u32[]{:S(2)}) %copy-start) | copy-done | bytes 4194328
  2.8 2.2 %copy-done.1 = bf16[16,1024,1,128]{3,1,2,0:T(8,128)(2,1)S(1)} copy-done((bf16[16,1024,1,128]{3,1,2,0:T(8,128)(2,1)S(1)}, bf16[16,1024,1,128]{3,1,2,0:T(8,128)(2,1)}, u32[]{:S(2)}) %copy-start.1) | copy-done | bytes 4194328
  5.0 1.0 %copy-done.2 = bf16[1,2048,128]{2,1,0:T(8,128)(2,1)S(1)} copy-done((bf16[1,2048,128]{2,1,0:T(8,128)(2,1)S(1)}, bf16[1,2048,128]{2,1,0:T(8,128)(2,1)}, u32[]{:S(2)}) %copy-start.2) | copy-done | bytes 524312
  6.1 1.0 %copy-done.3 = bf16[1,2048,128]{2,1,0:T(8,128)(2,1)S(1)} copy-done((bf16[1,2048,128]{2,1,0:T(8,128)(2,1)S(1)}, bf16[1,2048,128]{2,1,0:T(8,128)(2,1)}, u32[]{:S(2)}) %copy-start.3) | copy-done | bytes 524312
  7.1 1.0 %copy-done.4 = bf16[1,128,2048]{2,1,0:T(8,128)(2,1)S(1)} copy-done((bf16[1,128,2048]{2,1,0:T(8,128)(2,1)S(1)}, bf16[1,128,2048]{2,1,0:T(8,128)(2,1)}, u32[]{:S(2)}) %copy-start.4) | copy-done | bytes 524312
  8.1 1.0 %copy-done.5 = bf16[2048,128]{1,0:T(8,128)(2,1)S(1)} copy-done((bf16[2048,128]{1,0:T(8,128)(2,1)S(1)}, bf16[2048,128]{1,0:T(8,128)(2,1)}, u32[]{:S(2)}) %copy-start.5) | copy-done | bytes 524312
  9.2 1.0 %copy-done.6 = bf16[2048,128]{1,0:T(8,128)(2,1)S(1)} copy-done((bf16[2048,128]{1,0:T(8,128)(2,1)S(1)}, bf16[2048,128]{1,0:T(8,128)(2,1)}, u32[]{:S(2)}) %copy-start.6) | copy-done | bytes 524312
  10.2 1.0 %copy-done.7 = bf16[128,2048]{1,0:T(8,128)(2,1)S(1)} copy-done((bf16[128,2048]{1,0:T(8,128)(2,1)S(1)}, bf16[128,2048]{1,0:T(8,128)(2,1)}, u32[]{:S(2)}) %copy-start.7) | copy-done | bytes 524312
  11.3 0.9 %copy-done.8 = bf16[2048,64]{0,1:T(8,128)(2,1)S(1)} copy-done((bf16[2048,64]{0,1:T(8,128)(2,1)S(1)}, bf16[2048,64]{0,1:T(8,128)(2,1)}, u32[]{:S(2)}) %copy-start.8) | copy-done | bytes 262168
  12.2 0.9 copy-done.9
  13.1 0.8 copy-done.10
  14.0 0.7 copy-done.11
  14.7 0.7 copy-done.12
  15.4 0.7 copy-done.13
  16.1 0.7 copy-done.14
  16.8 0.7 copy-done.15
  17.5 0.7 copy-done.16
  18.2 0.7 copy-done.17
  18.9 0.7 copy-done.18
  19.5 0.7 copy-done.19
  20.2 68.6 %shard_map.211 = (bf16[16,512]{1,0:T(8,128)(2,1)S(1)}, bf16[16,128]{1,0:T(8,128)(2,1)S(1)}, bf16[16,128]{1,0:T(8,128)(2,1)S(1)}) custom-call(bf16[16,2048]{1,0:T(8,128)(2,1)S(1)} %copy-done.10, bf16[16,128]{1,0:T(8,128)(2,1)S(1)} %bitcast.10, bf16[32,256]{1,0:T(8,128)(2,1)S(1)} %copy-done.11, bf16[32,128]{1,0:T(8,128)(2,1)S(1)} %copy-done.13, ...), custom_call_target="tpu_custom_call" | custom-call | tf_op jit(solution)/shard_map/pallas_call | solution.py:452
  88.8 0.6 copy.26
  89.4 0.6 copy.27
  90.0 0.6 copy.28
  (20 shorter events, 0.0 us)
Async XLA Ops:
  0.6 2.2 %copy-start = (bf16[16,1024,1,128]{3,1,2,0:T(8,128)(2,1)S(1)}, bf16[16,1024,1,128]{3,1,2,0:T(8,128)(2,1)}, u32[]{:S(2)}) copy-start(bf16[16,1024,1,128]{3,1,2,0:T(8,128)(2,1)} %param.27) | copy-start | bytes 12582916
  2.8 2.2 %copy-start.1 = (bf16[16,1024,1,128]{3,1,2,0:T(8,128)(2,1)S(1)}, bf16[16,1024,1,128]{3,1,2,0:T(8,128)(2,1)}, u32[]{:S(2)}) copy-start(bf16[16,1024,1,128]{3,1,2,0:T(8,128)(2,1)} %param.28) | copy-start | bytes 12582916
  5.0 1.0 %copy-start.2 = (bf16[1,2048,128]{2,1,0:T(8,128)(2,1)S(1)}, bf16[1,2048,128]{2,1,0:T(8,128)(2,1)}, u32[]{:S(2)}) copy-start(bf16[1,2048,128]{2,1,0:T(8,128)(2,1)} %eg_h.1) | copy-start | bytes 1572868
  6.1 1.0 %copy-start.3 = (bf16[1,2048,128]{2,1,0:T(8,128)(2,1)S(1)}, bf16[1,2048,128]{2,1,0:T(8,128)(2,1)}, u32[]{:S(2)}) copy-start(bf16[1,2048,128]{2,1,0:T(8,128)(2,1)} %eu_h.1) | copy-start | bytes 1572868
  7.1 1.0 %copy-start.4 = (bf16[1,128,2048]{2,1,0:T(8,128)(2,1)S(1)}, bf16[1,128,2048]{2,1,0:T(8,128)(2,1)}, u32[]{:S(2)}) copy-start(bf16[1,128,2048]{2,1,0:T(8,128)(2,1)} %ed_h.1) | copy-start | bytes 1572868
  8.1 1.0 %copy-start.5 = (bf16[2048,128]{1,0:T(8,128)(2,1)S(1)}, bf16[2048,128]{1,0:T(8,128)(2,1)}, u32[]{:S(2)}) copy-start(bf16[2048,128]{1,0:T(8,128)(2,1)} %sg_h.1) | copy-start | bytes 1572868
  9.2 1.0 %copy-start.6 = (bf16[2048,128]{1,0:T(8,128)(2,1)S(1)}, bf16[2048,128]{1,0:T(8,128)(2,1)}, u32[]{:S(2)}) copy-start(bf16[2048,128]{1,0:T(8,128)(2,1)} %su_h.1) | copy-start | bytes 1572868
  10.2 1.0 %copy-start.7 = (bf16[128,2048]{1,0:T(8,128)(2,1)S(1)}, bf16[128,2048]{1,0:T(8,128)(2,1)}, u32[]{:S(2)}) copy-start(bf16[128,2048]{1,0:T(8,128)(2,1)} %sd_h.1) | copy-start | bytes 1572868
  11.3 0.9 %copy-start.8 = (bf16[2048,64]{0,1:T(8,128)(2,1)S(1)}, bf16[2048,64]{0,1:T(8,128)(2,1)}, u32[]{:S(2)}) copy-start(bf16[2048,64]{0,1:T(8,128)(2,1)} %param.32) | copy-start | bytes 786436
  12.2 0.9 copy-start.9
  13.1 0.8 copy-start.10
  14.0 0.7 copy-start.11
  14.7 0.7 copy-start.12
  15.4 0.7 copy-start.13
  16.1 0.7 copy-start.14
  16.8 0.7 copy-start.15
  17.5 0.7 copy-start.16
  18.2 0.7 copy-start.17
  18.9 0.7 copy-start.18
  19.5 0.7 copy-start.19

commit v3 on v2

--- a/solution.py
+++ b/solution.py
@@ -483,7 +483,7 @@
             dma((4,)), dma((4,)), dma((4,)), dma((4,)), dma, dma, dma((4,)), dma((4,)),
         ],
         compiler_params=pltpu.CompilerParams(
-            collective_id=0, has_side_effects=True, vmem_limit_bytes=36 * 1024 * 1024
+            collective_id=0, has_side_effects=True, vmem_limit_bytes=60 * 1024 * 1024
         ),
     )(
         tokens, attn_gain.reshape(16, HD), query_weight, key_weight, value_weight, out_weight,

time: 91.4 us -> 73.3 us (0.80)
  local copies, waits for them, and re-layouts: 21.3 us -> 3.86 us
    unnamed x43 -> x3, local copies, waits for them, and re-layouts: 21.3 us -> 3.86 us
where the time goes in v3:
time: 73.3 us; the launch traced here: 73 us
  Pallas kernels  68.5 us (93%)
  local copies, waits for them, and re-layouts  3.86 us (5%)
    pallas_call x1, Pallas kernels, body(): pl.pallas_call(kernel, out_shape=(jax.ShapeDtypeStruct((SEQ, 512), BF16),...  68.5 us
    unnamed x3, local copies, waits for them, and re-layouts  3.86 us

profile of v3, /device:TPU:1, one launch (start us, length us, event | category | flops | bytes accessed | tf_op | source)
XLA Modules:
  0.0 73.0 jit_solution(10696621539827843354)
XLA Ops:
  0.6 68.5 %shard_map.211 = (bf16[16,512]{1,0:T(8,128)(2,1)}, bf16[16,128]{1,0:T(8,128)(2,1)}, bf16[16,128]{1,0:T(8,128)(2,1)}) custom-call(bf16[16,2048]{1,0:T(8,128)(2,1)} %tok_h.1, bf16[16,128]{1,0:T(8,128)(2,1)} %bitcast.10, bf16[32,256]{1,0:T(8,128)(2,1)} %wq_h.1, bf16[32,128]{1,0:T(8,128)(2,1)} %wk_h.1, bf16[32,128]{1,0:T(8,128)(2,1)} %wv_h.1, ...), custom_call_target="tpu_custom_call" | custom-call | tf_op jit(solution)/shard_map/pallas_call | solution.py:452
  69.2 1.3 %copy.26 = bf16[16,512]{1,0:T(8,128)(2,1)} copy(bf16[16,512]{1,0:T(8,128)(2,1)} %get-tuple-element.6) | data formatting | bytes 32768
  70.5 1.3 %copy.27 = bf16[16,128]{1,0:T(8,128)(2,1)} copy(bf16[16,128]{1,0:T(8,128)(2,1)} %get-tuple-element.7) | data formatting | bytes 8192
  71.8 1.3 %copy.28 = bf16[16,128]{1,0:T(8,128)(2,1)} copy(bf16[16,128]{1,0:T(8,128)(2,1)} %get-tuple-element.8) | data formatting | bytes 8192

commit v4 on v3

--- a/solution.py
+++ b/solution.py
@@ -41,7 +41,7 @@
     mixed_o, fk_o, fv_o,
     tok, ag, hg, fg, rt, er, off, kb, vb, qb, kvb, ob, wgu, wd, sgu, sd,
     tkb, tk, part, qp, kvpart, kvp,
-    qs, lg, lenb, ho, pc, sq, nf, res, sbuf, rbuf, xb, gs, gr, hs, obuf, cbuf, ssb, ssr,
+    qs, lg, lenb, ho, pc, sq, nf, res, sbuf, rbuf, gs, gr, hs, obuf, cbuf, ssb, ssr,
     lsem, kvsem,
     qzs, qzr, kzs, kzr, ozs, ozr, oxs, oxr, ods, odr, tks, tkr, qps, qpr, kps, kpr,
     ys, yr, cs, cr, as_, ar, gss, gsr, hss, hsr, rs_, rr, sss, ssrr,
@@ -119,11 +119,6 @@
     first += [(z, x, c, td[d]) for d in range(1, NT)]
     for dev in first:
         pl.semaphore_signal(barrier, inc=1, device_id=dev, device_id_type=MESH)
-    pl.semaphore_wait(barrier, len(first))
-
-    ld_q.wait()
-    for d in far_first:
-        send(qb.at[z], qb.at[z], qzs.at[d], qzr.at[d], (zd[d], x, c, t))
 
     for cp in ld_tok:
         cp.wait()
@@ -142,55 +137,9 @@
         for k in range(1, 8):
             j = (g + k) % 8
             own = jnp.where(chunk == j, pltpu.roll(blocks[j], 32 * k, 1), own)
-        part[g] = own
-    for dx, dc in mates:
-        g = xd[dx] * NC + cd[dc]
-        tkb[g] = part[g].astype(BF16)
-        send(tkb.at[g], tk.at[m], tks.at[dx, dc], tkr.at[dx, dc], (z, xd[dx], cd[dc], t))
-    tk[m] = part[m].astype(BF16)
-
-    ld_o.wait()
-    mine_o = ob.at[z, x, c]
-    for d in far_first:
-        send(mine_o, mine_o, ozs.at[d], ozr.at[d], (zd[d], x, c, t))
-
-    def o_along(r):
-        src = ob.at[zd[r], x, c]
-        for i in (2, 1, 3):
-            send(src, src, oxs.at[r, i], oxr.at[r, i], (z, xd[i], c, t))
-
-    def o_forward(r):
-        src = ob.at[zd[r], x, c]
-        arrived(src, ozs.at[NZ - r], ozr.at[NZ - r])
-        o_along(r)
-
-    def o_across(r):
-        for i in (1, 3, 2):
-            arrived(ob.at[zd[r], xd[i], c], oxs.at[r, NX - i], oxr.at[r, NX - i])
-        src = ob.at[zd[r], :, c]
-        send(src, src, ods.at[r], odr.at[r], (z, x, 1 - c, t))
-
-    def o_last():
-        for r in range(NZ):
-            arrived(ob.at[zd[r], :, 1 - c], ods.at[r], odr.at[r])
-
-    o_along(0)
-    for cp in ld_kv:
-        cp.wait()
-    for d in far_first:
-        send(kvb.at[z], kvb.at[z], kzs.at[d], kzr.at[d], (zd[d], x, c, t))
-
-    for d in (1, 3, 2):
-        p = td[d]
-        dev = (z, x, c, p)
-        theirs = pl.ds(pl.multiple_of(p * 512, 512), 512)
-        for k, src in enumerate((eg_h, eu_h)):
-            half = pl.ds(128 * k, 128)
-            send(src.at[0, theirs, :], wgu.at[t, :, half], ys.at[k, d], yr.at[k, d], dev)
-        send(ed_h.at[0, :, theirs], wd.at[t], ys.at[2, d], yr.at[2, d], dev)
-
+        tkb[g] = own.astype(BF16)
     ld_er.wait()
-    rows = NE * SEQ
+    rows = NE * 12
     chosen = iota((NE, SEQ), 0) == er[0:1, :]
     for k in range(1, 6):
         chosen = chosen | (iota((NE, SEQ), 0) == er[k : k + 1, :])
@@ -201,32 +150,86 @@
     eye = ones_where(iota((SEQ, SEQ), 0) == iota((SEQ, SEQ), 1))
     code4_t = dot(code_t, repeat).astype(BF16)
     code = dot_nt(eye, code_t)
-    r0 = iota((rows, 64), 0)
+    q0 = iota((rows, 64), 0) >> 2
+    j0 = iota((rows, 64), 0) & 3
+    e0 = (q0 * 171) >> 9
     c0 = iota((rows, 64), 1)
-    spread = ones_where((r0 >> 4) == c0)
+    spread = ones_where(e0 == c0)
     slot_of = dot(spread, code4_t)
-    want = ((r0 & 3) + 1).astype(F32)
-    dispatch = ones_where((slot_of == want) & (((r0 >> 2) & 3) == (c0 >> 4)))
+    want = (q0 - 3 * e0 + 1).astype(F32)
+    dispatch = ones_where((slot_of == want) & (j0 == (c0 >> 4)))
+
+    pl.semaphore_wait(barrier, len(first))
+
+    ld_q.wait()
+    for d in far_first:
+        send(qb.at[z], qb.at[z], qzs.at[d], qzr.at[d], (zd[d], x, c, t))
+
+    for dx, dc in mates:
+        g = xd[dx] * NC + cd[dc]
+        send(tkb.at[g], tk.at[m], tks.at[dx, dc], tkr.at[dx, dc], (z, xd[dx], cd[dc], t))
+    tk[m] = tkb[m]
+
+    ld_o.wait()
+    mine_o = ob.at[z, x, c]
+    for d in far_first:
+        send(mine_o, mine_o, ozs.at[d], ozr.at[d], (zd[d], x, c, t))
+
+    def o_along(r):
+        src = ob.at[zd[r], x, c]
+        for i in (2, 1, 3):
+            send(src, src, oxs.at[r, i], oxr.at[r, i], (z, xd[i], c, t))
+
+    def o_forward(r):
+        src = ob.at[zd[r], x, c]
+        arrived(src, ozs.at[NZ - r], ozr.at[NZ - r])
+        o_along(r)
+
+    def o_across(r):
+        for i in (1, 3, 2):
+            arrived(ob.at[zd[r], xd[i], c], oxs.at[r, NX - i], oxr.at[r, NX - i])
+        src = ob.at[zd[r], :, c]
+        send(src, src, ods.at[r], odr.at[r], (z, x, 1 - c, t))
+
+    def o_last():
+        for r in range(NZ):
+            arrived(ob.at[zd[r], :, 1 - c], ods.at[r], odr.at[r])
+
+    o_along(0)
+    for cp in ld_kv:
+        cp.wait()
+    for d in far_first:
+        send(kvb.at[z], kvb.at[z], kzs.at[d], kzr.at[d], (zd[d], x, c, t))
+
+    for d in (1, 3, 2):
+        p = td[d]
+        dev = (z, x, c, p)
+        theirs = pl.ds(pl.multiple_of(p * 512, 512), 512)
+        for k, src in enumerate((eg_h, eu_h)):
+            half = pl.ds(128 * k, 128)
+            send(src.at[0, theirs, :], wgu.at[t, :, half], ys.at[k, d], yr.at[k, d], dev)
 
     for dx, dc in mates:
         src = tk.at[lax.rem(x + NX - dx, NX) * NC + cd[dc]]
         arrived(src, tks.at[dx, dc], tkr.at[dx, dc])
+    for r in (7, 1, 6, 2):
+        o_forward(r)
     for d in near_first:
         arrived(qb.at[lax.rem(z + NZ - d, NZ)], qzs.at[d], qzr.at[d])
     rows_in = tk[...].reshape(8 * SEQ, 256)
-    part[...] = dot(rows_in, qb[...].reshape(256, 256)).reshape(8, SEQ, 256)
+    part[...] = dot(rows_in, qb[...].reshape(256, 256)).astype(BF16).reshape(8, SEQ, 256)
     for dx, dc in mates:
         g = xd[dx] * NC + cd[dc]
         send(part.at[g], qp.at[m], qps.at[dx, dc], qpr.at[dx, dc], (z, xd[dx], cd[dc], t))
     qp[m] = part[m]
-    for r in (7, 1, 6, 2, 5, 3, 4):
+    for r in (5, 3, 4):
         o_forward(r)
     for dx, dc in mates:
         src = qp.at[lax.rem(x + NX - dx, NX) * NC + cd[dc]]
         arrived(src, qps.at[dx, dc], qpr.at[dx, dc])
-    total = qp[0]
+    total = qp[0].astype(F32)
     for i in range(1, 8):
-        total = total + qp[i]
+        total = total + qp[i].astype(F32)
     queries = total.astype(BF16).astype(F32)
 
     for h in range(2):
@@ -318,18 +321,30 @@
         nf[i] = pieces[i].astype(BF16)
     normed_ffn = jnp.concatenate(pieces, axis=1).astype(BF16)
 
-    def to_all(src, dst, ssem, rsem):
-        for d in far_first + [0]:
-            for dx, dc in ([(0, 0)] if d else []) + mates:
-                p = (zd[d] * NX + xd[dx]) * NC + cd[dc]
-                remote(src.at[p], dst.at[e], ssem, rsem, (zd[d], xd[dx], cd[dc], t)).start()
-
+    for d in (1, 3, 2):
+        theirs = pl.ds(pl.multiple_of(td[d] * 512, 512), 512)
+        send(ed_h.at[0, :, theirs], wd.at[t], ys.at[2, d], yr.at[2, d], (z, x, c, td[d]))
     block = nf[pl.ds(4 * t, 4)].reshape(64, HD)
-    sbuf[...] = dot(dispatch, block).astype(BF16).reshape(NE, SEQ, HD)
-
-    to_all(sbuf, rbuf, as_, ar)
-
-    rbuf[e] = sbuf[e]
+    sbuf[...] = dot(dispatch, block).astype(BF16).reshape(3 * NE, 4, HD)
+    order = (3, 4, 5, 6, 7, 0, 1, 2)
+
+    def three(i):
+        return pl.ds(3 * i, 3)
+
+    def half_of(r):
+        return order.index(r) // 4
+
+    def around(r):
+        return [(0, 0), *mates] if r else mates
+
+    for r in (4, 5, 3, 6, 2, 7, 1, 0):
+        d = (NZ - r) % NZ
+        to = three(8 * order.index(r) + m)
+        for dx, dc in around(r):
+            p = (zd[d] * NX + xd[dx]) * NC + cd[dc]
+            dev = (zd[d], xd[dx], cd[dc], t)
+            remote(sbuf.at[three(p)], rbuf.at[to], as_.at[half_of(r)], ar.at[half_of(r)], dev).start()
+    rbuf[three(8 * order.index(0) + m)] = sbuf[three(e)]
 
     for cp in ld_sh:
         cp.wait()
@@ -351,70 +366,82 @@
     w_hi = weight4.astype(BF16)
     w_lo = (weight4 - w_hi.astype(F32)).astype(BF16)
     code4 = jnp.concatenate([code] * 4, axis=0).astype(BF16)
-    r1 = iota((64, rows), 1)
+    q1 = iota((64, rows), 1) >> 2
+    j1 = iota((64, rows), 1) & 3
+    e1 = (q1 * 171) >> 9
     c1 = iota((64, rows), 0)
-    spread_t = ones_where((r1 >> 4) == c1)
+    spread_t = ones_where(e1 == c1)
     slot_to = dot(code4, spread_t)
-    fits = (slot_to == ((r1 & 3) + 1).astype(F32)) & (((r1 >> 2) & 3) == (c1 >> 4))
+    fits = (slot_to == (q1 - 3 * e1 + 1).astype(F32)) & (j1 == (c1 >> 4))
     comb_hi = jnp.where(fits, dot(w_hi, spread_t), 0.0).astype(BF16)
     comb_lo = jnp.where(fits, dot(w_lo, spread_t), 0.0).astype(BF16)
 
-    def everyone(buf):
-        return buf.at[pl.ds(0, NE - 1)]
-
-    def wait_all(src, dst, ssem, rsem):
-        cp = remote(everyone(src), everyone(dst), ssem, rsem, (z, x, 1 - c, t))
-        cp.wait_recv()
-        cp.wait_send()
-
-    wait_all(sbuf, rbuf, as_, ar)
-
-    p48 = iota((48, 256), 0)
-    q48 = iota((48, 256), 1)
-    for g in range(4):
-        group = rbuf[16 * g : 16 * g + 16].reshape(256, HD)
-        for j in range(4):
-            pick = ones_where(q48 == ((p48 & 15) << 4) + 4 * j + (p48 >> 4))
-            xb[48 * g : 48 * g + 48, HD * j : HD * j + HD] = dot(pick, group).astype(BF16)
+    def to_rows(half, g):
+        group = rbuf[96 * half + 48 * g : 96 * half + 48 * g + 48].reshape(192, HD)
+        p, q = iota((48, 192), 0), iota((48, 192), 1)
+        cols = [dot(ones_where(q == 4 * p + j), group).astype(BF16) for j in range(4)]
+        return jnp.concatenate(cols, axis=1)
+
+    def start_half(half):
+        n = 96 if half == 0 else 93
+        both = remote(
+            sbuf.at[pl.ds(0, n)], rbuf.at[pl.ds(0, n)], as_.at[half], ar.at[half],
+            (z, x, 1 - c, t),
+        )
+        both.wait_recv()
+        rows_of = jnp.concatenate([to_rows(half, 0), to_rows(half, 1)], axis=0)
+        for d in (2, 1, 3):
+            gs[half, d] = dot(rows_of, wgu[td[d]]).astype(BF16)
+            send(gs.at[half, d], gr.at[half, d], gss.at[half, d], gsr.at[half, d], (z, x, c, td[d]))
+        return dot(rows_of, wgu[t]), both
+
+    def middle_half(half, gate_up):
+        for d in (2, 1, 3):
+            arrived(gr.at[half, d], gss.at[half, d], gsr.at[half, d])
+            gate_up = gate_up + gr[half, d].astype(F32)
+        gate = gate_up[:, 0:HD]
+        hidden = gate / (1.0 + jnp.exp(-gate)) * gate_up[:, HD : 2 * HD]
+        hs[half, t] = hidden.astype(BF16)
+        for d in (2, 1, 3):
+            own = hs.at[half, t]
+            send(own, own, hss.at[half, d], hsr.at[half, d], (z, x, c, td[d]))
+
+    def end_half(half):
+        for d in (2, 1, 3):
+            arrived(hs.at[half, td[NT - d]], hss.at[half, d], hsr.at[half, d])
+        out = dot(hs[half, 0], wd[0])
+        for i in range(1, NT):
+            out = out + dot(hs[half, i], wd[i])
+        out = out.astype(BF16)
+        p, q = iota((192, 48), 1), iota((192, 48), 0)
+        for g in range(2):
+            back = jnp.zeros((192, HD), F32)
+            for j in range(4):
+                block = out[48 * g : 48 * g + 48, HD * j : HD * j + HD]
+                back = back + dot(ones_where(q == 4 * p + j), block)
+            at = 96 * half + 48 * g
+            obuf[at : at + 48] = back.astype(BF16).reshape(48, 4, HD)
+        for r in ((4, 5, 3, 6) if half == 0 else (2, 7, 1, 0)):
+            for dx, dc in around(r):
+                p = 8 * order.index(r) + xd[dx] * NC + cd[dc]
+                dev = (zd[r], xd[dx], cd[dc], t)
+                remote(obuf.at[three(p)], cbuf.at[three(e)], rs_, rr, dev).start()
+
     for cp in ld_ex:
         cp.wait()
     for d in (1, 3, 2):
         src = td[NT - d]
         for k in range(2):
             arrived(wgu.at[src, :, pl.ds(128 * k, 128)], ys.at[k, d], yr.at[k, d])
-        arrived(wd.at[src], ys.at[2, d], yr.at[2, d])
-    xv = xb[...]
-    for d in (2, 1, 3):
-        gs[d] = dot(xv, wgu[td[d]]).astype(BF16)
-        send(gs.at[d], gr.at[d], gss.at[d], gsr.at[d], (z, x, c, td[d]))
-    gate_up = dot(xv, wgu[t])
-    for d in (2, 1, 3):
-        arrived(gr.at[d], gss.at[d], gsr.at[d])
-        gate_up = gate_up + gr[d].astype(F32)
-    gate = gate_up[:, 0:HD]
-    hidden = (gate / (1.0 + jnp.exp(-gate)) * gate_up[:, HD : 2 * HD]).astype(BF16)
-    hs[t] = hidden
-    for d in (2, 1, 3):
-        send(hs.at[t], hs.at[t], hss.at[d], hsr.at[d], (z, x, c, td[d]))
-    for d in (2, 1, 3):
-        arrived(hs.at[td[NT - d]], hss.at[d], hsr.at[d])
-    out = dot(hs[0], wd[0])
-    for i in range(1, NT):
-        out = out + dot(hs[i], wd[i])
-    out = out.astype(BF16)
-
-    pt = iota((256, 48), 1)
-    qt = iota((256, 48), 0)
-    for g in range(4):
-        back = jnp.zeros((256, HD), F32)
-        for j in range(4):
-            pick = ones_where(qt == ((pt & 15) << 4) + 4 * j + (pt >> 4))
-            back = back + dot(pick, out[48 * g : 48 * g + 48, HD * j : HD * j + HD])
-        obuf[16 * g : 16 * g + 16] = back.astype(BF16).reshape(16, 16, HD)
-
-    to_all(obuf, cbuf, rs_, rr)
-
-    cbuf[e] = obuf[e]
+    gate_up0, sent0 = start_half(0)
+    gate_up1, sent1 = start_half(1)
+    middle_half(0, gate_up0)
+    middle_half(1, gate_up1)
+    for d in (1, 3, 2):
+        arrived(wd.at[td[NT - d]], ys.at[2, d], yr.at[2, d])
+    end_half(0)
+    end_half(1)
+    cbuf[three(e)] = obuf[three(8 * order.index(0) + m)]
     shared_total = jnp.zeros((SEQ, 512), F32)
     for d in (2, 1, 3):
         arrived(ssr.at[td[NT - d]], sss.at[d], ssrr.at[d])
@@ -429,15 +456,27 @@
         fresh = fresh + kvp[i].astype(F32)
     fk_o[...] = fresh[:, 0:HD].astype(BF16)
     fv_o[...] = fresh[:, HD : 2 * HD].astype(BF16)
-    wait_all(obuf, cbuf, rs_, rr)
+    back = remote(
+        obuf.at[pl.ds(0, 3 * NE - 3)], cbuf.at[pl.ds(0, 3 * NE - 3)], rs_, rr, (z, x, 1 - c, t)
+    )
+    back.wait_recv()
     came = cbuf[...].reshape(rows, HD)
     routed = dot(comb_hi, came) + dot(comb_lo, came)
     for j in range(4):
         mixed_o[:, HD * j : HD * j + HD] = (
             base[:, HD * j : HD * j + HD] + routed[SEQ * j : SEQ * j + SEQ]
         ).astype(BF16)
-    for cp in pending:
+    for cp in [*pending, sent0, sent1, back]:
         cp.wait_send()
+
+
+def hand_over(a, b, c, a_o, b_o, c_o, sem):
+    moves = []
+    for i, (src, dst) in enumerate(((a, a_o), (b, b_o), (c, c_o))):
+        moves.append(pltpu.make_async_copy(src, dst, sem.at[i]))
+        moves[i].start()
+    for cp in moves:
+        cp.wait()
 
 
 def body(
@@ -449,7 +488,7 @@
     vmem = pl.BlockSpec(memory_space=pltpu.VMEM)
     smem = pl.BlockSpec(memory_space=pltpu.SMEM)
     v, dma = pltpu.VMEM, pltpu.SemaphoreType.DMA
-    return pl.pallas_call(
+    outs = pl.pallas_call(
         kernel,
         out_shape=(
             jax.ShapeDtypeStruct((SEQ, 512), BF16),
@@ -466,21 +505,21 @@
             v((NT, 512, 256), BF16), v((NT, 128, 512), BF16),
             v((2048, 256), BF16), v((128, 2048), BF16),
             v((8, SEQ, 256), BF16), v((8, SEQ, 256), BF16),
-            v((8, SEQ, 256), F32), v((8, SEQ, 256), F32),
+            v((8, SEQ, 256), BF16), v((8, SEQ, 256), BF16),
             v((8, SEQ, 256), BF16), v((8, SEQ, 256), BF16),
             v((2 * SEQ, HD), F32), v((2 * SEQ, POS), F32), v((2 * SEQ, HD), jnp.int32),
             v((SEQ, 256), F32), v((NT, SEQ, 2048), BF16), v((NT, SEQ, HD), F32),
             v((16, SEQ, HD), BF16), v((NT, SEQ, 512), BF16),
-            v((NE, SEQ, HD), BF16), v((NE, SEQ, HD), BF16), v((192, 512), BF16),
-            v((NT, 192, 256), BF16), v((NT, 192, 256), BF16), v((NT, 192, HD), BF16),
-            v((NE, SEQ, HD), BF16), v((NE, SEQ, HD), BF16),
+            v((3 * NE, 4, HD), BF16), v((3 * NE, 4, HD), BF16),
+            v((2, NT, 96, 256), BF16), v((2, NT, 96, 256), BF16), v((2, NT, 96, HD), BF16),
+            v((3 * NE, 4, HD), BF16), v((3 * NE, 4, HD), BF16),
             v((NT, SEQ, 512), BF16), v((NT, SEQ, 512), BF16),
             dma((24,)), dma((8,)),
             *[dma((NZ,)) for _ in range(6)],
             dma((NZ, NX)), dma((NZ, NX)), dma((NZ,)), dma((NZ,)),
             *[dma((NX, NC)) for _ in range(6)],
-            dma((3, 4)), dma((3, 4)), dma((2, 4)), dma((2, 4)), dma, dma,
-            dma((4,)), dma((4,)), dma((4,)), dma((4,)), dma, dma, dma((4,)), dma((4,)),
+            dma((3, 4)), dma((3, 4)), dma((2, 4)), dma((2, 4)), dma((2,)), dma((2,)),
+            dma((2, 4)), dma((2, 4)), dma((2, 4)), dma((2, 4)), dma, dma, dma((4,)), dma((4,)),
         ],
         compiler_params=pltpu.CompilerParams(
             collective_id=0, has_side_effects=True, vmem_limit_bytes=60 * 1024 * 1024
@@ -492,6 +531,13 @@
         ffn_gain.reshape(16, HD), router_weight.T, expert_routes.T, expert_gate, expert_up,
         expert_down, shared_gate, shared_up, shared_down,
     )
+    return pl.pallas_call(
+        hand_over,
+        out_shape=tuple(jax.ShapeDtypeStruct(o.shape, o.dtype) for o in outs),
+        in_specs=[hbm] * 3,
+        out_specs=(hbm,) * 3,
+        scratch_shapes=[dma((3,))],
+    )(*outs)
 
 
 def solution(mesh):

time: 73.3 us -> 66.4 us (0.906)
  local copies, waits for them, and re-layouts: 3.86 us -> 0 us
  Pallas kernels: 68.5 us -> 65.7 us
    pallas_call x1, Pallas kernels: 68.5 us -> 63.8 us  [body(): pl.pallas_call(kernel, out_shape=(jax.ShapeDtypeStruct((SEQ, 512), BF16),...]
    unnamed x3 -> x0, local copies, waits for them, and re-layouts: 3.86 us -> none
    pallas_call x0 -> x1, Pallas kernels: none -> 1.87 us  [body(): pl.pallas_call(hand_over, out_shape=tuple((jax.ShapeDtypeStruct(o.shape,...]
where the time goes in v4:
time: 66.4 us; the launch traced here: 66.3 us
  Pallas kernels  65.7 us (99%)
    pallas_call x1, Pallas kernels, body(): pl.pallas_call(kernel, out_shape=(jax.ShapeDtypeStruct((SEQ, 512), BF16),...  63.8 us
    pallas_call x1, Pallas kernels, body(): pl.pallas_call(hand_over, out_shape=tuple((jax.ShapeDtypeStruct(o.shape,...  1.87 us

profile of v4, /device:TPU:1, one launch (start us, length us, event | category | flops | bytes accessed | tf_op | source)
XLA Modules:
  0.0 66.3 jit_solution(16164427863741800785)
XLA Ops:
  0.6 63.8 %shard_map.211 = (bf16[16,512]{1,0:T(8,128)(2,1)}, bf16[16,128]{1,0:T(8,128)(2,1)}, bf16[16,128]{1,0:T(8,128)(2,1)}) custom-call(bf16[16,2048]{1,0:T(8,128)(2,1)} %tok_h.1, bf16[16,128]{1,0:T(8,128)(2,1)} %bitcast.10, bf16[32,256]{1,0:T(8,128)(2,1)} %wq_h.1, bf16[32,128]{1,0:T(8,128)(2,1)} %wk_h.1, bf16[32,128]{1,0:T(8,128)(2,1)} %wv_h.1, ...), custom_call_target="tpu_custom_call" | custom-call | tf_op jit(solution)/shard_map/pallas_call | solution.py:491
  64.4 1.9 %shard_map.212 = (bf16[16,512]{1,0:T(8,128)(2,1)}, bf16[16,128]{1,0:T(8,128)(2,1)}, bf16[16,128]{1,0:T(8,128)(2,1)}) custom-call(bf16[16,512]{1,0:T(8,128)(2,1)} %get-tuple-element.6.a, bf16[16,128]{1,0:T(8,128)(2,1)} %get-tuple-element.7.b, bf16[16,128]{1,0:T(8,128)(2,1)} %get-tuple-element.8.c), custom_call_target="tpu_custom_call" | custom-call | tf_op jit(solution)/shard_map/pallas_call | solution.py:534

commit v5 on v4

--- a/solution.py
+++ b/solution.py
@@ -36,15 +36,15 @@
 
 
 def kernel(
-    tok_h, ag_h, wq_h, wk_h, wv_h, wo_h, hg_h, pk_h, pv_h, off_h, lens, fg_h, rt_h, er_h,
+    tok_h, ag_h, wq_h, wk_h, wv_h, wo_h, hg_h, pk_h, pv_h, off_h, lens_h, fg_h, rt_h, er_h,
     eg_h, eu_h, ed_h, sg_h, su_h, sd_h,
     mixed_o, fk_o, fv_o,
     tok, ag, hg, fg, rt, er, off, kb, vb, qb, kvb, ob, wgu, wd, sgu, sd,
     tkb, tk, part, qp, kvpart, kvp,
-    qs, lg, lenb, ho, pc, sq, nf, res, sbuf, rbuf, gs, gr, hs, obuf, cbuf, ssb, ssr,
-    lsem, kvsem,
+    qs, lg, lenb, ho, pcs, pc, sq, fs, res, sbuf, rbuf, gs, gr, hs, obuf, cbuf, ssb, ssr,
+    lens, tokb, mixed, fresh, lsem, kvsem,
     qzs, qzr, kzs, kzr, ozs, ozr, oxs, oxr, ods, odr, tks, tkr, qps, qpr, kps, kpr,
-    ys, yr, cs, cr, as_, ar, gss, gsr, hss, hsr, rs_, rr, sss, ssrr,
+    ys, yr, cs, cr, as_, ar, gss, gsr, hss, hsr, rs_, rr, sss, ssrr, as2, ar2, fss, fsr,
 ):
     z = lax.axis_index("ep_0")
     x = lax.axis_index("ep_1")
@@ -92,7 +92,7 @@
         load(wv_h, kvb.at[z, :, pl.ds(128, 128)]),
     ]
     ld_er = load(er_h, er)
-    ld_att = [load(off_h, off), load(hg_h, hg)]
+    ld_att = [load(off_h, off), load(hg_h, hg), load(lens_h, lens)]
     kv_loads = []
     for i in range(4):
         ds = pl.ds(4 * i, 4)
@@ -107,6 +107,7 @@
         load(sd_h, sd),
     ]
     mine = pl.ds(pl.multiple_of(t * 512, 512), 512)
+    ld_own = load(tok_h.at[:, mine], tokb)
     ld_ex = [
         load(eg_h.at[0, mine, :], wgu.at[t, :, pl.ds(0, 128)]),
         load(eu_h.at[0, mine, :], wgu.at[t, :, pl.ds(128, 128)]),
@@ -212,8 +213,6 @@
     for dx, dc in mates:
         src = tk.at[lax.rem(x + NX - dx, NX) * NC + cd[dc]]
         arrived(src, tks.at[dx, dc], tkr.at[dx, dc])
-    for r in (7, 1, 6, 2):
-        o_forward(r)
     for d in near_first:
         arrived(qb.at[lax.rem(z + NZ - d, NZ)], qzs.at[d], qzr.at[d])
     rows_in = tk[...].reshape(8 * SEQ, 256)
@@ -222,7 +221,7 @@
         g = xd[dx] * NC + cd[dc]
         send(part.at[g], qp.at[m], qps.at[dx, dc], qpr.at[dx, dc], (z, xd[dx], cd[dc], t))
     qp[m] = part[m]
-    for r in (5, 3, 4):
+    for r in (7, 1, 6, 2, 5, 3, 4):
         o_forward(r)
     for dx, dc in mates:
         src = qp.at[lax.rem(x + NX - dx, NX) * NC + cd[dc]]
@@ -283,13 +282,15 @@
     ).astype(BF16)
     sq[t] = jnp.broadcast_to(jnp.sum(heads_out * heads_out, axis=-1, keepdims=True), (SEQ, HD))
     o_last()
-    for zi in range(NZ):
-        part = dot_nt(scaled, ob[zi].reshape(256, 256))
-        pc[t, :, 256 * zi : 256 * zi + 256] = part.astype(BF16)
+    for i in range(NT):
+        halves = [dot_nt(scaled, ob[zi].reshape(256, 256)) for zi in (2 * i, 2 * i + 1)]
+        pcs[i] = jnp.concatenate(halves, axis=1).astype(BF16)
 
     for d in (2, 1, 3):
-        for k, buf in enumerate((sq, pc)):
-            send(buf.at[t], buf.at[t], cs.at[k, d], cr.at[k, d], (z, x, c, td[d]))
+        dev = (z, x, c, td[d])
+        send(sq.at[t], sq.at[t], cs.at[0, d], cr.at[0, d], dev)
+        send(pcs.at[td[d]], pc.at[t], cs.at[1, d], cr.at[1, d], dev)
+    pc[t] = pcs[t]
     for d in near_first:
         arrived(kvb.at[lax.rem(z + NZ - d, NZ)], kzs.at[d], kzr.at[d])
     kvpart[...] = dot(rows_in, kvb[...].reshape(256, 256)).astype(BF16).reshape(8, SEQ, 256)
@@ -307,24 +308,13 @@
         head_total = head_total + pc[i].astype(F32)
         square = square + sq[i]
     attention = head_total * lax.rsqrt(square[:, 0:1] / 1024.0 + EPS)
-    residual = (tok[...].astype(F32) + attention).astype(BF16)
-    for i in range(NT):
-        res[i] = residual[:, 512 * i : 512 * i + 512]
-    for cp in ld_ffn:
-        cp.wait()
-    data = residual.astype(F32)
-    factor = lax.rsqrt(jnp.mean(data * data, axis=-1, keepdims=True) + EPS)
-    gain = fg[...].astype(F32)
-    pieces = []
-    for i in range(16):
-        pieces.append(data[:, HD * i : HD * i + HD] * factor * gain[i : i + 1, :])
-        nf[i] = pieces[i].astype(BF16)
-    normed_ffn = jnp.concatenate(pieces, axis=1).astype(BF16)
-
-    for d in (1, 3, 2):
-        theirs = pl.ds(pl.multiple_of(td[d] * 512, 512), 512)
-        send(ed_h.at[0, :, theirs], wd.at[t], ys.at[2, d], yr.at[2, d], (z, x, c, td[d]))
-    block = nf[pl.ds(4 * t, 4)].reshape(64, HD)
+    ld_own.wait()
+    residual = (tokb[...].astype(F32) + attention).astype(BF16)
+    res[t] = residual
+    for d in (2, 1, 3):
+        send(res.at[t], res.at[t], as2.at[d], ar2.at[d], (z, x, c, td[d]))
+
+    block = jnp.concatenate([residual[:, HD * j : HD * j + HD] for j in range(4)], axis=0)
     sbuf[...] = dot(dispatch, block).astype(BF16).reshape(3 * NE, 4, HD)
     order = (3, 4, 5, 6, 7, 0, 1, 2)
 
@@ -346,6 +336,26 @@
             remote(sbuf.at[three(p)], rbuf.at[to], as_.at[half_of(r)], ar.at[half_of(r)], dev).start()
     rbuf[three(8 * order.index(0) + m)] = sbuf[three(e)]
 
+    for d in (1, 3, 2):
+        theirs = pl.ds(pl.multiple_of(td[d] * 512, 512), 512)
+        send(ed_h.at[0, :, theirs], wd.at[t], ys.at[2, d], yr.at[2, d], (z, x, c, td[d]))
+
+    for d in (1, 3, 2):
+        arrived(res.at[td[NT - d]], as2.at[d], ar2.at[d])
+    for cp in ld_ffn:
+        cp.wait()
+    data = jnp.concatenate([res[i] for i in range(NT)], axis=1).astype(F32)
+    factor = lax.rsqrt(jnp.mean(data * data, axis=-1, keepdims=True) + EPS)
+    gain = fg[...].astype(F32)
+    pieces = [data[:, HD * i : HD * i + HD] * factor * gain[i : i + 1, :] for i in range(16)]
+    normed_ffn = jnp.concatenate(pieces, axis=1).astype(BF16)
+    own_gain = []
+    for j in range(4):
+        row = gain[j : j + 1, :]
+        for i in range(1, NT):
+            row = jnp.where(t == i, gain[4 * i + j : 4 * i + j + 1, :], row)
+        own_gain.append(row)
+    own_gain = jnp.concatenate(own_gain, axis=1)
     for cp in ld_sh:
         cp.wait()
     both = dot(normed_ffn, sgu[...])
@@ -389,16 +399,27 @@
             (z, x, 1 - c, t),
         )
         both.wait_recv()
-        rows_of = jnp.concatenate([to_rows(half, 0), to_rows(half, 1)], axis=0)
+        raw = jnp.concatenate([to_rows(half, 0), to_rows(half, 1)], axis=0).astype(F32)
+        rows_of = (raw * own_gain).astype(BF16)
+        square = jnp.sum(raw * raw, axis=-1, keepdims=True)
+        square = jnp.concatenate([square, jnp.zeros((32, 1), F32)], axis=0)
+        square = jnp.broadcast_to(square, (HD, HD)).T[0:8, :]
+        fs[half, 0] = square
         for d in (2, 1, 3):
             gs[half, d] = dot(rows_of, wgu[td[d]]).astype(BF16)
-            send(gs.at[half, d], gr.at[half, d], gss.at[half, d], gsr.at[half, d], (z, x, c, td[d]))
+            dev = (z, x, c, td[d])
+            send(fs.at[half, 0], fs.at[half, d], fss.at[half, d], fsr.at[half, d], dev)
+            send(gs.at[half, d], gr.at[half, d], gss.at[half, d], gsr.at[half, d], dev)
         return dot(rows_of, wgu[t]), both
 
     def middle_half(half, gate_up):
         for d in (2, 1, 3):
             arrived(gr.at[half, d], gss.at[half, d], gsr.at[half, d])
             gate_up = gate_up + gr[half, d].astype(F32)
+            arrived(fs.at[half, d], fss.at[half, d], fsr.at[half, d])
+        square = fs[half, 0] + fs[half, 1] + fs[half, 2] + fs[half, 3]
+        square = jnp.broadcast_to(square[0:1, :], (HD, HD)).T[0:96, 0:1]
+        gate_up = gate_up * lax.rsqrt(square / 2048.0 + EPS)
         gate = gate_up[:, 0:HD]
         hidden = gate / (1.0 + jnp.exp(-gate)) * gate_up[:, HD : 2 * HD]
         hs[half, t] = hidden.astype(BF16)
@@ -451,11 +472,12 @@
     for dx, dc in mates:
         src = kvp.at[lax.rem(x + NX - dx, NX) * NC + cd[dc]]
         arrived(src, kps.at[dx, dc], kpr.at[dx, dc])
-    fresh = kvp[0].astype(F32)
+    new = kvp[0].astype(F32)
     for i in range(1, 8):
-        fresh = fresh + kvp[i].astype(F32)
-    fk_o[...] = fresh[:, 0:HD].astype(BF16)
-    fv_o[...] = fresh[:, HD : 2 * HD].astype(BF16)
+        new = new + kvp[i].astype(F32)
+    fresh[0] = new[:, 0:HD].astype(BF16)
+    fresh[1] = new[:, HD : 2 * HD].astype(BF16)
+    stores = [load(fresh.at[0], fk_o), load(fresh.at[1], fv_o)]
     back = remote(
         obuf.at[pl.ds(0, 3 * NE - 3)], cbuf.at[pl.ds(0, 3 * NE - 3)], rs_, rr, (z, x, 1 - c, t)
     )
@@ -463,11 +485,14 @@
     came = cbuf[...].reshape(rows, HD)
     routed = dot(comb_hi, came) + dot(comb_lo, came)
     for j in range(4):
-        mixed_o[:, HD * j : HD * j + HD] = (
+        mixed[:, HD * j : HD * j + HD] = (
             base[:, HD * j : HD * j + HD] + routed[SEQ * j : SEQ * j + SEQ]
         ).astype(BF16)
+    stores.append(load(mixed, mixed_o))
     for cp in [*pending, sent0, sent1, back]:
         cp.wait_send()
+    for cp in stores:
+        cp.wait()
 
 
 def hand_over(a, b, c, a_o, b_o, c_o, sem):
@@ -485,8 +510,6 @@
     expert_routes, expert_gate, expert_up, expert_down, shared_gate, shared_up, shared_down,
 ):
     hbm = pl.BlockSpec(memory_space=pl.ANY)
-    vmem = pl.BlockSpec(memory_space=pltpu.VMEM)
-    smem = pl.BlockSpec(memory_space=pltpu.SMEM)
     v, dma = pltpu.VMEM, pltpu.SemaphoreType.DMA
     outs = pl.pallas_call(
         kernel,
@@ -495,8 +518,8 @@
             jax.ShapeDtypeStruct((SEQ, HD), BF16),
             jax.ShapeDtypeStruct((SEQ, HD), BF16),
         ),
-        in_specs=[smem if i == 10 else hbm for i in range(20)],
-        out_specs=(vmem, vmem, vmem),
+        in_specs=[hbm] * 20,
+        out_specs=(hbm,) * 3,
         scratch_shapes=[
             v((SEQ, 2048), BF16), v((16, HD), BF16), v((2, HD), BF16), v((16, HD), BF16),
             v((64, 2048), BF16), v((6, SEQ), jnp.int32), v((SEQ, 2, POS), F32),
@@ -508,18 +531,20 @@
             v((8, SEQ, 256), BF16), v((8, SEQ, 256), BF16),
             v((8, SEQ, 256), BF16), v((8, SEQ, 256), BF16),
             v((2 * SEQ, HD), F32), v((2 * SEQ, POS), F32), v((2 * SEQ, HD), jnp.int32),
-            v((SEQ, 256), F32), v((NT, SEQ, 2048), BF16), v((NT, SEQ, HD), F32),
-            v((16, SEQ, HD), BF16), v((NT, SEQ, 512), BF16),
+            v((SEQ, 256), F32), v((NT, SEQ, 512), BF16), v((NT, SEQ, 512), BF16),
+            v((NT, SEQ, HD), F32), v((2, NT, 8, HD), F32), v((NT, SEQ, 512), BF16),
             v((3 * NE, 4, HD), BF16), v((3 * NE, 4, HD), BF16),
             v((2, NT, 96, 256), BF16), v((2, NT, 96, 256), BF16), v((2, NT, 96, HD), BF16),
             v((3 * NE, 4, HD), BF16), v((3 * NE, 4, HD), BF16),
             v((NT, SEQ, 512), BF16), v((NT, SEQ, 512), BF16),
-            dma((24,)), dma((8,)),
+            pltpu.SMEM((SEQ,), jnp.int32), v((SEQ, 512), BF16), v((SEQ, 512), BF16),
+            v((2, SEQ, HD), BF16), dma((32,)), dma((8,)),
             *[dma((NZ,)) for _ in range(6)],
             dma((NZ, NX)), dma((NZ, NX)), dma((NZ,)), dma((NZ,)),
             *[dma((NX, NC)) for _ in range(6)],
             dma((3, 4)), dma((3, 4)), dma((2, 4)), dma((2, 4)), dma((2,)), dma((2,)),
             dma((2, 4)), dma((2, 4)), dma((2, 4)), dma((2, 4)), dma, dma, dma((4,)), dma((4,)),
+            dma((4,)), dma((4,)), dma((2, 4)), dma((2, 4)),
         ],
         compiler_params=pltpu.CompilerParams(
             collective_id=0, has_side_effects=True, vmem_limit_bytes=60 * 1024 * 1024

time: 66.4 us -> 61.6 us (0.928)
  Pallas kernels: 65.7 us -> 60.8 us
    pallas_call x1, Pallas kernels: 63.8 us -> 59 us  [body(): pl.pallas_call(kernel, out_shape=(jax.ShapeDtypeStruct((SEQ, 512), BF16),...]
where the time goes in v5:
time: 61.6 us; the launch traced here: 61.5 us
  Pallas kernels  60.8 us (99%)
  between operations  0.65 us (1%)
    pallas_call x1, Pallas kernels, body(): pl.pallas_call(kernel, out_shape=(jax.ShapeDtypeStruct((SEQ, 512), BF16),...  59 us
    pallas_call x1, Pallas kernels, body(): pl.pallas_call(hand_over, out_shape=tuple((jax.ShapeDtypeStruct(o.shape,...  1.87 us

profile of v5, /device:TPU:1, one launch (start us, length us, event | category | flops | bytes accessed | tf_op | source)
XLA Modules:
  0.0 61.5 jit_solution(1052193611244637746)
XLA Ops:
  0.6 59.0 %shard_map.211 = (bf16[16,512]{1,0:T(8,128)(2,1)}, bf16[16,128]{1,0:T(8,128)(2,1)}, bf16[16,128]{1,0:T(8,128)(2,1)}) custom-call(bf16[16,2048]{1,0:T(8,128)(2,1)} %tok_h.1, bf16[16,128]{1,0:T(8,128)(2,1)} %bitcast.10, bf16[32,256]{1,0:T(8,128)(2,1)} %wq_h.1, bf16[32,128]{1,0:T(8,128)(2,1)} %wk_h.1, bf16[32,128]{1,0:T(8,128)(2,1)} %wv_h.1, ...), custom_call_target="tpu_custom_call" | custom-call | tf_op jit(solution)/shard_map/pallas_call | solution.py:514
  59.6 1.9 %shard_map.212 = (bf16[16,512]{1,0:T(8,128)(2,1)}, bf16[16,128]{1,0:T(8,128)(2,1)}, bf16[16,128]{1,0:T(8,128)(2,1)}) custom-call(bf16[16,512]{1,0:T(8,128)(2,1)} %get-tuple-element.6.a, bf16[16,128]{1,0:T(8,128)(2,1)} %get-tuple-element.7.b, bf16[16,128]{1,0:T(8,128)(2,1)} %get-tuple-element.8.c), custom_call_target="tpu_custom_call" | custom-call | tf_op jit(solution)/shard_map/pallas_call | solution.py:559

commit v6 on v5

--- a/solution.py
+++ b/solution.py
@@ -39,7 +39,7 @@
     tok_h, ag_h, wq_h, wk_h, wv_h, wo_h, hg_h, pk_h, pv_h, off_h, lens_h, fg_h, rt_h, er_h,
     eg_h, eu_h, ed_h, sg_h, su_h, sd_h,
     mixed_o, fk_o, fv_o,
-    tok, ag, hg, fg, rt, er, off, kb, vb, qb, kvb, ob, wgu, wd, sgu, sd,
+    tok, ag, hg, fg, rt, er, off, kb, kt, vb, qb, kvb, ob, wgu, wd, sgu, sd,
     tkb, tk, part, qp, kvpart, kvp,
     qs, lg, lenb, ho, pcs, pc, sq, fs, res, sbuf, rbuf, gs, gr, hs, obuf, cbuf, ssb, ssr,
     lens, tokb, mixed, fresh, lsem, kvsem,
@@ -91,6 +91,73 @@
         load(wk_h, kvb.at[z, :, pl.ds(0, 128)]),
         load(wv_h, kvb.at[z, :, pl.ds(128, 128)]),
     ]
+    barrier = pltpu.get_barrier_semaphore()
+    first = [(zd[d], x, c, t) for d in range(1, NZ)]
+    first += [(z, xd[dx], cd[dc], t) for dx, dc in mates]
+    first += [(z, x, c, td[d]) for d in range(1, NT)]
+    for dev in first:
+        pl.semaphore_signal(barrier, inc=1, device_id=dev, device_id_type=MESH)
+
+    pl.semaphore_wait(barrier, len(first))
+
+    mine_o = ob.at[z, x, c]
+
+    def q_around(*steps):
+        for d in steps:
+            send(qb.at[z], qb.at[z], qzs.at[d], qzr.at[d], (zd[d], x, c, t))
+
+    def o_around(*steps):
+        for d in steps:
+            send(mine_o, mine_o, ozs.at[d], ozr.at[d], (zd[d], x, c, t))
+
+    ld_q.wait()
+    q_around(*far_first)
+
+    ld_o.wait()
+    for cp in ld_tok:
+        cp.wait()
+    data = tok[...].astype(F32)
+    factor = lax.rsqrt(jnp.mean(data * data, axis=-1, keepdims=True) + EPS)
+    gain = ag[...].astype(F32)
+    blocks = []
+    for i in range(NZ):
+        halves = []
+        for k in (2 * i, 2 * i + 1):
+            halves.append(data[:, HD * k : HD * k + HD] * factor * gain[k : k + 1, :])
+        blocks.append(jnp.concatenate(halves, axis=1).astype(BF16).astype(F32))
+    chunk = iota((SEQ, 256), 1) >> 5
+    for g in range(8):
+        own = blocks[g]
+        for k in range(1, 8):
+            j = (g + k) % 8
+            own = jnp.where(chunk == j, pltpu.roll(blocks[j], 32 * k, 1), own)
+        tkb[g] = own.astype(BF16)
+    for dx, dc in mates:
+        g = xd[dx] * NC + cd[dc]
+        send(tkb.at[g], tk.at[m], tks.at[dx, dc], tkr.at[dx, dc], (z, xd[dx], cd[dc], t))
+    tk[m] = tkb[m]
+
+    def o_along(r):
+        src = ob.at[zd[r], x, c]
+        for i in (2, 1, 3):
+            send(src, src, oxs.at[r, i], oxr.at[r, i], (z, xd[i], c, t))
+
+    def o_forward(r):
+        src = ob.at[zd[r], x, c]
+        arrived(src, ozs.at[NZ - r], ozr.at[NZ - r])
+        o_along(r)
+
+    def o_across(r):
+        for i in (1, 3, 2):
+            arrived(ob.at[zd[r], xd[i], c], oxs.at[r, NX - i], oxr.at[r, NX - i])
+        src = ob.at[zd[r], :, c]
+        send(src, src, ods.at[r], odr.at[r], (z, x, 1 - c, t))
+
+    def o_last():
+        for r in range(NZ):
+            arrived(ob.at[zd[r], :, 1 - c], ods.at[r], odr.at[r])
+
+    o_along(0)
     ld_er = load(er_h, er)
     ld_att = [load(off_h, off), load(hg_h, hg), load(lens_h, lens)]
     kv_loads = []
@@ -114,31 +181,20 @@
         load(ed_h.at[0, :, mine], wd.at[t]),
     ]
 
-    barrier = pltpu.get_barrier_semaphore()
-    first = [(zd[d], x, c, t) for d in range(1, NZ)]
-    first += [(z, xd[dx], cd[dc], t) for dx, dc in mates]
-    first += [(z, x, c, td[d]) for d in range(1, NT)]
-    for dev in first:
-        pl.semaphore_signal(barrier, inc=1, device_id=dev, device_id_type=MESH)
-
-    for cp in ld_tok:
-        cp.wait()
-    data = tok[...].astype(F32)
-    factor = lax.rsqrt(jnp.mean(data * data, axis=-1, keepdims=True) + EPS)
-    gain = ag[...].astype(F32)
-    blocks = []
-    for i in range(NZ):
-        halves = []
-        for k in (2 * i, 2 * i + 1):
-            halves.append(data[:, HD * k : HD * k + HD] * factor * gain[k : k + 1, :])
-        blocks.append(jnp.concatenate(halves, axis=1).astype(BF16).astype(F32))
-    chunk = iota((SEQ, 256), 1) >> 5
-    for g in range(8):
-        own = blocks[g]
-        for k in range(1, 8):
-            j = (g + k) % 8
-            own = jnp.where(chunk == j, pltpu.roll(blocks[j], 32 * k, 1), own)
-        tkb[g] = own.astype(BF16)
+    def recut_down(peers):
+        for d in peers:
+            theirs = pl.ds(pl.multiple_of(td[d] * 512, 512), 512)
+            send(ed_h.at[0, :, theirs], wd.at[t], ys.at[2, d], yr.at[2, d], (z, x, c, td[d]))
+
+    for d in (1, 3, 2):
+        p = td[d]
+        dev = (z, x, c, p)
+        theirs = pl.ds(pl.multiple_of(p * 512, 512), 512)
+        for k, src in enumerate((eg_h, eu_h)):
+            half = pl.ds(128 * k, 128)
+            send(src.at[0, theirs, :], wgu.at[t, :, half], ys.at[k, d], yr.at[k, d], dev)
+    recut_down((1, 3))
+
     ld_er.wait()
     rows = NE * 12
     chosen = iota((NE, SEQ), 0) == er[0:1, :]
@@ -160,55 +216,11 @@
     want = (q0 - 3 * e0 + 1).astype(F32)
     dispatch = ones_where((slot_of == want) & (j0 == (c0 >> 4)))
 
-    pl.semaphore_wait(barrier, len(first))
-
-    ld_q.wait()
-    for d in far_first:
-        send(qb.at[z], qb.at[z], qzs.at[d], qzr.at[d], (zd[d], x, c, t))
-
-    for dx, dc in mates:
-        g = xd[dx] * NC + cd[dc]
-        send(tkb.at[g], tk.at[m], tks.at[dx, dc], tkr.at[dx, dc], (z, xd[dx], cd[dc], t))
-    tk[m] = tkb[m]
-
-    ld_o.wait()
-    mine_o = ob.at[z, x, c]
-    for d in far_first:
-        send(mine_o, mine_o, ozs.at[d], ozr.at[d], (zd[d], x, c, t))
-
-    def o_along(r):
-        src = ob.at[zd[r], x, c]
-        for i in (2, 1, 3):
-            send(src, src, oxs.at[r, i], oxr.at[r, i], (z, xd[i], c, t))
-
-    def o_forward(r):
-        src = ob.at[zd[r], x, c]
-        arrived(src, ozs.at[NZ - r], ozr.at[NZ - r])
-        o_along(r)
-
-    def o_across(r):
-        for i in (1, 3, 2):
-            arrived(ob.at[zd[r], xd[i], c], oxs.at[r, NX - i], oxr.at[r, NX - i])
-        src = ob.at[zd[r], :, c]
-        send(src, src, ods.at[r], odr.at[r], (z, x, 1 - c, t))
-
-    def o_last():
-        for r in range(NZ):
-            arrived(ob.at[zd[r], :, 1 - c], ods.at[r], odr.at[r])
-
-    o_along(0)
-    for cp in ld_kv:
-        cp.wait()
-    for d in far_first:
-        send(kvb.at[z], kvb.at[z], kzs.at[d], kzr.at[d], (zd[d], x, c, t))
-
-    for d in (1, 3, 2):
-        p = td[d]
-        dev = (z, x, c, p)
-        theirs = pl.ds(pl.multiple_of(p * 512, 512), 512)
-        for k, src in enumerate((eg_h, eu_h)):
-            half = pl.ds(128 * k, 128)
-            send(src.at[0, theirs, :], wgu.at[t, :, half], ys.at[k, d], yr.at[k, d], dev)
+    o_around(1, 7, 4, 3, 5, 2, 6)
+    for b in range(SEQ):
+        if b % 4 == 0:
+            kv_loads[2 * (b // 4)].wait()
+        kt[b] = kb[b].T
 
     for dx, dc in mates:
         src = tk.at[lax.rem(x + NX - dx, NX) * NC + cd[dc]]
@@ -216,19 +228,21 @@
     for d in near_first:
         arrived(qb.at[lax.rem(z + NZ - d, NZ)], qzs.at[d], qzr.at[d])
     rows_in = tk[...].reshape(8 * SEQ, 256)
-    part[...] = dot(rows_in, qb[...].reshape(256, 256)).astype(BF16).reshape(8, SEQ, 256)
+    part[...] = dot(rows_in, qb[...].reshape(256, 256)).reshape(8, SEQ, 256)
     for dx, dc in mates:
         g = xd[dx] * NC + cd[dc]
         send(part.at[g], qp.at[m], qps.at[dx, dc], qpr.at[dx, dc], (z, xd[dx], cd[dc], t))
     qp[m] = part[m]
     for r in (7, 1, 6, 2, 5, 3, 4):
         o_forward(r)
+    for r in (0, 7, 1):
+        o_across(r)
     for dx, dc in mates:
         src = qp.at[lax.rem(x + NX - dx, NX) * NC + cd[dc]]
         arrived(src, qps.at[dx, dc], qpr.at[dx, dc])
-    total = qp[0].astype(F32)
+    total = qp[0]
     for i in range(1, 8):
-        total = total + qp[i].astype(F32)
+        total = total + qp[i]
     queries = total.astype(BF16).astype(F32)
 
     for h in range(2):
@@ -236,12 +250,14 @@
     for cp in ld_att:
         cp.wait()
     for b in range(SEQ):
-        if b % 4 == 0:
-            kv_loads[2 * (b // 4)].wait()
         q = qs[2 * b : 2 * b + 2, :].astype(BF16)
-        lg[2 * b : 2 * b + 2, :] = dot_nt(q, kb[b]) * HD ** (-0.5) + off[b]
+        lg[2 * b : 2 * b + 2, :] = dot(q, kt[b]) * HD ** (-0.5) + off[b]
         lenb[2 * b : 2 * b + 2, :] = jnp.full((2, HD), lens[b], jnp.int32)
-    for r in (0, 7, 1):
+    for cp in ld_kv:
+        cp.wait()
+    for d in far_first:
+        send(kvb.at[z], kvb.at[z], kzs.at[d], kzr.at[d], (zd[d], x, c, t))
+    for r in (6, 2):
         o_across(r)
     logits = lg[...]
     length = lenb[:, 0:1]
@@ -265,8 +281,6 @@
     after = jnp.concatenate(after, axis=1)
     sticks = jnp.where(usable, jnp.exp(jnp.minimum(logits, 0.0) - tail + after), 0.0)
     lg[...] = sticks
-    for r in (6, 2):
-        o_across(r)
     for b in range(SEQ):
         if b % 4 == 0:
             kv_loads[2 * (b // 4) + 1].wait()
@@ -291,13 +305,6 @@
         send(sq.at[t], sq.at[t], cs.at[0, d], cr.at[0, d], dev)
         send(pcs.at[td[d]], pc.at[t], cs.at[1, d], cr.at[1, d], dev)
     pc[t] = pcs[t]
-    for d in near_first:
-        arrived(kvb.at[lax.rem(z + NZ - d, NZ)], kzs.at[d], kzr.at[d])
-    kvpart[...] = dot(rows_in, kvb[...].reshape(256, 256)).astype(BF16).reshape(8, SEQ, 256)
-    for dx, dc in mates:
-        g = xd[dx] * NC + cd[dc]
-        send(kvpart.at[g], kvp.at[m], kps.at[dx, dc], kpr.at[dx, dc], (z, xd[dx], cd[dc], t))
-    kvp[m] = kvpart[m]
     for d in (1, 3, 2):
         src = td[NT - d]
         for k, buf in enumerate((sq, pc)):
@@ -336,9 +343,7 @@
             remote(sbuf.at[three(p)], rbuf.at[to], as_.at[half_of(r)], ar.at[half_of(r)], dev).start()
     rbuf[three(8 * order.index(0) + m)] = sbuf[three(e)]
 
-    for d in (1, 3, 2):
-        theirs = pl.ds(pl.multiple_of(td[d] * 512, 512), 512)
-        send(ed_h.at[0, :, theirs], wd.at[t], ys.at[2, d], yr.at[2, d], (z, x, c, td[d]))
+    recut_down((2,))
 
     for d in (1, 3, 2):
         arrived(res.at[td[NT - d]], as2.at[d], ar2.at[d])
@@ -386,6 +391,13 @@
     comb_hi = jnp.where(fits, dot(w_hi, spread_t), 0.0).astype(BF16)
     comb_lo = jnp.where(fits, dot(w_lo, spread_t), 0.0).astype(BF16)
 
+    for d in near_first:
+        arrived(kvb.at[lax.rem(z + NZ - d, NZ)], kzs.at[d], kzr.at[d])
+    kvpart[...] = dot(rows_in, kvb[...].reshape(256, 256)).astype(BF16).reshape(8, SEQ, 256)
+    for dx, dc in mates:
+        g = xd[dx] * NC + cd[dc]
+        send(kvpart.at[g], kvp.at[m], kps.at[dx, dc], kpr.at[dx, dc], (z, xd[dx], cd[dc], t))
+    kvp[m] = kvpart[m]
     def to_rows(half, g):
         group = rbuf[96 * half + 48 * g : 96 * half + 48 * g + 48].reshape(192, HD)
         p, q = iota((48, 192), 0), iota((48, 192), 1)
@@ -401,16 +413,19 @@
         both.wait_recv()
         raw = jnp.concatenate([to_rows(half, 0), to_rows(half, 1)], axis=0).astype(F32)
         rows_of = (raw * own_gain).astype(BF16)
+        for d in (2, 1, 3):
+            gs[half, d] = dot(rows_of, wgu[td[d]]).astype(BF16)
+        for d in (2, 1, 3):
+            dev = (z, x, c, td[d])
+            send(gs.at[half, d], gr.at[half, d], gss.at[half, d], gsr.at[half, d], dev)
+        gate_up = dot(rows_of, wgu[t])
         square = jnp.sum(raw * raw, axis=-1, keepdims=True)
         square = jnp.concatenate([square, jnp.zeros((32, 1), F32)], axis=0)
-        square = jnp.broadcast_to(square, (HD, HD)).T[0:8, :]
-        fs[half, 0] = square
+        fs[half, 0] = jnp.broadcast_to(square, (HD, HD)).T[0:8, :]
         for d in (2, 1, 3):
-            gs[half, d] = dot(rows_of, wgu[td[d]]).astype(BF16)
             dev = (z, x, c, td[d])
             send(fs.at[half, 0], fs.at[half, d], fss.at[half, d], fsr.at[half, d], dev)
-            send(gs.at[half, d], gr.at[half, d], gss.at[half, d], gsr.at[half, d], dev)
-        return dot(rows_of, wgu[t]), both
+        return gate_up, both
 
     def middle_half(half, gate_up):
         for d in (2, 1, 3):
@@ -495,13 +510,10 @@
         cp.wait()
 
 
-def hand_over(a, b, c, a_o, b_o, c_o, sem):
-    moves = []
-    for i, (src, dst) in enumerate(((a, a_o), (b, b_o), (c, c_o))):
-        moves.append(pltpu.make_async_copy(src, dst, sem.at[i]))
-        moves[i].start()
-    for cp in moves:
-        cp.wait()
+def hand_over(a, b, c, a_o, b_o, c_o):
+    a_o[...] = a[...]
+    b_o[...] = b[...]
+    c_o[...] = c[...]
 
 
 def body(
@@ -523,12 +535,12 @@
         scratch_shapes=[
             v((SEQ, 2048), BF16), v((16, HD), BF16), v((2, HD), BF16), v((16, HD), BF16),
             v((64, 2048), BF16), v((6, SEQ), jnp.int32), v((SEQ, 2, POS), F32),
-            v((SEQ, POS, HD), BF16), v((SEQ, POS, HD), BF16),
+            v((SEQ, POS, HD), BF16), v((SEQ, HD, POS), BF16), v((SEQ, POS, HD), BF16),
             v((NZ, 32, 256), BF16), v((NZ, 32, 256), BF16), v((NZ, NX, NC, 32, 256), BF16),
             v((NT, 512, 256), BF16), v((NT, 128, 512), BF16),
             v((2048, 256), BF16), v((128, 2048), BF16),
             v((8, SEQ, 256), BF16), v((8, SEQ, 256), BF16),
-            v((8, SEQ, 256), BF16), v((8, SEQ, 256), BF16),
+            v((8, SEQ, 256), F32), v((8, SEQ, 256), F32),
             v((8, SEQ, 256), BF16), v((8, SEQ, 256), BF16),
             v((2 * SEQ, HD), F32), v((2 * SEQ, POS), F32), v((2 * SEQ, HD), jnp.int32),
             v((SEQ, 256), F32), v((NT, SEQ, 512), BF16), v((NT, SEQ, 512), BF16),
@@ -559,9 +571,8 @@
     return pl.pallas_call(
         hand_over,
         out_shape=tuple(jax.ShapeDtypeStruct(o.shape, o.dtype) for o in outs),
-        in_specs=[hbm] * 3,
-        out_specs=(hbm,) * 3,
-        scratch_shapes=[dma((3,))],
+        in_specs=[pl.BlockSpec(memory_space=pltpu.VMEM)] * 3,
+        out_specs=(pl.BlockSpec(memory_space=pltpu.VMEM),) * 3,
     )(*outs)
 
 

time: 61.6 us -> 60.4 us (0.981)
  Pallas kernels: 60.8 us -> 59.7 us
    pallas_call x1, Pallas kernels: 59 us -> 58.3 us  [body(): pl.pallas_call(kernel, out_shape=(jax.ShapeDtypeStruct((SEQ, 512), BF16),...]
where the time goes in v6:
time: 60.4 us; the launch traced here: 60.3 us
  Pallas kernels  59.7 us (99%)
  between operations  0.65 us (1%)
    pallas_call x1, Pallas kernels, body(): pl.pallas_call(kernel, out_shape=(jax.ShapeDtypeStruct((SEQ, 512), BF16),...  58.3 us
    pallas_call x1, Pallas kernels, body(): pl.pallas_call(hand_over, out_shape=tuple((jax.ShapeDtypeStruct(o.shape,...  1.34 us

profile of v6, /device:TPU:1, one launch (start us, length us, event | category | flops | bytes accessed | tf_op | source)
XLA Modules:
  0.0 60.3 jit_solution(8700882478200360153)
XLA Ops:
  0.6 58.3 %shard_map.211 = (bf16[16,512]{1,0:T(8,128)(2,1)}, bf16[16,128]{1,0:T(8,128)(2,1)}, bf16[16,128]{1,0:T(8,128)(2,1)}) custom-call(bf16[16,2048]{1,0:T(8,128)(2,1)} %tok_h.1, bf16[16,128]{1,0:T(8,128)(2,1)} %bitcast.10, bf16[32,256]{1,0:T(8,128)(2,1)} %wq_h.1, bf16[32,128]{1,0:T(8,128)(2,1)} %wk_h.1, bf16[32,128]{1,0:T(8,128)(2,1)} %wv_h.1, ...), custom_call_target="tpu_custom_call" | custom-call | tf_op jit(solution)/shard_map/pallas_call | solution.py:526
  59.0 1.3 %shard_map.212 = (bf16[16,512]{1,0:T(8,128)(2,1)}, bf16[16,128]{1,0:T(8,128)(2,1)}, bf16[16,128]{1,0:T(8,128)(2,1)}) custom-call(bf16[16,512]{1,0:T(8,128)(2,1)} %get-tuple-element.6.a, bf16[16,128]{1,0:T(8,128)(2,1)} %get-tuple-element.7.b, bf16[16,128]{1,0:T(8,128)(2,1)} %get-tuple-element.8.c), custom_call_target="tpu_custom_call" | custom-call | tf_op jit(solution)/shard_map/pallas_call | solution.py:571

commit v7 on v6

--- a/solution.py
+++ b/solution.py
@@ -41,7 +41,8 @@
     mixed_o, fk_o, fv_o,
     tok, ag, hg, fg, rt, er, off, kb, kt, vb, qb, kvb, ob, wgu, wd, sgu, sd,
     tkb, tk, part, qp, kvpart, kvp,
-    qs, lg, lenb, ho, pcs, pc, sq, fs, res, sbuf, rbuf, gs, gr, hs, obuf, cbuf, ssb, ssr,
+    qs, lg, lenb, ho, pcs, pc, sq, fs, res, sbuf, rbuf, gs0, gs1, gs2, gr0, gr1, gr2, hs0, hs1, hs2,
+    pick72, back72, pick48, back48, obuf, cbuf, ssb, ssr,
     lens, tokb, mixed, fresh, lsem, kvsem,
     qzs, qzr, kzs, kzr, ozs, ozr, oxs, oxr, ods, odr, tks, tkr, qps, qpr, kps, kpr,
     ys, yr, cs, cr, as_, ar, gss, gsr, hss, hsr, rs_, rr, sss, ssrr, as2, ar2, fss, fsr,
@@ -217,6 +218,13 @@
     dispatch = ones_where((slot_of == want) & (j0 == (c0 >> 4)))
 
     o_around(1, 7, 4, 3, 5, 2, 6)
+    for n, pick, back in ((72, pick72, back72), (48, pick48, back48)):
+        for j in range(4):
+            p, q = iota((n, 4 * n), 0), iota((n, 4 * n), 1)
+            pick[n * j : n * j + n, :] = jnp.where(q == 4 * p + j, 1.0, 0.0)
+        p, q = iota((4 * n, 4 * n), 1), iota((4 * n, 4 * n), 0)
+        j = (p >= n).astype(jnp.int32) + (p >= 2 * n) + (p >= 3 * n)
+        back[...] = ones_where(q == 4 * (p - n * j) + j)
     for b in range(SEQ):
         if b % 4 == 0:
             kv_loads[2 * (b // 4)].wait()
@@ -323,37 +331,33 @@
 
     block = jnp.concatenate([residual[:, HD * j : HD * j + HD] for j in range(4)], axis=0)
     sbuf[...] = dot(dispatch, block).astype(BF16).reshape(3 * NE, 4, HD)
-    order = (3, 4, 5, 6, 7, 0, 1, 2)
+    order = (3, 4, 5, 2, 6, 7, 0, 1)
+    part_rows = (72, 48, 72)
+    first_row = (0, 72, 120)
 
     def three(i):
         return pl.ds(3 * i, 3)
 
-    def half_of(r):
-        return order.index(r) // 4
+    def part_of(r):
+        return (0, 0, 0, 1, 1, 2, 2, 2)[order.index(r)]
 
     def around(r):
         return [(0, 0), *mates] if r else mates
 
-    for r in (4, 5, 3, 6, 2, 7, 1, 0):
+    for r in (7, 1, 0, 4, 5, 3, 6, 2):
         d = (NZ - r) % NZ
         to = three(8 * order.index(r) + m)
         for dx, dc in around(r):
             p = (zd[d] * NX + xd[dx]) * NC + cd[dc]
             dev = (zd[d], xd[dx], cd[dc], t)
-            remote(sbuf.at[three(p)], rbuf.at[to], as_.at[half_of(r)], ar.at[half_of(r)], dev).start()
+            remote(sbuf.at[three(p)], rbuf.at[to], as_.at[part_of(r)], ar.at[part_of(r)], dev).start()
     rbuf[three(8 * order.index(0) + m)] = sbuf[three(e)]
 
     recut_down((2,))
 
-    for d in (1, 3, 2):
-        arrived(res.at[td[NT - d]], as2.at[d], ar2.at[d])
     for cp in ld_ffn:
         cp.wait()
-    data = jnp.concatenate([res[i] for i in range(NT)], axis=1).astype(F32)
-    factor = lax.rsqrt(jnp.mean(data * data, axis=-1, keepdims=True) + EPS)
     gain = fg[...].astype(F32)
-    pieces = [data[:, HD * i : HD * i + HD] * factor * gain[i : i + 1, :] for i in range(16)]
-    normed_ffn = jnp.concatenate(pieces, axis=1).astype(BF16)
     own_gain = []
     for j in range(4):
         row = gain[j : j + 1, :]
@@ -361,6 +365,78 @@
             row = jnp.where(t == i, gain[4 * i + j : 4 * i + j + 1, :], row)
         own_gain.append(row)
     own_gain = jnp.concatenate(own_gain, axis=1)
+
+    gs, gr, hs = (gs0, gs1, gs2), (gr0, gr1, gr2), (hs0, hs1, hs2)
+
+    def start_part(k):
+        n, at = part_rows[k], first_row[k]
+        pick = pick48 if n == 48 else pick72
+        remote_rows = n if k < 2 else n - 3
+        both = remote(
+            sbuf.at[pl.ds(0, remote_rows)], rbuf.at[pl.ds(0, remote_rows)], as_.at[k], ar.at[k],
+            (z, x, 1 - c, t),
+        )
+        both.wait_recv()
+        came = dot(pick[...].astype(BF16), rbuf[at : at + n].reshape(4 * n, HD))
+        raw = jnp.concatenate([came[n * j : n * j + n] for j in range(4)], axis=1)
+        rows_of = (raw * own_gain).astype(BF16)
+        for d in (2, 1, 3):
+            gs[k][d] = dot(rows_of, wgu[td[d]]).astype(BF16)
+        for d in (2, 1, 3):
+            send(gs[k].at[d], gr[k].at[d], gss.at[k, d], gsr.at[k, d], (z, x, c, td[d]))
+        gate_up = dot(rows_of, wgu[t])
+        square = jnp.sum(raw * raw, axis=-1, keepdims=True)
+        square = jnp.concatenate([square, jnp.zeros((HD - n, 1), F32)], axis=0)
+        fs[k, 0] = jnp.broadcast_to(square, (HD, HD)).T[0:8, :]
+        for d in (2, 1, 3):
+            send(fs.at[k, 0], fs.at[k, d], fss.at[k, d], fsr.at[k, d], (z, x, c, td[d]))
+        return gate_up, both
+
+    def middle_part(k, gate_up):
+        for d in (2, 1, 3):
+            arrived(gr[k].at[d], gss.at[k, d], gsr.at[k, d])
+            gate_up = gate_up + gr[k][d].astype(F32)
+            arrived(fs.at[k, d], fss.at[k, d], fsr.at[k, d])
+        square = fs[k, 0] + fs[k, 1] + fs[k, 2] + fs[k, 3]
+        square = jnp.broadcast_to(square[0:1, :], (HD, HD)).T[0 : part_rows[k], 0:1]
+        gate_up = gate_up * lax.rsqrt(square / 2048.0 + EPS)
+        gate = gate_up[:, 0:HD]
+        hidden = gate / (1.0 + jnp.exp(-gate)) * gate_up[:, HD : 2 * HD]
+        hs[k][t] = hidden.astype(BF16)
+        own = hs[k].at[t]
+        for d in (2, 1, 3):
+            send(own, own, hss.at[k, d], hsr.at[k, d], (z, x, c, td[d]))
+
+    def end_part(k):
+        n, at = part_rows[k], first_row[k]
+        back = back48 if n == 48 else back72
+        for d in (2, 1, 3):
+            arrived(hs[k].at[td[NT - d]], hss.at[k, d], hsr.at[k, d])
+        out = dot(hs[k][0], wd[0])
+        for i in range(1, NT):
+            out = out + dot(hs[k][i], wd[i])
+        out = jnp.concatenate([out[:, HD * j : HD * j + HD] for j in range(4)], axis=0)
+        obuf[at : at + n] = dot(back[...], out.astype(BF16)).astype(BF16).reshape(n, 4, HD)
+        for r in ((4, 5, 3), (6, 2), (7, 1, 0))[k]:
+            for dx, dc in around(r):
+                p = 8 * order.index(r) + xd[dx] * NC + cd[dc]
+                dev = (zd[r], xd[dx], cd[dc], t)
+                remote(obuf.at[three(p)], cbuf.at[three(e)], rs_, rr, dev).start()
+
+    for cp in ld_ex:
+        cp.wait()
+    for d in (1, 3, 2):
+        src = td[NT - d]
+        for k in range(2):
+            arrived(wgu.at[src, :, pl.ds(128 * k, 128)], ys.at[k, d], yr.at[k, d])
+    gate_up2, sent2 = start_part(2)
+
+    for d in (1, 3, 2):
+        arrived(res.at[td[NT - d]], as2.at[d], ar2.at[d])
+    data = jnp.concatenate([res[i] for i in range(NT)], axis=1).astype(F32)
+    factor = lax.rsqrt(jnp.mean(data * data, axis=-1, keepdims=True) + EPS)
+    pieces = [data[:, HD * i : HD * i + HD] * factor * gain[i : i + 1, :] for i in range(16)]
+    normed_ffn = jnp.concatenate(pieces, axis=1).astype(BF16)
     for cp in ld_sh:
         cp.wait()
     both = dot(normed_ffn, sgu[...])
@@ -398,85 +474,16 @@
         g = xd[dx] * NC + cd[dc]
         send(kvpart.at[g], kvp.at[m], kps.at[dx, dc], kpr.at[dx, dc], (z, xd[dx], cd[dc], t))
     kvp[m] = kvpart[m]
-    def to_rows(half, g):
-        group = rbuf[96 * half + 48 * g : 96 * half + 48 * g + 48].reshape(192, HD)
-        p, q = iota((48, 192), 0), iota((48, 192), 1)
-        cols = [dot(ones_where(q == 4 * p + j), group).astype(BF16) for j in range(4)]
-        return jnp.concatenate(cols, axis=1)
-
-    def start_half(half):
-        n = 96 if half == 0 else 93
-        both = remote(
-            sbuf.at[pl.ds(0, n)], rbuf.at[pl.ds(0, n)], as_.at[half], ar.at[half],
-            (z, x, 1 - c, t),
-        )
-        both.wait_recv()
-        raw = jnp.concatenate([to_rows(half, 0), to_rows(half, 1)], axis=0).astype(F32)
-        rows_of = (raw * own_gain).astype(BF16)
-        for d in (2, 1, 3):
-            gs[half, d] = dot(rows_of, wgu[td[d]]).astype(BF16)
-        for d in (2, 1, 3):
-            dev = (z, x, c, td[d])
-            send(gs.at[half, d], gr.at[half, d], gss.at[half, d], gsr.at[half, d], dev)
-        gate_up = dot(rows_of, wgu[t])
-        square = jnp.sum(raw * raw, axis=-1, keepdims=True)
-        square = jnp.concatenate([square, jnp.zeros((32, 1), F32)], axis=0)
-        fs[half, 0] = jnp.broadcast_to(square, (HD, HD)).T[0:8, :]
-        for d in (2, 1, 3):
-            dev = (z, x, c, td[d])
-            send(fs.at[half, 0], fs.at[half, d], fss.at[half, d], fsr.at[half, d], dev)
-        return gate_up, both
-
-    def middle_half(half, gate_up):
-        for d in (2, 1, 3):
-            arrived(gr.at[half, d], gss.at[half, d], gsr.at[half, d])
-            gate_up = gate_up + gr[half, d].astype(F32)
-            arrived(fs.at[half, d], fss.at[half, d], fsr.at[half, d])
-        square = fs[half, 0] + fs[half, 1] + fs[half, 2] + fs[half, 3]
-        square = jnp.broadcast_to(square[0:1, :], (HD, HD)).T[0:96, 0:1]
-        gate_up = gate_up * lax.rsqrt(square / 2048.0 + EPS)
-        gate = gate_up[:, 0:HD]
-        hidden = gate / (1.0 + jnp.exp(-gate)) * gate_up[:, HD : 2 * HD]
-        hs[half, t] = hidden.astype(BF16)
-        for d in (2, 1, 3):
-            own = hs.at[half, t]
-            send(own, own, hss.at[half, d], hsr.at[half, d], (z, x, c, td[d]))
-
-    def end_half(half):
-        for d in (2, 1, 3):
-            arrived(hs.at[half, td[NT - d]], hss.at[half, d], hsr.at[half, d])
-        out = dot(hs[half, 0], wd[0])
-        for i in range(1, NT):
-            out = out + dot(hs[half, i], wd[i])
-        out = out.astype(BF16)
-        p, q = iota((192, 48), 1), iota((192, 48), 0)
-        for g in range(2):
-            back = jnp.zeros((192, HD), F32)
-            for j in range(4):
-                block = out[48 * g : 48 * g + 48, HD * j : HD * j + HD]
-                back = back + dot(ones_where(q == 4 * p + j), block)
-            at = 96 * half + 48 * g
-            obuf[at : at + 48] = back.astype(BF16).reshape(48, 4, HD)
-        for r in ((4, 5, 3, 6) if half == 0 else (2, 7, 1, 0)):
-            for dx, dc in around(r):
-                p = 8 * order.index(r) + xd[dx] * NC + cd[dc]
-                dev = (zd[r], xd[dx], cd[dc], t)
-                remote(obuf.at[three(p)], cbuf.at[three(e)], rs_, rr, dev).start()
-
-    for cp in ld_ex:
-        cp.wait()
-    for d in (1, 3, 2):
-        src = td[NT - d]
-        for k in range(2):
-            arrived(wgu.at[src, :, pl.ds(128 * k, 128)], ys.at[k, d], yr.at[k, d])
-    gate_up0, sent0 = start_half(0)
-    gate_up1, sent1 = start_half(1)
-    middle_half(0, gate_up0)
-    middle_half(1, gate_up1)
+    gate_up0, sent0 = start_part(0)
+    gate_up1, sent1 = start_part(1)
+    middle_part(2, gate_up2)
+    middle_part(0, gate_up0)
+    middle_part(1, gate_up1)
     for d in (1, 3, 2):
         arrived(wd.at[td[NT - d]], ys.at[2, d], yr.at[2, d])
-    end_half(0)
-    end_half(1)
+    end_part(0)
+    end_part(2)
+    end_part(1)
     cbuf[three(e)] = obuf[three(8 * order.index(0) + m)]
     shared_total = jnp.zeros((SEQ, 512), F32)
     for d in (2, 1, 3):
@@ -504,7 +511,7 @@
             base[:, HD * j : HD * j + HD] + routed[SEQ * j : SEQ * j + SEQ]
         ).astype(BF16)
     stores.append(load(mixed, mixed_o))
-    for cp in [*pending, sent0, sent1, back]:
+    for cp in [*pending, sent0, sent1, sent2, back]:
         cp.wait_send()
     for cp in stores:
         cp.wait()
@@ -544,9 +551,12 @@
             v((8, SEQ, 256), BF16), v((8, SEQ, 256), BF16),
             v((2 * SEQ, HD), F32), v((2 * SEQ, POS), F32), v((2 * SEQ, HD), jnp.int32),
             v((SEQ, 256), F32), v((NT, SEQ, 512), BF16), v((NT, SEQ, 512), BF16),
-            v((NT, SEQ, HD), F32), v((2, NT, 8, HD), F32), v((NT, SEQ, 512), BF16),
+            v((NT, SEQ, HD), F32), v((3, NT, 8, HD), F32), v((NT, SEQ, 512), BF16),
             v((3 * NE, 4, HD), BF16), v((3 * NE, 4, HD), BF16),
-            v((2, NT, 96, 256), BF16), v((2, NT, 96, 256), BF16), v((2, NT, 96, HD), BF16),
+            *[v((NT, n, 256), BF16) for _ in range(2) for n in (72, 48, 72)],
+            *[v((NT, n, HD), BF16) for n in (72, 48, 72)],
+            v((288, 288), F32), v((288, 288), BF16), v((192, 192), F32), v((192, 192), BF16),
+
             v((3 * NE, 4, HD), BF16), v((3 * NE, 4, HD), BF16),
             v((NT, SEQ, 512), BF16), v((NT, SEQ, 512), BF16),
             pltpu.SMEM((SEQ,), jnp.int32), v((SEQ, 512), BF16), v((SEQ, 512), BF16),
@@ -554,9 +564,9 @@
             *[dma((NZ,)) for _ in range(6)],
             dma((NZ, NX)), dma((NZ, NX)), dma((NZ,)), dma((NZ,)),
             *[dma((NX, NC)) for _ in range(6)],
-            dma((3, 4)), dma((3, 4)), dma((2, 4)), dma((2, 4)), dma((2,)), dma((2,)),
-            dma((2, 4)), dma((2, 4)), dma((2, 4)), dma((2, 4)), dma, dma, dma((4,)), dma((4,)),
-            dma((4,)), dma((4,)), dma((2, 4)), dma((2, 4)),
+            dma((3, 4)), dma((3, 4)), dma((2, 4)), dma((2, 4)), dma((3,)), dma((3,)),
+            dma((3, 4)), dma((3, 4)), dma((3, 4)), dma((3, 4)), dma, dma, dma((4,)), dma((4,)),
+            dma((4,)), dma((4,)), dma((3, 4)), dma((3, 4)),
         ],
         compiler_params=pltpu.CompilerParams(
             collective_id=0, has_side_effects=True, vmem_limit_bytes=60 * 1024 * 1024

time: 60.4 us -> 59.8 us (0.990)
  no operation moved by 1% of the time
where the time goes in v7:
time: 59.8 us; the launch traced here: 59.7 us
  Pallas kernels  59.1 us (99%)
  between operations  0.65 us (1%)
    pallas_call x1, Pallas kernels, body(): pl.pallas_call(kernel, out_shape=(jax.ShapeDtypeStruct((SEQ, 512), BF16),...  57.7 us
    pallas_call x1, Pallas kernels, body(): pl.pallas_call(hand_over, out_shape=tuple((jax.ShapeDtypeStruct(o.shape,...  1.34 us

profile of v7, /device:TPU:1, one launch (start us, length us, event | category | flops | bytes accessed | tf_op | source)
XLA Modules:
  0.0 59.7 jit_solution(11131031679019389167)
XLA Ops:
  0.6 57.7 %shard_map.211 = (bf16[16,512]{1,0:T(8,128)(2,1)}, bf16[16,128]{1,0:T(8,128)(2,1)}, bf16[16,128]{1,0:T(8,128)(2,1)}) custom-call(bf16[16,2048]{1,0:T(8,128)(2,1)} %tok_h.1, bf16[16,128]{1,0:T(8,128)(2,1)} %bitcast.10, bf16[32,256]{1,0:T(8,128)(2,1)} %wq_h.1, bf16[32,128]{1,0:T(8,128)(2,1)} %wk_h.1, bf16[32,128]{1,0:T(8,128)(2,1)} %wv_h.1, ...), custom_call_target="tpu_custom_call" | custom-call | tf_op jit(solution)/shard_map/pallas_call | solution.py:533
  58.4 1.3 %shard_map.212 = (bf16[16,512]{1,0:T(8,128)(2,1)}, bf16[16,128]{1,0:T(8,128)(2,1)}, bf16[16,128]{1,0:T(8,128)(2,1)}) custom-call(bf16[16,512]{1,0:T(8,128)(2,1)} %get-tuple-element.6.a, bf16[16,128]{1,0:T(8,128)(2,1)} %get-tuple-element.7.b, bf16[16,128]{1,0:T(8,128)(2,1)} %get-tuple-element.8.c), custom_call_target="tpu_custom_call" | custom-call | tf_op jit(solution)/shard_map/pallas_call | solution.py:581

commit v8 on v7

--- a/solution.py
+++ b/solution.py
@@ -43,7 +43,7 @@
     tkb, tk, part, qp, kvpart, kvp,
     qs, lg, lenb, ho, pcs, pc, sq, fs, res, sbuf, rbuf, gs0, gs1, gs2, gr0, gr1, gr2, hs0, hs1, hs2,
     pick72, back72, pick48, back48, obuf, cbuf, ssb, ssr,
-    lens, tokb, mixed, fresh, lsem, kvsem,
+    lens, tokb, lsem, kvsem,
     qzs, qzr, kzs, kzr, ozs, ozr, oxs, oxr, ods, odr, tks, tkr, qps, qpr, kps, kpr,
     ys, yr, cs, cr, as_, ar, gss, gsr, hss, hsr, rs_, rr, sss, ssrr, as2, ar2, fss, fsr,
 ):
@@ -243,8 +243,6 @@
     qp[m] = part[m]
     for r in (7, 1, 6, 2, 5, 3, 4):
         o_forward(r)
-    for r in (0, 7, 1):
-        o_across(r)
     for dx, dc in mates:
         src = qp.at[lax.rem(x + NX - dx, NX) * NC + cd[dc]]
         arrived(src, qps.at[dx, dc], qpr.at[dx, dc])
@@ -265,7 +263,7 @@
         cp.wait()
     for d in far_first:
         send(kvb.at[z], kvb.at[z], kzs.at[d], kzr.at[d], (zd[d], x, c, t))
-    for r in (6, 2):
+    for r in (0, 7, 1, 6, 2):
         o_across(r)
     logits = lg[...]
     length = lenb[:, 0:1]
@@ -497,9 +495,8 @@
     new = kvp[0].astype(F32)
     for i in range(1, 8):
         new = new + kvp[i].astype(F32)
-    fresh[0] = new[:, 0:HD].astype(BF16)
-    fresh[1] = new[:, HD : 2 * HD].astype(BF16)
-    stores = [load(fresh.at[0], fk_o), load(fresh.at[1], fv_o)]
+    fk_o[...] = new[:, 0:HD].astype(BF16)
+    fv_o[...] = new[:, HD : 2 * HD].astype(BF16)
     back = remote(
         obuf.at[pl.ds(0, 3 * NE - 3)], cbuf.at[pl.ds(0, 3 * NE - 3)], rs_, rr, (z, x, 1 - c, t)
     )
@@ -507,20 +504,20 @@
     came = cbuf[...].reshape(rows, HD)
     routed = dot(comb_hi, came) + dot(comb_lo, came)
     for j in range(4):
-        mixed[:, HD * j : HD * j + HD] = (
+        mixed_o[:, HD * j : HD * j + HD] = (
             base[:, HD * j : HD * j + HD] + routed[SEQ * j : SEQ * j + SEQ]
         ).astype(BF16)
-    stores.append(load(mixed, mixed_o))
     for cp in [*pending, sent0, sent1, sent2, back]:
         cp.wait_send()
-    for cp in stores:
+
+
+def hand_over(a, b, c, a_o, b_o, c_o, sem):
+    moves = []
+    for i, (src, dst) in enumerate(((a, a_o), (b, b_o), (c, c_o))):
+        moves.append(pltpu.make_async_copy(src, dst, sem.at[i]))
+        moves[i].start()
+    for cp in moves:
         cp.wait()
-
-
-def hand_over(a, b, c, a_o, b_o, c_o):
-    a_o[...] = a[...]
-    b_o[...] = b[...]
-    c_o[...] = c[...]
 
 
 def body(
@@ -532,13 +529,9 @@
     v, dma = pltpu.VMEM, pltpu.SemaphoreType.DMA
     outs = pl.pallas_call(
         kernel,
-        out_shape=(
-            jax.ShapeDtypeStruct((SEQ, 512), BF16),
-            jax.ShapeDtypeStruct((SEQ, HD), BF16),
-            jax.ShapeDtypeStruct((SEQ, HD), BF16),
-        ),
+        out_shape=(v((SEQ, 512), BF16), v((SEQ, HD), BF16), v((SEQ, HD), BF16)),
         in_specs=[hbm] * 20,
-        out_specs=(hbm,) * 3,
+        out_specs=(pl.BlockSpec(memory_space=pltpu.VMEM),) * 3,
         scratch_shapes=[
             v((SEQ, 2048), BF16), v((16, HD), BF16), v((2, HD), BF16), v((16, HD), BF16),
             v((64, 2048), BF16), v((6, SEQ), jnp.int32), v((SEQ, 2, POS), F32),
@@ -559,8 +552,7 @@
 
             v((3 * NE, 4, HD), BF16), v((3 * NE, 4, HD), BF16),
             v((NT, SEQ, 512), BF16), v((NT, SEQ, 512), BF16),
-            pltpu.SMEM((SEQ,), jnp.int32), v((SEQ, 512), BF16), v((SEQ, 512), BF16),
-            v((2, SEQ, HD), BF16), dma((32,)), dma((8,)),
+            pltpu.SMEM((SEQ,), jnp.int32), v((SEQ, 512), BF16), dma((32,)), dma((8,)),
             *[dma((NZ,)) for _ in range(6)],
             dma((NZ, NX)), dma((NZ, NX)), dma((NZ,)), dma((NZ,)),
             *[dma((NX, NC)) for _ in range(6)],
@@ -582,8 +574,9 @@
         hand_over,
         out_shape=tuple(jax.ShapeDtypeStruct(o.shape, o.dtype) for o in outs),
         in_specs=[pl.BlockSpec(memory_space=pltpu.VMEM)] * 3,
-        out_specs=(pl.BlockSpec(memory_space=pltpu.VMEM),) * 3,
-    )(*outs)
+        out_specs=(hbm,) * 3,
+        scratch_shapes=[dma((3,))],
+    )(*[pltpu.with_memory_space_constraint(o, pltpu.VMEM) for o in outs])
 
 
 def solution(mesh):

time: 59.8 us -> 58.7 us (0.982)
  Pallas kernels: 59.1 us -> 58 us
    pallas_call x1, Pallas kernels: 1.34 us -> 0.64 us  [body(): pl.pallas_call(hand_over, out_shape=tuple((jax.ShapeDtypeStruct(o.shape,...]
where the time goes in v8:
time: 58.7 us; the launch traced here: 58.6 us
  Pallas kernels  58 us (99%)
  between operations  0.65 us (1%)
    pallas_call x1, Pallas kernels, body(): pl.pallas_call(kernel, out_shape=(v((SEQ, 512), BF16), v((SEQ, HD), BF16)...  57.3 us

profile of v8, /device:TPU:1, one launch (start us, length us, event | category | flops | bytes accessed | tf_op | source)
XLA Modules:
  0.0 58.6 jit_solution(15008992636587702635)
XLA Ops:
  0.6 57.3 %shard_map.211 = (bf16[16,512]{1,0:T(8,128)(2,1)S(1)}, bf16[16,128]{1,0:T(8,128)(2,1)S(1)}, bf16[16,128]{1,0:T(8,128)(2,1)S(1)}) custom-call(bf16[16,2048]{1,0:T(8,128)(2,1)} %tok_h.1, bf16[16,128]{1,0:T(8,128)(2,1)} %bitcast.10, bf16[32,256]{1,0:T(8,128)(2,1)} %wq_h.1, bf16[32,128]{1,0:T(8,128)(2,1)} %wk_h.1, bf16[32,128]{1,0:T(8,128)(2,1)} %wv_h.1, ...), custom_call_target="tpu_custom_call" | custom-call | tf_op jit(solution)/shard_map/pallas_call | solution.py:530
  58.0 0.6 %shard_map.212 = (bf16[16,512]{1,0:T(8,128)(2,1)}, bf16[16,128]{1,0:T(8,128)(2,1)}, bf16[16,128]{1,0:T(8,128)(2,1)}) custom-call(bf16[16,512]{1,0:T(8,128)(2,1)S(1)} %get-tuple-element.6.a, bf16[16,128]{1,0:T(8,128)(2,1)S(1)} %get-tuple-element.7.b, bf16[16,128]{1,0:T(8,128)(2,1)S(1)} %get-tuple-element.8.c), custom_call_target="tpu_custom_call" | custom-call | tf_op jit(solution)/shard_map/pallas_call | solution.py:573

commit v9 on v8

--- a/solution.py
+++ b/solution.py
@@ -111,10 +111,11 @@
         for d in steps:
             send(mine_o, mine_o, ozs.at[d], ozr.at[d], (zd[d], x, c, t))
 
+    ld_o.wait()
+    o_around(*(1, 7, 2, 6))
     ld_q.wait()
     q_around(*far_first)
 
-    ld_o.wait()
     for cp in ld_tok:
         cp.wait()
     data = tok[...].astype(F32)
@@ -217,7 +218,7 @@
     want = (q0 - 3 * e0 + 1).astype(F32)
     dispatch = ones_where((slot_of == want) & (j0 == (c0 >> 4)))
 
-    o_around(1, 7, 4, 3, 5, 2, 6)
+    o_around(*(4, 3, 5))
     for n, pick, back in ((72, pick72, back72), (48, pick48, back48)):
         for j in range(4):
             p, q = iota((n, 4 * n), 0), iota((n, 4 * n), 1)
@@ -229,6 +230,10 @@
         if b % 4 == 0:
             kv_loads[2 * (b // 4)].wait()
         kt[b] = kb[b].T
+    o_forward(7)
+    o_forward(1)
+    o_forward(6)
+    o_forward(2)
 
     for dx, dc in mates:
         src = tk.at[lax.rem(x + NX - dx, NX) * NC + cd[dc]]
@@ -241,7 +246,7 @@
         g = xd[dx] * NC + cd[dc]
         send(part.at[g], qp.at[m], qps.at[dx, dc], qpr.at[dx, dc], (z, xd[dx], cd[dc], t))
     qp[m] = part[m]
-    for r in (7, 1, 6, 2, 5, 3, 4):
+    for r in (5, 3, 4):
         o_forward(r)
     for dx, dc in mates:
         src = qp.at[lax.rem(x + NX - dx, NX) * NC + cd[dc]]
@@ -287,14 +292,14 @@
     after = jnp.concatenate(after, axis=1)
     sticks = jnp.where(usable, jnp.exp(jnp.minimum(logits, 0.0) - tail + after), 0.0)
     lg[...] = sticks
+    for r in (5, 3, 4):
+        o_across(r)
     for b in range(SEQ):
         if b % 4 == 0:
             kv_loads[2 * (b // 4) + 1].wait()
         got = dot(lg[2 * b : 2 * b + 2, :].astype(BF16), vb[b])
         ho[b : b + 1, 0:HD] = got[0:1, :]
         ho[b : b + 1, HD : 2 * HD] = got[1:2, :]
-    for r in (5, 3, 4):
-        o_across(r)
     heads_out = ho[...]
     scaled = jnp.concatenate(
         [heads_out[:, HD * i : HD * i + HD] * hg[i : i + 1, :].astype(F32) for i in range(2)],

time: 58.7 us -> 57.6 us (0.981)
  Pallas kernels: 58 us -> 56.9 us
    pallas_call x1, Pallas kernels: 57.3 us -> 56.3 us  [body(): pl.pallas_call(kernel, out_shape=(v((SEQ, 512), BF16), v((SEQ, HD), BF16)...]
where the time goes in v9:
time: 57.6 us
  Pallas kernels  56.9 us (99%)
  between operations  0.65 us (1%)
    pallas_call x1, Pallas kernels, body(): pl.pallas_call(kernel, out_shape=(v((SEQ, 512), BF16), v((SEQ, HD), BF16)...  56.3 us

profile of v9, /device:TPU:1, one launch (start us, length us, event | category | flops | bytes accessed | tf_op | source)
XLA Modules:
  0.0 57.6 jit_solution(15455340839376477860)
XLA Ops:
  0.6 56.3 %shard_map.211 = (bf16[16,512]{1,0:T(8,128)(2,1)S(1)}, bf16[16,128]{1,0:T(8,128)(2,1)S(1)}, bf16[16,128]{1,0:T(8,128)(2,1)S(1)}) custom-call(bf16[16,2048]{1,0:T(8,128)(2,1)} %tok_h.1, bf16[16,128]{1,0:T(8,128)(2,1)} %bitcast.10, bf16[32,256]{1,0:T(8,128)(2,1)} %wq_h.1, bf16[32,128]{1,0:T(8,128)(2,1)} %wk_h.1, bf16[32,128]{1,0:T(8,128)(2,1)} %wv_h.1, ...), custom_call_target="tpu_custom_call" | custom-call | tf_op jit(solution)/shard_map/pallas_call | solution.py:535
  56.9 0.6 %shard_map.212 = (bf16[16,512]{1,0:T(8,128)(2,1)}, bf16[16,128]{1,0:T(8,128)(2,1)}, bf16[16,128]{1,0:T(8,128)(2,1)}) custom-call(bf16[16,512]{1,0:T(8,128)(2,1)S(1)} %get-tuple-element.6.a, bf16[16,128]{1,0:T(8,128)(2,1)S(1)} %get-tuple-element.7.b, bf16[16,128]{1,0:T(8,128)(2,1)S(1)} %get-tuple-element.8.c), custom_call_target="tpu_custom_call" | custom-call | tf_op jit(solution)/shard_map/pallas_call | solution.py:578

commit v10 on v9

--- a/solution.py
+++ b/solution.py
@@ -141,7 +141,7 @@
 
     def o_along(r):
         src = ob.at[zd[r], x, c]
-        for i in (2, 1, 3):
+        for i in (1, 3, 2):
             send(src, src, oxs.at[r, i], oxr.at[r, i], (z, xd[i], c, t))
 
     def o_forward(r):
@@ -347,7 +347,7 @@
     def around(r):
         return [(0, 0), *mates] if r else mates
 
-    for r in (7, 1, 0, 4, 5, 3, 6, 2):
+    for r in (4, 7, 1, 0, 5, 3, 6, 2):
         d = (NZ - r) % NZ
         to = three(8 * order.index(r) + m)
         for dx, dc in around(r):

time: 57.6 us -> 57.5 us (level)
  no operation moved by 1% of the time
where the time goes in v10:
time: 57.5 us; the launch traced here: 57.4 us
  Pallas kernels  56.8 us (99%)
  between operations  0.65 us (1%)
    pallas_call x1, Pallas kernels, body(): pl.pallas_call(kernel, out_shape=(v((SEQ, 512), BF16), v((SEQ, HD), BF16)...  56.1 us

profile of v10, /device:TPU:1, one launch (start us, length us, event | category | flops | bytes accessed | tf_op | source)
XLA Modules:
  0.0 57.4 jit_solution(9879830776589292609)
XLA Ops:
  0.6 56.1 %shard_map.211 = (bf16[16,512]{1,0:T(8,128)(2,1)S(1)}, bf16[16,128]{1,0:T(8,128)(2,1)S(1)}, bf16[16,128]{1,0:T(8,128)(2,1)S(1)}) custom-call(bf16[16,2048]{1,0:T(8,128)(2,1)} %tok_h.1, bf16[16,128]{1,0:T(8,128)(2,1)} %bitcast.10, bf16[32,256]{1,0:T(8,128)(2,1)} %wq_h.1, bf16[32,128]{1,0:T(8,128)(2,1)} %wk_h.1, bf16[32,128]{1,0:T(8,128)(2,1)} %wv_h.1, ...), custom_call_target="tpu_custom_call" | custom-call | tf_op jit(solution)/shard_map/pallas_call | solution.py:535
  56.8 0.6 %shard_map.212 = (bf16[16,512]{1,0:T(8,128)(2,1)}, bf16[16,128]{1,0:T(8,128)(2,1)}, bf16[16,128]{1,0:T(8,128)(2,1)}) custom-call(bf16[16,512]{1,0:T(8,128)(2,1)S(1)} %get-tuple-element.6.a, bf16[16,128]{1,0:T(8,128)(2,1)S(1)} %get-tuple-element.7.b, bf16[16,128]{1,0:T(8,128)(2,1)S(1)} %get-tuple-element.8.c), custom_call_target="tpu_custom_call" | custom-call | tf_op jit(solution)/shard_map/pallas_call | solution.py:578

commit v11 on v10

--- a/solution.py
+++ b/solution.py
@@ -139,6 +139,8 @@
         send(tkb.at[g], tk.at[m], tks.at[dx, dc], tkr.at[dx, dc], (z, xd[dx], cd[dc], t))
     tk[m] = tkb[m]
 
+    o_around(4, 3, 5)
+
     def o_along(r):
         src = ob.at[zd[r], x, c]
         for i in (1, 3, 2):
@@ -218,7 +220,6 @@
     want = (q0 - 3 * e0 + 1).astype(F32)
     dispatch = ones_where((slot_of == want) & (j0 == (c0 >> 4)))
 
-    o_around(*(4, 3, 5))
     for n, pick, back in ((72, pick72, back72), (48, pick48, back48)):
         for j in range(4):
             p, q = iota((n, 4 * n), 0), iota((n, 4 * n), 1)

time: 57.5 us -> 57.4 us (level)
  no operation moved by 1% of the time
where the time goes in v11:
time: 57.4 us; the launch traced here: 57.3 us
  Pallas kernels  56.7 us (99%)
  between operations  0.65 us (1%)
    pallas_call x1, Pallas kernels, body(): pl.pallas_call(kernel, out_shape=(v((SEQ, 512), BF16), v((SEQ, HD), BF16)...  56 us

profile of v11, /device:TPU:1, one launch (start us, length us, event | category | flops | bytes accessed | tf_op | source)
XLA Modules:
  0.0 57.3 jit_solution(1454662293339610106)
XLA Ops:
  0.6 56.0 %shard_map.211 = (bf16[16,512]{1,0:T(8,128)(2,1)S(1)}, bf16[16,128]{1,0:T(8,128)(2,1)S(1)}, bf16[16,128]{1,0:T(8,128)(2,1)S(1)}) custom-call(bf16[16,2048]{1,0:T(8,128)(2,1)} %tok_h.1, bf16[16,128]{1,0:T(8,128)(2,1)} %bitcast.10, bf16[32,256]{1,0:T(8,128)(2,1)} %wq_h.1, bf16[32,128]{1,0:T(8,128)(2,1)} %wk_h.1, bf16[32,128]{1,0:T(8,128)(2,1)} %wv_h.1, ...), custom_call_target="tpu_custom_call" | custom-call | tf_op jit(solution)/shard_map/pallas_call | solution.py:536
  56.7 0.6 %shard_map.212 = (bf16[16,512]{1,0:T(8,128)(2,1)}, bf16[16,128]{1,0:T(8,128)(2,1)}, bf16[16,128]{1,0:T(8,128)(2,1)}) custom-call(bf16[16,512]{1,0:T(8,128)(2,1)S(1)} %get-tuple-element.6.a, bf16[16,128]{1,0:T(8,128)(2,1)S(1)} %get-tuple-element.7.b, bf16[16,128]{1,0:T(8,128)(2,1)S(1)} %get-tuple-element.8.c), custom_call_target="tpu_custom_call" | custom-call | tf_op jit(solution)/shard_map/pallas_call | solution.py:579
